TPU v7x, 512 devices: a whole 4x4x16 slice. The times are simulated.
512 devices in a mesh: sp: 16 (over z), dp: 32 (over y, x, core).
Axes of the slice: x: 4, y: 4, z: 16, core: 2. Of those that a mesh axis runs over, the one named last changes fastest.
Arguments:
- stream_x: bfloat16 [32, 2048, 2048], P('dp', 'sp'), may hold values from -6 to 6
- stream_b: bfloat16 [32, 2048, 1024], P('dp', 'sp'), may hold values from -6 to 6
- stream_c: bfloat16 [32, 2048, 1024], P('dp', 'sp'), may hold values from -6 to 6
- gate_z: bfloat16 [32, 2048, 2048], P('dp', 'sp'), may hold values from -6 to 6
- step_raw: bfloat16 [32, 2048, 32], P('dp', 'sp'), may hold values from -4 to 3
- conv_x: bfloat16 [4, 2048], P(None, 'sp'), may hold values from -3 to 3
- conv_b: bfloat16 [4, 1024], replicated, may hold values from -3 to 3
- conv_c: bfloat16 [4, 1024], replicated, may hold values from -3 to 3
- decay_log: float32 [32], P('sp'), may hold values from -20 to 0
- norm_gain: float32 [2048], replicated, may hold values from 0.1 to 1.9
- w_out: bfloat16 [2048, 2048], P('dp'), may hold values from -0.125 to 0.125
Outputs:
- mixed: bfloat16 [32, 2048, 2048], P('dp', 'sp')
All inputs are finite; a program needn't handle non-finite values.
Results may differ from a plain program's by a relative error of at most 0.011.
Values may be sent and summed in bfloat16 or wider, within the bound.
No kernel may reach another device: no remote copies, remote signals or barrier semaphores. Data moves between devices by JAX's collectives and lax.ppermute only.
A program may use at most 64 MiB of HBM per device.

v0:
```python
import jax
import jax.numpy as jnp
from jax import lax
from jax.experimental import pallas as pl
from jax.experimental.pallas import tpu as pltpu
from jax.sharding import PartitionSpec as P

HEAD_DIM = 64
STATE = 128
RATIO = 4
NORM_EPS = 1.0
HIGHEST = lax.Precision.HIGHEST
F32 = jnp.float32
BF16 = jnp.bfloat16
HALO = 8


def silu(u):
    return 0.5 * u * (1.0 + jnp.tanh(0.5 * u))


def conv_silu(pad_ref, halo, value, taps):
    rows = value.shape[0]
    pad_ref[0:HALO, :] = halo.astype(F32)
    pad_ref[HALO : HALO + rows, :] = value.astype(F32)
    total = taps[3:4, :] * pad_ref[HALO : HALO + rows, :]
    for back in range(1, 4):
        total = total + taps[3 - back : 4 - back, :] * pad_ref[HALO - back : HALO - back + rows, :]
    return silu(total).astype(BF16)


def per_head(columns, first, width):
    tokens = columns.shape[0]
    lane = lax.broadcasted_iota(jnp.int32, (tokens, 128), 1)
    pieces = []
    for pair in range(width // 128):
        left = jnp.broadcast_to(columns[:, first + 2 * pair : first + 2 * pair + 1], (tokens, 128))
        right = jnp.broadcast_to(
            columns[:, first + 2 * pair + 1 : first + 2 * pair + 2], (tokens, 128)
        )
        pieces.append(jnp.where(lane < HEAD_DIM, left, right))
    return jnp.concatenate(pieces, axis=1)


def state_kernel(
    x_ref, b_ref, hx_ref, hb_ref, shared_ref, tb_ref, dt_ref,
    state_ref, xin_ref, bin_ref, cum_ref, padx_ref, padb_ref,
):
    tokens = x_ref.shape[0]
    taps_x = jnp.concatenate([shared_ref[0], shared_ref[1]], axis=1)
    xin = conv_silu(padx_ref, hx_ref[...], x_ref[...], taps_x)
    bin_ = conv_silu(padb_ref, hb_ref[...], b_ref[...], tb_ref[...].astype(F32))
    xin_ref[...] = xin
    bin_ref[...] = bin_
    dt = dt_ref[0]
    logs = jnp.concatenate([shared_ref[0, 4:6, :], shared_ref[1, 4:6, :]], axis=0)
    la = -jnp.exp(logs) * dt
    src = lax.broadcasted_iota(jnp.int32, (tokens, tokens), 0)
    dst = lax.broadcasted_iota(jnp.int32, (tokens, tokens), 1)
    upper = (src <= dst).astype(F32)
    both = jnp.concatenate([la, dt], axis=0)
    summed = jnp.dot(both, upper, precision=HIGHEST, preferred_element_type=F32)
    cum = summed[0:RATIO]
    packed = jnp.concatenate([cum, dt], axis=0)
    cum_ref[0] = packed
    last = cum[:, tokens - 1 : tokens]
    tail = jnp.exp(last - cum) * dt
    tails = jnp.concatenate([tail, tail], axis=0)
    columns = jnp.transpose(tails)
    scaled = (xin.astype(F32) * per_head(columns, 0, RATIO * HEAD_DIM)).astype(BF16)
    state = lax.dot_general(
        scaled, bin_, (((0,), (0,)), ((), ())), preferred_element_type=F32
    )
    state_ref[...] = state.astype(BF16)


def inner_kernel(c_ref, hc_ref, tc_ref, bin_ref, xin_ref, cum_ref, cin_ref, inner_ref, padc_ref):
    tokens = c_ref.shape[0]
    cin = conv_silu(padc_ref, hc_ref[...], c_ref[...], tc_ref[...].astype(F32))
    cin_ref[...] = cin
    scores = lax.dot_general(
        cin, bin_ref[...], (((1,), (1,)), ((), ())), preferred_element_type=F32
    )
    rows = cum_ref[0]
    columns = jnp.transpose(rows)
    row_id = lax.broadcasted_iota(jnp.int32, (tokens, tokens), 0)
    col_id = lax.broadcasted_iota(jnp.int32, (tokens, tokens), 1)
    causal = row_id >= col_id
    for head in range(RATIO):
        spread = columns[:, head : head + 1] - rows[head : head + 1, :]
        decay = jnp.exp(jnp.where(causal, spread, -jnp.inf))
        weights = (scores * decay * rows[RATIO + head : RATIO + head + 1, :]).astype(BF16)
        cols = slice(head * HEAD_DIM, (head + 1) * HEAD_DIM)
        inner_ref[:, cols] = jnp.dot(weights, xin_ref[:, cols], preferred_element_type=F32)


def scan_kernel(decay_ref, local_ref, out_ref):
    count = local_ref.shape[0]
    for head in range(2):
        rows = slice(head * HEAD_DIM, (head + 1) * HEAD_DIM)
        entering = jnp.zeros((HEAD_DIM, STATE), F32)
        for step in range(count):
            out_ref[step, rows, :] = entering.astype(BF16)
            if step + 1 < count:
                entering = entering * decay_ref[step, head] + local_ref[step, rows, :].astype(F32)


def out_kernel(
    ent_ref, cin_ref, inner_ref, cum_ref, z_ref, gain_ref, w_ref, out_ref, acc_ref
):
    group = pl.program_id(0)
    carried = lax.dot_general(
        cin_ref[...], ent_ref[...], (((1,), (1,)), ((), ())), preferred_element_type=F32
    )
    width = RATIO * HEAD_DIM
    columns = jnp.transpose(jnp.exp(cum_ref[0]))
    core = (inner_ref[...] + carried * per_head(columns, 0, width)).astype(BF16)
    v = core.astype(F32) * silu(z_ref[...].astype(F32))
    squares = v * v
    high = squares.astype(BF16)
    low = (squares - high.astype(F32)).astype(BF16)
    row_id = lax.broadcasted_iota(jnp.int32, (width, width), 0) // HEAD_DIM
    col_id = lax.broadcasted_iota(jnp.int32, (width, width), 1) // HEAD_DIM
    average = jnp.where(row_id == col_id, 1.0 / HEAD_DIM, 0.0).astype(BF16)
    mean = jnp.dot(high, average, preferred_element_type=F32) + jnp.dot(
        low, average, preferred_element_type=F32
    )
    normed = (v * lax.rsqrt(mean + NORM_EPS) * gain_ref[...]).astype(BF16)
    part = jnp.dot(normed, w_ref[...], preferred_element_type=F32)

    @pl.when(group == 0)
    def _():
        acc_ref[...] = part

    @pl.when(group > 0)
    def _():
        acc_ref[...] += part

    @pl.when(group == pl.num_programs(0) - 1)
    def _():
        out_ref[...] = acc_ref[...].astype(BF16)


def body(
    stream_x, stream_b, stream_c, gate_z, step_raw,
    conv_x, conv_b, conv_c, decay_log, norm_gain, w_out,
):
    ranks = lax.axis_size("sp")
    me = lax.axis_index("sp")
    x, b, c, z, raw = (v[0] for v in (stream_x, stream_b, stream_c, gate_z, step_raw))
    tokens, inner_width = x.shape
    groups = b.shape[1] // STATE
    heads = raw.shape[1]
    width = RATIO * HEAD_DIM
    own = heads // ranks

    dt = jax.nn.softplus(jnp.transpose(raw).astype(F32))
    sums = jnp.sum(dt, axis=1)
    small = jnp.concatenate(
        [
            conv_x.astype(F32),
            jnp.broadcast_to(decay_log[:, None], (own, 128)),
            jnp.pad(sums, (0, 128 - heads))[None],
            jnp.zeros((1, 128), F32),
        ]
    )
    shared = lax.all_to_all(
        jnp.broadcast_to(small[None], (ranks,) + small.shape), "sp", 0, 0, tiled=True
    )
    ends = jnp.concatenate([x[tokens - HALO :], b[tokens - HALO :], c[tokens - HALO :]], axis=1)
    halo = lax.ppermute(ends, "sp", [(i, i + 1) for i in range(ranks - 1)])
    w_full = lax.all_gather(w_out, "dp", axis=0, tiled=True)

    dt_group = dt.reshape(groups, RATIO, tokens)
    xb, bb = inner_width // STATE, groups
    state, xin, bin_, cum = pl.pallas_call(
        state_kernel,
        grid=(groups,),
        in_specs=[
            pl.BlockSpec((tokens, width), lambda g: (0, g)),
            pl.BlockSpec((tokens, STATE), lambda g: (0, g)),
            pl.BlockSpec((HALO, width), lambda g: (0, g)),
            pl.BlockSpec((HALO, STATE), lambda g: (0, xb + g)),
            pl.BlockSpec((2, 8, 128), lambda g: (g, 0, 0)),
            pl.BlockSpec((4, STATE), lambda g: (0, g)),
            pl.BlockSpec((1, RATIO, tokens), lambda g: (g, 0, 0)),
        ],
        out_specs=[
            pl.BlockSpec((width, STATE), lambda g: (g, 0)),
            pl.BlockSpec((tokens, width), lambda g: (0, g)),
            pl.BlockSpec((tokens, STATE), lambda g: (0, g)),
            pl.BlockSpec((1, 2 * RATIO, tokens), lambda g: (g, 0, 0)),
        ],
        out_shape=[
            jax.ShapeDtypeStruct((inner_width, STATE), BF16),
            jax.ShapeDtypeStruct((tokens, inner_width), BF16),
            jax.ShapeDtypeStruct((tokens, groups * STATE), BF16),
            jax.ShapeDtypeStruct((groups, 2 * RATIO, tokens), F32),
        ],
        scratch_shapes=[
            pltpu.VMEM((HALO + tokens, width), F32),
            pltpu.VMEM((HALO + tokens, STATE), F32),
        ],
        cost_estimate=pl.CostEstimate(
            flops=4_000_000_000, bytes_accessed=2_000_000, transcendentals=400_000
        ),
        name="state",
    )(x, b, halo, halo, shared, conv_b, dt_group)

    local = lax.all_to_all(
        state.reshape(ranks, inner_width // ranks, STATE), "sp", 0, 0, tiled=True
    )

    cin, inner = pl.pallas_call(
        inner_kernel,
        grid=(groups,),
        in_specs=[
            pl.BlockSpec((tokens, STATE), lambda g: (0, g)),
            pl.BlockSpec((HALO, STATE), lambda g: (0, xb + bb + g)),
            pl.BlockSpec((4, STATE), lambda g: (0, g)),
            pl.BlockSpec((tokens, STATE), lambda g: (0, g)),
            pl.BlockSpec((tokens, width), lambda g: (0, g)),
            pl.BlockSpec((1, 2 * RATIO, tokens), lambda g: (g, 0, 0)),
        ],
        out_specs=[
            pl.BlockSpec((tokens, STATE), lambda g: (0, g)),
            pl.BlockSpec((tokens, width), lambda g: (0, g)),
        ],
        out_shape=[
            jax.ShapeDtypeStruct((tokens, groups * STATE), BF16),
            jax.ShapeDtypeStruct((tokens, inner_width), F32),
        ],
        scratch_shapes=[pltpu.VMEM((HALO + tokens, STATE), F32)],
        cost_estimate=pl.CostEstimate(
            flops=4_000_000_000, bytes_accessed=2_000_000, transcendentals=700_000
        ),
        name="inner",
    )(c, halo, conv_c, bin_, xin, cum)

    own_sums = lax.dynamic_slice_in_dim(shared[:, 6, :], me * own, own, 1)
    decay = jnp.exp(own_sums * -jnp.exp(decay_log)[None, :])
    entering = pl.pallas_call(
        scan_kernel,
        in_specs=[
            pl.BlockSpec(memory_space=pltpu.SMEM),
            pl.BlockSpec(memory_space=pltpu.VMEM),
        ],
        out_specs=pl.BlockSpec(memory_space=pltpu.VMEM),
        out_shape=jax.ShapeDtypeStruct(local.shape, BF16),
        cost_estimate=pl.CostEstimate(
            flops=1_000_000_000, bytes_accessed=1_000_000, transcendentals=0
        ),
        name="scan",
    )(decay, local)
    entering = lax.all_to_all(entering, "sp", 0, 0, tiled=True).reshape(inner_width, STATE)

    mixed = pl.pallas_call(
        out_kernel,
        grid=(groups,),
        in_specs=[
            pl.BlockSpec((width, STATE), lambda g: (g, 0)),
            pl.BlockSpec((tokens, STATE), lambda g: (0, g)),
            pl.BlockSpec((tokens, width), lambda g: (0, g)),
            pl.BlockSpec((1, 2 * RATIO, tokens), lambda g: (g, 0, 0)),
            pl.BlockSpec((tokens, width), lambda g: (0, g)),
            pl.BlockSpec((1, width), lambda g: (0, g)),
            pl.BlockSpec((width, w_full.shape[1]), lambda g: (g, 0)),
        ],
        out_specs=pl.BlockSpec((tokens, w_full.shape[1]), lambda g: (0, 0)),
        out_shape=jax.ShapeDtypeStruct((tokens, w_full.shape[1]), BF16),
        scratch_shapes=[pltpu.VMEM((tokens, w_full.shape[1]), F32)],
        cost_estimate=pl.CostEstimate(
            flops=4_000_000_000, bytes_accessed=10_000_000, transcendentals=300_000
        ),
        name="project",
    )(entering, cin, inner, cum, z, norm_gain[None], w_full)
    return mixed[None]


def solution(mesh):
    placed = (
        P("dp", "sp", None),
        P("dp", "sp", None),
        P("dp", "sp", None),
        P("dp", "sp", None),
        P("dp", "sp", None),
        P(None, "sp"),
        P(),
        P(),
        P("sp"),
        P(),
        P("dp", None),
    )
    return jax.shard_map(
        body, mesh=mesh, in_specs=placed, out_specs=P("dp", "sp", None), check_vma=False
    )
```

profile of v0, /device:TPU:50, one launch (start us, length us, event | category | flops | bytes accessed | tf_op | source)
XLA Modules:
  0.0 138.3 jit_solution(7804547297248181233)
XLA Ops:
  6.5 0.0 copy-start.4
  6.5 0.0 all-gather.2.cloned.1.call-start
  6.5 0.7 all-gather.2.cloned.1.call-update
  7.3 0.7 convert_element_type.14
  7.9 0.1 pad.11.clone
  8.0 0.7 pad.9.clone
  8.7 1.4 %compare_select_fusion = (f32[32,128]{1,0:T(8,128)}, f32[32]{0:T(128)S(1)}) fusion(bf16[1,128,32]{1,2,0:T(8,128)(2,1)} %param.15), kind=kLoop, calls=%fused_computation.1 | loop fusion | flops 32736 | bytes 24704 | tf_op jit(solution)/shard_map/jit(softplus)/select_n | solution.py:157
  10.2 0.1 maximum_maximum_fusion
  10.2 0.6 broadcast_in_dim.28
  10.9 15.2 %all-to-all-start = ((f32[16,8,128]{2,1,0:T(8,128)}), f32[16,8,128]{2,1,0:T(8,128)S(1)}, u32[]{:S(2)}, u32[]{:S(2)}) async-start(f32[16,8,128]{2,1,0:T(8,128)} %broadcast_in_dim.28), calls=%async_computation | async-start | bytes 131072 | tf_op jit(solution)/shard_map/all_to_all | solution.py:167
  26.1 0.7 slice_bitcast_fusion.1
  26.8 0.8 slice_bitcast_fusion
  27.6 3.4 %collective-permute-start = (bf16[8,4096]{1,0:T(8,128)(2,1)S(1)}, bf16[8,4096]{1,0:T(8,128)(2,1)S(1)}, u32[]{:S(2)}, u32[]{:S(2)}) collective-permute-start(bf16[8,4096]{1,0:T(8,128)(2,1)S(1)} %pad_maximum_fusion), channel_id=1, source_target_pairs={{0,32},{32,64},{64,96},{96,128},{128,160},{160,192},{192,224},{224... | collective-permute-start | bytes 196616 | tf_op jit(solution)/shard_map/ppermute | solution.py:171
  31.0 3.0 %collective-permute-done.hx_ref.hb_ref.hc_ref = bf16[8,4096]{1,0:T(8,128)(2,1)S(1)} collective-permute-done((bf16[8,4096]{1,0:T(8,128)(2,1)S(1)}, bf16[8,4096]{1,0:T(8,128)(2,1)S(1)}, u32[]{:S(2)}, u32[]{:S(2)}) %collective-permute-start) | collective-permute-done | bytes 65568 | tf_op jit(solution)/shard_map/ppermute | solution.py:171
  33.9 0.0 copy-start.3
  33.9 3.7 %all-to-all-done.shared_ref = f32[16,8,128]{2,1,0:T(8,128)S(1)} async-done(((f32[16,8,128]{2,1,0:T(8,128)}), f32[16,8,128]{2,1,0:T(8,128)S(1)}, u32[]{:S(2)}, u32[]{:S(2)}) %all-to-all-start) | async-done | bytes 65568 | tf_op jit(solution)/shard_map/all_to_all | solution.py:167
  37.6 0.0 copy-start.2
  37.6 0.0 copy-done.3
  37.6 0.6 copy-done.2
  38.3 8.0 %state.1 = (bf16[2048,128]{1,0:T(8,128)(2,1)}, bf16[128,2048]{1,0:T(8,128)(2,1)}, bf16[128,1024]{1,0:T(8,128)(2,1)}, f32[8,8,128]{2,1,0:T(8,128)}) custom-call(bf16[128,2048]{1,0:T(8,128)(2,1)} %bitcast.50, bf16[128,1024]{1,0:T(8,128)(2,1)} %bitcast.51, bf16[8,4096]{1,0:T(8,128)(2,1)} %copy-done.3, bf16[8,4096]{1,0:T(8,128)(2,1)} %copy-done.3, ...), custom_call_target="tpu_custom_call" | custom-call | flops 4000000000 | bytes 2000000 | tf_op jit(solution)/shard_map/state/pallas_call | solution.py:176
  46.2 9.4 %all-to-all-start.1 = ((bf16[16,128,128]{2,1,0:T(8,128)(2,1)}), bf16[16,128,128]{2,1,0:T(8,128)(2,1)S(1)}, u32[]{:S(2)}, u32[]{:S(2)}) async-start(bf16[16,128,128]{2,1,0:T(8,128)(2,1)} %bitcast.46), calls=%async_computation.1 | async-start | bytes 1048576 | tf_op jit(solution)/shard_map/all_to_all | solution.py:210
  55.6 0.0 copy-done.4
  55.6 0.8 slice.28
  56.5 0.1 constant_dynamic-slice_fusion
  56.6 0.6 multiply_exponential_fusion.decay_ref
  57.2 25.6 %all-to-all-done.1.local_ref = bf16[16,128,128]{2,1,0:T(8,128)(2,1)S(1)} async-done(((bf16[16,128,128]{2,1,0:T(8,128)(2,1)}), bf16[16,128,128]{2,1,0:T(8,128)(2,1)S(1)}, u32[]{:S(2)}, u32[]{:S(2)}) %all-to-all-start.1) | async-done | bytes 524320 | tf_op jit(solution)/shard_map/all_to_all | solution.py:210
  82.8 0.0 copy-start
  82.8 0.8 copy-done
  83.6 2.0 %scan.1 = bf16[16,128,128]{2,1,0:T(8,128)(2,1)} custom-call(f32[16,2]{1,0:T(8,128)} %multiply_exponential_fusion.decay_ref, bf16[16,128,128]{2,1,0:T(8,128)(2,1)} %copy-done), custom_call_target="tpu_custom_call" | custom-call | flops 1000000000 | bytes 1000000 | tf_op jit(solution)/shard_map/scan/pallas_call | solution.py:242
  85.6 6.6 %all-to-all-start.2 = ((bf16[16,128,128]{2,1,0:T(8,128)(2,1)}), bf16[16,128,128]{2,1,0:T(8,128)(2,1)S(1)}, u32[]{:S(2)}, u32[]{:S(2)}) async-start(bf16[16,128,128]{2,1,0:T(8,128)(2,1)} %scan.1), calls=%async_computation.2 | async-start | bytes 1048576 | tf_op jit(solution)/shard_map/all_to_all | solution.py:255
  92.1 7.0 %inner.1 = (bf16[128,1024]{1,0:T(8,128)(2,1)}, f32[128,2048]{1,0:T(8,128)}) custom-call(bf16[128,1024]{1,0:T(8,128)(2,1)} %bitcast.52, bf16[8,4096]{1,0:T(8,128)(2,1)} %copy-done.3, bf16[4,1024]{1,0:T(4,128)(2,1)} %tc_ref.1, bf16[128,1024]{1,0:T(8,128)(2,1)} %get-tuple-element.12.bin_ref, bf16[128,2048]{1,0:T(8,128)(2,1)} %get-tuple-element.13.xin_ref, ...), custom_call_target="tpu_custom_call" | custom-call | flops 4000000000 | bytes 2000000 | tf_op jit(solution)/shard_map/inner/pallas_call | solution.py:214
  99.1 20.8 %all-to-all-done.2 = bf16[16,128,128]{2,1,0:T(8,128)(2,1)S(1)} async-done(((bf16[16,128,128]{2,1,0:T(8,128)(2,1)}), bf16[16,128,128]{2,1,0:T(8,128)(2,1)S(1)}, u32[]{:S(2)}, u32[]{:S(2)}) %all-to-all-start.2) | async-done | bytes 524320 | tf_op jit(solution)/shard_map/all_to_all | solution.py:255
  119.9 0.0 copy-start.1
  119.9 0.0 all-gather.2.cloned.1.call-done.w_ref
  119.9 0.8 copy-done.1
  120.7 10.8 %project.1 = bf16[128,2048]{1,0:T(8,128)(2,1)} custom-call(bf16[2048,128]{1,0:T(8,128)(2,1)} %bitcast.47, bf16[128,1024]{1,0:T(8,128)(2,1)} %get-tuple-element.15.cin_ref, f32[128,2048]{1,0:T(8,128)} %get-tuple-element.16.inner_ref, f32[8,8,128]{2,1,0:T(8,128)} %get-tuple-element.14.cum_ref, bf16[128,2048]{1,0:T(8,128)(2,1)} %bitcast.53, ...), custom_call_target="tpu_custom_call" | custom-call | flops 4000000000 | bytes 10000000 | tf_op jit(solution)/shard_map/project/pallas_call | solution.py:257
  (3 shorter events, 0.0 us)
Async XLA Ops:
  6.5 49.1 %copy-start.4 = (f32[2]{0:T(128)S(1)}, f32[2]{0:T(128)}, u32[]{:S(2)}) copy-start(f32[2]{0:T(128)} %param.19) | copy-start | bytes 28
  6.5 113.4 %all-gather.2.cloned.1.call-start = ((), (), s32[]{:S(2)}) async-start(), calls=%async_computation.3 | async-start | bytes 8650752 | tf_op jit(solution)/shard_map/all_gather | solution.py:172
  10.9 26.7 %all-to-all-start = ((f32[16,8,128]{2,1,0:T(8,128)}), f32[16,8,128]{2,1,0:T(8,128)S(1)}, u32[]{:S(2)}, u32[]{:S(2)}) async-start(f32[16,8,128]{2,1,0:T(8,128)} %broadcast_in_dim.28), calls=%async_computation | async-start | bytes 131072 | tf_op jit(solution)/shard_map/all_to_all | solution.py:167
  27.6 6.3 %collective-permute-start = (bf16[8,4096]{1,0:T(8,128)(2,1)S(1)}, bf16[8,4096]{1,0:T(8,128)(2,1)S(1)}, u32[]{:S(2)}, u32[]{:S(2)}) collective-permute-start(bf16[8,4096]{1,0:T(8,128)(2,1)S(1)} %pad_maximum_fusion), channel_id=1, source_target_pairs={{0,32},{32,64},{64,96},{96,128},{128,160},{160,192},{192,224},{224... | collective-permute-start | bytes 196616 | tf_op jit(solution)/shard_map/ppermute | solution.py:171
  33.9 3.7 %copy-start.3 = (bf16[8,4096]{1,0:T(8,128)(2,1)}, bf16[8,4096]{1,0:T(8,128)(2,1)S(1)}, u32[]{:S(2)}) copy-start(bf16[8,4096]{1,0:T(8,128)(2,1)S(1)} %collective-permute-done.hx_ref.hb_ref.hc_ref) | copy-start | bytes 196612
  37.6 0.6 copy-start.2
  46.2 36.5 %all-to-all-start.1 = ((bf16[16,128,128]{2,1,0:T(8,128)(2,1)}), bf16[16,128,128]{2,1,0:T(8,128)(2,1)S(1)}, u32[]{:S(2)}, u32[]{:S(2)}) async-start(bf16[16,128,128]{2,1,0:T(8,128)(2,1)} %bitcast.46), calls=%async_computation.1 | async-start | bytes 1048576 | tf_op jit(solution)/shard_map/all_to_all | solution.py:210
  82.8 0.8 copy-start
  85.6 34.3 %all-to-all-start.2 = ((bf16[16,128,128]{2,1,0:T(8,128)(2,1)}), bf16[16,128,128]{2,1,0:T(8,128)(2,1)S(1)}, u32[]{:S(2)}, u32[]{:S(2)}) async-start(bf16[16,128,128]{2,1,0:T(8,128)(2,1)} %scan.1), calls=%async_computation.2 | async-start | bytes 1048576 | tf_op jit(solution)/shard_map/all_to_all | solution.py:255
  119.9 0.8 copy-start.1
Sparse Core Ops, SparseCore 0:
  10.5 70.5 all-gather.1
where the time goes:
time: 140 us; the launch traced here: 138 us
  waiting for transfers between devices  53.8 us (38%)
  starting transfers between devices  34.6 us (25%)
  Pallas kernels  27.7 us (20%)
  between operations  13.4 us (10%)
  local copies, waits for them, and re-layouts  6.1 us (4%)
  other arithmetic  2.8 us (2%)
    all_to_all x1, waiting for transfers between devices, body(): lax.all_to_all(state.reshape(ranks, inner_width // ranks, STATE), 'sp', 0...  25.6 us
    all_to_all x1, waiting for transfers between devices, body(): lax.all_to_all(entering, 'sp', 0, 0, tiled=True).reshape(inner_width, STATE)  20.8 us
    all_to_all x1, starting transfers between devices, body(): lax.all_to_all(jnp.broadcast_to(small[None], (ranks,) + small.shape), 'sp...  15.2 us
    pallas_call x1, Pallas kernels, body(): pl.pallas_call(out_kernel, grid=(groups,), in_specs=[pl.BlockSpec((width,...  10.8 us
    all_to_all x1, starting transfers between devices, body(): lax.all_to_all(state.reshape(ranks, inner_width // ranks, STATE), 'sp', 0...  9.4 us
    pallas_call x1, Pallas kernels, body(): pl.pallas_call(state_kernel, grid=(groups,), in_specs=[pl.BlockSpec((toke...  7.96 us
    pallas_call x1, Pallas kernels, body(): pl.pallas_call(inner_kernel, grid=(groups,), in_specs=[pl.BlockSpec((toke...  6.96 us
    all_to_all x1, starting transfers between devices, body(): lax.all_to_all(entering, 'sp', 0, 0, tiled=True).reshape(inner_width, STATE)  6.57 us
  transfers between devices with their start and end apart: 5, of which 4 were waited for; matrix products, arithmetic and copies ran while one was open for 5% of the time, Pallas kernels for 12%

commit v1 on v0

v1 whole, which is shorter than its diff:
```python
import jax
import jax.numpy as jnp
from jax import lax
from jax.experimental import pallas as pl
from jax.experimental.pallas import tpu as pltpu
from jax.sharding import PartitionSpec as P

HEAD_DIM = 64
STATE = 128
RATIO = 4
WIDTH = RATIO * HEAD_DIM
NORM_EPS = 1.0
HIGHEST = lax.Precision.HIGHEST
F32 = jnp.float32
BF16 = jnp.bfloat16
HALO = 4
PAD = 8
CHUNKS = 4
MIB = 1 << 20


def silu(u):
    half = 0.5 * u
    return half + half * jnp.tanh(half)


def conv_silu(pad_ref, halo, value, taps):
    rows = value.shape[0]
    pad_ref[PAD - HALO : PAD, :] = halo.astype(F32)
    pad_ref[PAD : PAD + rows, :] = value.astype(F32)
    total = taps[3:4, :] * pad_ref[PAD : PAD + rows, :]
    for back in range(1, 4):
        total = total + taps[3 - back : 4 - back, :] * pad_ref[PAD - back : PAD - back + rows, :]
    return silu(total)


def per_head(columns, first):
    tokens = columns.shape[0]
    lane = lax.broadcasted_iota(jnp.int32, (tokens, 128), 1)
    left = jnp.broadcast_to(columns[:, first : first + 1], (tokens, 128))
    right = jnp.broadcast_to(columns[:, first + 1 : first + 2], (tokens, 128))
    return jnp.where(lane < HEAD_DIM, left, right)


def share_kernel(decay_ref, raw_ref, taps_ref, x_ref, b_ref, c_ref, small_ref, ends_ref, dt_ref):
    tokens, heads = raw_ref.shape
    ranks = small_ref.shape[0]
    raw = jnp.transpose(raw_ref[...].astype(F32))
    dt = jnp.maximum(raw, 0.0) + jnp.log1p(jnp.exp(-jnp.abs(raw)))
    src = lax.broadcasted_iota(jnp.int32, (tokens, tokens), 0)
    dst = lax.broadcasted_iota(jnp.int32, (tokens, tokens), 1)
    upper = (src <= dst).astype(F32)
    prefix = jnp.dot(dt, upper, precision=HIGHEST, preferred_element_type=F32)
    for group in range(heads // RATIO):
        rows = slice(group * RATIO, (group + 1) * RATIO)
        dt_ref[group, 0:RATIO, :] = prefix[rows]
        dt_ref[group, RATIO:, :] = dt[rows]
    ones = jnp.ones((8, tokens), F32)
    sums = lax.dot_general(
        ones, dt, (((1,), (1,)), ((), ())), precision=HIGHEST, preferred_element_type=F32
    )
    small = jnp.concatenate(
        [
            taps_ref[...].astype(F32),
            jnp.full((1, 128), decay_ref[0], F32),
            jnp.full((1, 128), decay_ref[1], F32),
            jnp.concatenate([sums[0:1], jnp.zeros((1, 128 - heads), F32)], axis=1),
            jnp.zeros((1, 128), F32),
        ],
        axis=0,
    )
    for rank in range(ranks):
        small_ref[rank] = small
    left = 0
    for ref in (x_ref, b_ref, c_ref):
        cols = ref.shape[1]
        ends_ref[:, left : left + cols] = ref[ref.shape[0] - HALO :, :]
        left += cols


def state_kernel(
    x_ref, b_ref, hx_ref, hb_ref, shared_ref, tb_ref, dt_ref,
    state_ref, xin_ref, bin_ref, cum_ref, padx_ref, padb_ref,
):
    tokens = x_ref.shape[0]
    for k in range(dt_ref.shape[0]):
        wide = slice(k * WIDTH, (k + 1) * WIDTH)
        thin = slice(k * STATE, (k + 1) * STATE)
        rows = dt_ref[k]
        logs = jnp.concatenate(
            [shared_ref[2 * k, 4:6, :], shared_ref[2 * k + 1, 4:6, :]], axis=0
        )
        cum = -jnp.exp(logs) * rows[0:RATIO]
        dt = rows[RATIO:]
        cum_ref[k] = jnp.concatenate([cum, dt], axis=0)
        tail = jnp.exp(cum[:, tokens - 1 : tokens] - cum) * dt
        columns = jnp.transpose(jnp.concatenate([tail, tail], axis=0))
        taps_x = jnp.concatenate([shared_ref[2 * k, 0:4], shared_ref[2 * k + 1, 0:4]], axis=1)
        xin = conv_silu(padx_ref.at[k], hx_ref[:, wide], x_ref[:, wide], taps_x)
        xin = xin.astype(BF16)
        bin_ = conv_silu(padb_ref.at[k], hb_ref[:, thin], b_ref[:, thin], tb_ref[:, thin].astype(F32))
        bin_ = bin_.astype(BF16)
        xin_ref[:, wide] = xin
        bin_ref[:, thin] = bin_
        scale = jnp.concatenate([per_head(columns, 0), per_head(columns, 2)], axis=1)
        scaled = (xin.astype(F32) * scale).astype(BF16)
        state = lax.dot_general(
            bin_, scaled, (((0,), (0,)), ((), ())), preferred_element_type=F32
        ).astype(BF16)
        state_ref[2 * k] = state[:, :STATE]
        state_ref[2 * k + 1] = state[:, STATE:]


def inner_kernel(c_ref, hc_ref, tc_ref, bin_ref, xin_ref, cum_ref, cin_ref, inner_ref, padc_ref):
    tokens = c_ref.shape[0]
    cin = conv_silu(padc_ref, hc_ref[...], c_ref[...], tc_ref[...].astype(F32)).astype(BF16)
    cin_ref[...] = cin
    scores = lax.dot_general(
        cin, bin_ref[...], (((1,), (1,)), ((), ())), preferred_element_type=F32
    )
    rows = cum_ref[0]
    columns = jnp.transpose(rows)
    row_id = lax.broadcasted_iota(jnp.int32, (tokens, tokens), 0)
    col_id = lax.broadcasted_iota(jnp.int32, (tokens, tokens), 1)
    causal = row_id >= col_id
    for head in range(RATIO):
        spread = columns[:, head : head + 1] - rows[head : head + 1, :]
        decay = jnp.exp(jnp.where(causal, spread, -jnp.inf))
        weights = (scores * decay * rows[RATIO + head : RATIO + head + 1, :]).astype(BF16)
        cols = slice(head * HEAD_DIM, (head + 1) * HEAD_DIM)
        inner_ref[:, cols] = jnp.dot(weights, xin_ref[:, cols], preferred_element_type=F32)


def scan_kernel(decay_ref, local_ref, out_ref):
    count = local_ref.shape[0]
    for part in range(STATE // 32):
        rows = slice(part * 32, (part + 1) * 32)
        entering = jnp.zeros((32, 2 * HEAD_DIM), F32)
        for step in range(count):
            out_ref[step, rows, :] = entering.astype(BF16)
            if step + 1 < count:
                entering = entering * decay_ref[step : step + 1, :] + local_ref[
                    step, rows, :
                ].astype(F32)


def out_kernel(
    ent_ref, cin_ref, inner_ref, cum_ref, z_ref, gain_ref, w_ref, out_ref, normed_ref, held_ref, sems
):
    chunk = w_ref.shape[1] // CHUNKS
    copies = []
    for k in range(CHUNKS):
        cols = slice(k * chunk, (k + 1) * chunk)
        copies.append(
            pltpu.make_async_copy(w_ref.at[:, cols], held_ref.at[:, cols], sems.at[k])
        )
        copies[k].start()
    row_id = lax.broadcasted_iota(jnp.int32, (STATE, STATE), 0) // HEAD_DIM
    col_id = lax.broadcasted_iota(jnp.int32, (STATE, STATE), 1) // HEAD_DIM
    average = jnp.where(row_id == col_id, 1.0 / HEAD_DIM, 0.0).astype(BF16)
    for group in range(cum_ref.shape[0]):
        columns = jnp.transpose(jnp.exp(cum_ref[group]))
        cin = cin_ref[:, group * STATE : (group + 1) * STATE]
        for half in range(2):
            pair = 2 * group + half
            cols = slice(pair * STATE, (pair + 1) * STATE)
            carried = jnp.dot(cin, ent_ref[pair], preferred_element_type=F32)
            core = inner_ref[:, cols] + carried * per_head(columns, 2 * half)
            v = core.astype(BF16).astype(F32) * silu(z_ref[:, cols].astype(F32))
            squares = v * v
            high = squares.astype(BF16)
            low = (squares - high.astype(F32)).astype(BF16)
            mean = jnp.dot(high, average, preferred_element_type=F32) + jnp.dot(
                low, average, preferred_element_type=F32
            )
            normed = v * lax.rsqrt(mean + NORM_EPS) * gain_ref[:, cols]
            normed_ref[:, cols] = normed.astype(BF16)
    for k in range(CHUNKS):
        cols = slice(k * chunk, (k + 1) * chunk)
        copies[k].wait()
        out_ref[:, cols] = jnp.dot(
            normed_ref[...], held_ref[:, cols], preferred_element_type=F32
        ).astype(BF16)


def vmem():
    return pl.BlockSpec(memory_space=pltpu.VMEM)


def cost(flops, moved, special):
    return pl.CostEstimate(flops=flops, bytes_accessed=moved, transcendentals=special)


def body(
    stream_x, stream_b, stream_c, gate_z, step_raw,
    conv_x, conv_b, conv_c, decay_log, norm_gain, w_out,
):
    ranks = lax.axis_size("sp")
    me = lax.axis_index("sp")
    x, b, c, z, raw = (v[0] for v in (stream_x, stream_b, stream_c, gate_z, step_raw))
    tokens, inner_width = x.shape
    groups = b.shape[1] // STATE
    heads = raw.shape[1]
    own = heads // ranks
    thin = groups * STATE
    last = tokens // 8 - 1

    w_full = lax.all_gather(w_out, "dp", axis=0, tiled=True)

    small, ends, dt = pl.pallas_call(
        share_kernel,
        grid=(1,),
        in_specs=[
            pl.BlockSpec(memory_space=pltpu.SMEM),
            pl.BlockSpec((tokens, heads), lambda i: (0, 0)),
            pl.BlockSpec((4, 128), lambda i: (0, 0)),
            pl.BlockSpec((8, inner_width), lambda i: (last, 0)),
            pl.BlockSpec((8, thin), lambda i: (last, 0)),
            pl.BlockSpec((8, thin), lambda i: (last, 0)),
        ],
        out_specs=[
            pl.BlockSpec((ranks, 8, 128), lambda i: (0, 0, 0)),
            pl.BlockSpec((HALO, inner_width + 2 * thin), lambda i: (0, 0)),
            pl.BlockSpec((groups, 2 * RATIO, tokens), lambda i: (0, 0, 0)),
        ],
        out_shape=[
            jax.ShapeDtypeStruct((ranks, 8, 128), F32),
            jax.ShapeDtypeStruct((HALO, inner_width + 2 * thin), BF16),
            jax.ShapeDtypeStruct((groups, 2 * RATIO, tokens), F32),
        ],
        compiler_params=pltpu.CompilerParams(vmem_limit_bytes=8 * MIB),
        cost_estimate=cost(10_000_000, 200_000, 10_000),
        name="share",
    )(decay_log, raw, conv_x, x, b, c)
    shared = lax.all_to_all(small, "sp", 0, 0, tiled=True)
    halo = lax.ppermute(ends, "sp", [(i, i + 1) for i in range(ranks - 1)])

    xb, bb = inner_width // STATE, groups
    per = 2
    state, xin, bin_, cum = pl.pallas_call(
        state_kernel,
        grid=(groups // per,),
        in_specs=[
            pl.BlockSpec((tokens, per * WIDTH), lambda g: (0, g)),
            pl.BlockSpec((tokens, per * STATE), lambda g: (0, g)),
            pl.BlockSpec((HALO, per * WIDTH), lambda g: (0, g)),
            pl.BlockSpec((HALO, per * STATE), lambda g: (0, xb // per + g)),
            pl.BlockSpec((2 * per, 8, 128), lambda g: (g, 0, 0)),
            pl.BlockSpec((4, per * STATE), lambda g: (0, g)),
            pl.BlockSpec((per, 2 * RATIO, tokens), lambda g: (g, 0, 0)),
        ],
        out_specs=[
            pl.BlockSpec((2 * per, STATE, STATE), lambda g: (g, 0, 0)),
            pl.BlockSpec((tokens, per * WIDTH), lambda g: (0, g)),
            pl.BlockSpec((tokens, per * STATE), lambda g: (0, g)),
            pl.BlockSpec((per, 2 * RATIO, tokens), lambda g: (g, 0, 0)),
        ],
        out_shape=[
            jax.ShapeDtypeStruct((ranks, STATE, inner_width // ranks), BF16),
            jax.ShapeDtypeStruct((tokens, inner_width), BF16),
            jax.ShapeDtypeStruct((tokens, thin), BF16),
            jax.ShapeDtypeStruct((groups, 2 * RATIO, tokens), F32),
        ],
        scratch_shapes=[
            pltpu.VMEM((per, PAD + tokens, WIDTH), F32),
            pltpu.VMEM((per, PAD + tokens, STATE), F32),
        ],
        compiler_params=pltpu.CompilerParams(vmem_limit_bytes=16 * MIB),
        cost_estimate=cost(4_000_000_000, 2_000_000, 400_000),
        name="state",
    )(x, b, halo, halo, shared, conv_b, dt)

    local = lax.all_to_all(state, "sp", 0, 0, tiled=True)

    cin, inner = pl.pallas_call(
        inner_kernel,
        grid=(groups,),
        in_specs=[
            pl.BlockSpec((tokens, STATE), lambda g: (0, g)),
            pl.BlockSpec((HALO, STATE), lambda g: (0, xb + bb + g)),
            pl.BlockSpec((4, STATE), lambda g: (0, g)),
            pl.BlockSpec((tokens, STATE), lambda g: (0, g)),
            pl.BlockSpec((tokens, WIDTH), lambda g: (0, g)),
            pl.BlockSpec((1, 2 * RATIO, tokens), lambda g: (g, 0, 0)),
        ],
        out_specs=[
            pl.BlockSpec((tokens, STATE), lambda g: (0, g)),
            pl.BlockSpec((tokens, WIDTH), lambda g: (0, g)),
        ],
        out_shape=[
            jax.ShapeDtypeStruct((tokens, thin), BF16),
            jax.ShapeDtypeStruct((tokens, inner_width), F32),
        ],
        scratch_shapes=[pltpu.VMEM((PAD + tokens, STATE), F32)],
        compiler_params=pltpu.CompilerParams(vmem_limit_bytes=16 * MIB),
        cost_estimate=cost(4_000_000_000, 2_000_000, 700_000),
        name="inner",
    )(c, halo, conv_c, bin_, xin, cum)

    own_sums = lax.dynamic_slice_in_dim(shared[:, 6, :], me * own, own, 1)
    decay = jnp.repeat(jnp.exp(own_sums * -jnp.exp(decay_log)[None, :]), HEAD_DIM, axis=1)
    entering = pl.pallas_call(
        scan_kernel,
        in_specs=[vmem(), vmem()],
        out_specs=vmem(),
        out_shape=jax.ShapeDtypeStruct(local.shape, BF16),
        compiler_params=pltpu.CompilerParams(vmem_limit_bytes=8 * MIB),
        cost_estimate=cost(1_000_000_000, 1_000_000, 0),
        name="scan",
    )(decay, local)
    entering = lax.all_to_all(entering, "sp", 0, 0, tiled=True)

    mixed = pl.pallas_call(
        out_kernel,
        in_specs=[vmem()] * 6 + [pl.BlockSpec(memory_space=pltpu.HBM)],
        out_specs=vmem(),
        out_shape=jax.ShapeDtypeStruct((tokens, w_full.shape[1]), BF16),
        scratch_shapes=[
            pltpu.VMEM((tokens, inner_width), BF16),
            pltpu.VMEM(w_full.shape, BF16),
            pltpu.SemaphoreType.DMA((CHUNKS,)),
        ],
        compiler_params=pltpu.CompilerParams(vmem_limit_bytes=24 * MIB),
        cost_estimate=cost(4_000_000_000, 10_000_000, 300_000),
        name="project",
    )(entering, cin, inner, cum, z, norm_gain[None], w_full)
    return mixed[None]


def solution(mesh):
    placed = (
        P("dp", "sp", None),
        P("dp", "sp", None),
        P("dp", "sp", None),
        P("dp", "sp", None),
        P("dp", "sp", None),
        P(None, "sp"),
        P(),
        P(),
        P("sp"),
        P(),
        P("dp", None),
    )
    return jax.shard_map(
        body, mesh=mesh, in_specs=placed, out_specs=P("dp", "sp", None), check_vma=False
    )
```

time: 140 us -> 134 us (0.957)
  the two profiles are of different devices: /device:TPU:50 before, /device:TPU:54 now
where the time goes in v1:
time: 134 us; the launch traced here: 133 us
  waiting for transfers between devices  59.1 us (44%)
  starting transfers between devices  32.7 us (24%)
  Pallas kernels  16 us (12%)
  between operations  13.5 us (10%)
  local copies, waits for them, and re-layouts  11.6 us (9%)
    all_to_all x1, waiting for transfers between devices, body(): local = lax.all_to_all(state, 'sp', 0, 0, tiled=True)  26.6 us
    all_to_all x1, waiting for transfers between devices, body(): entering = lax.all_to_all(entering, 'sp', 0, 0, tiled=True)  23.6 us
    all_to_all x1, starting transfers between devices, body(): shared = lax.all_to_all(small, 'sp', 0, 0, tiled=True)  15.2 us
    unnamed x29, local copies, waits for them, and re-layouts  11.2 us
    all_to_all x1, starting transfers between devices, body(): local = lax.all_to_all(state, 'sp', 0, 0, tiled=True)  7.51 us
    all_to_all x1, starting transfers between devices, body(): entering = lax.all_to_all(entering, 'sp', 0, 0, tiled=True)  6.66 us
    pallas_call x1, Pallas kernels, body(): pl.pallas_call(out_kernel, in_specs=[vmem()] * 6 + [pl.BlockSpec(memory_s...  5.72 us
    all_to_all x1, waiting for transfers between devices, body(): shared = lax.all_to_all(small, 'sp', 0, 0, tiled=True)  5.51 us
  transfers between devices with their start and end apart: 5, of which 4 were waited for; matrix products, arithmetic and copies ran while one was open for 1% of the time, Pallas kernels for 8%

profile of v1, /device:TPU:54, one launch (start us, length us, event | category | flops | bytes accessed | tf_op | source)
XLA Modules:
  0.0 133.0 jit_solution(200868926665717594)
XLA Ops:
  6.5 0.0 all-gather.2.cloned.1.call-start
  6.5 0.7 all-gather.2.cloned.1.call-update
  7.3 0.8 copy.12
  8.1 0.0 copy-start
  8.1 1.0 copy-done
  9.1 0.0 copy-start.2
  9.1 0.9 copy-done.2
  10.1 0.0 copy-start.4
  10.1 0.9 copy-done.4
  11.0 0.0 copy-start.6
  11.0 0.7 copy-done.6
  11.7 0.0 copy-start.7
  11.7 0.7 copy-done.7
  12.4 0.0 copy-start.8
  12.4 1.4 %share.1 = (f32[16,8,128]{2,1,0:T(8,128)}, bf16[4,4096]{1,0:T(4,128)(2,1)S(1)}, f32[8,8,128]{2,1,0:T(8,128)S(1)}) custom-call(f32[2]{0:T(128)S(1)} %copy-done.7, bf16[128,32]{1,0:T(8,128)(2,1)S(1)} %bitcast.17, bf16[4,128]{1,0:T(4,128)(2,1)S(1)} %copy-done.6, bf16[128,2048]{1,0:T(8,128)(2,1)S(1)} %bitcast.11, bf16[128,1024]{1,0:T(8,128)(2,1)S(1)} %bitcast.13, ...), custom_call_target="tpu_custom_call" | custom-call | flops 10000000 | bytes 200000 | tf_op jit(solution)/shard_map/share/pallas_call | solution.py:210
  13.8 15.2 %all-to-all-start = ((f32[16,8,128]{2,1,0:T(8,128)}), f32[16,8,128]{2,1,0:T(8,128)S(1)}, u32[]{:S(2)}, u32[]{:S(2)}) async-start(f32[16,8,128]{2,1,0:T(8,128)} %get-tuple-element.14), calls=%async_computation | async-start | bytes 131072 | tf_op jit(solution)/shard_map/all_to_all | solution.py:235
  29.0 3.4 %collective-permute-start = (bf16[4,4096]{1,0:T(4,128)(2,1)S(1)}, bf16[4,4096]{1,0:T(4,128)(2,1)S(1)}, u32[]{:S(2)}, u32[]{:S(2)}) collective-permute-start(bf16[4,4096]{1,0:T(4,128)(2,1)S(1)} %get-tuple-element.15), channel_id=1, source_target_pairs={{0,32},{32,64},{64,96},{96,128},{128,160},{160,192},{192,224},{224... | collective-permute-start | bytes 98312 | tf_op jit(solution)/shard_map/ppermute | solution.py:236
  32.4 2.7 %collective-permute-done.hx_ref.hb_ref.hc_ref = bf16[4,4096]{1,0:T(4,128)(2,1)S(1)} collective-permute-done((bf16[4,4096]{1,0:T(4,128)(2,1)S(1)}, bf16[4,4096]{1,0:T(4,128)(2,1)S(1)}, u32[]{:S(2)}, u32[]{:S(2)}) %collective-permute-start) | collective-permute-done | bytes 32800 | tf_op jit(solution)/shard_map/ppermute | solution.py:236
  35.0 5.5 %all-to-all-done.shared_ref = f32[16,8,128]{2,1,0:T(8,128)S(1)} async-done(((f32[16,8,128]{2,1,0:T(8,128)}), f32[16,8,128]{2,1,0:T(8,128)S(1)}, u32[]{:S(2)}, u32[]{:S(2)}) %all-to-all-start) | async-done | bytes 65568 | tf_op jit(solution)/shard_map/all_to_all | solution.py:235
  40.5 0.0 copy-start.1
  40.5 1.0 copy-done.1
  41.6 0.0 copy-start.3
  41.6 0.9 copy-done.3
  42.5 0.0 copy-start.11
  42.5 0.7 copy-done.11
  43.2 0.0 copy-start.5
  43.2 0.0 copy-start.12
  43.2 3.8 %state.1 = (bf16[16,128,128]{2,1,0:T(8,128)(2,1)}, bf16[128,2048]{1,0:T(8,128)(2,1)S(1)}, bf16[128,1024]{1,0:T(8,128)(2,1)S(1)}, f32[8,8,128]{2,1,0:T(8,128)S(1)}) custom-call(bf16[128,2048]{1,0:T(8,128)(2,1)S(1)} %bitcast.12, bf16[128,1024]{1,0:T(8,128)(2,1)S(1)} %bitcast.14, bf16[4,4096]{1,0:T(4,128)(2,1)S(1)} %collective-permute-done.hx_ref.hb_ref.hc_ref, ...), custom_call_target="tpu_custom_call" | custom-call | flops 4000000000 | bytes 2000000 | tf_op jit(solution)/shard_map/state/pallas_call | solution.py:240
  47.0 7.5 %all-to-all-start.1 = ((bf16[16,128,128]{2,1,0:T(8,128)(2,1)}), bf16[16,128,128]{2,1,0:T(8,128)(2,1)S(1)}, u32[]{:S(2)}, u32[]{:S(2)}) async-start(bf16[16,128,128]{2,1,0:T(8,128)(2,1)} %get-tuple-element.17), calls=%async_computation.1 | async-start | bytes 1048576 | tf_op jit(solution)/shard_map/all_to_all | solution.py:273
  54.5 0.0 copy-done.8
  54.6 0.1 constant_dynamic-slice_fusion
  54.7 0.1 copy.13
  54.7 0.1 fusion
  54.8 0.1 copy.14
  54.9 0.1 broadcast_in_dim.10
  55.0 0.1 reshape.6.decay_ref
  55.1 26.6 %all-to-all-done.1.local_ref = bf16[16,128,128]{2,1,0:T(8,128)(2,1)S(1)} async-done(((bf16[16,128,128]{2,1,0:T(8,128)(2,1)}), bf16[16,128,128]{2,1,0:T(8,128)(2,1)S(1)}, u32[]{:S(2)}, u32[]{:S(2)}) %all-to-all-start.1) | async-done | bytes 524320 | tf_op jit(solution)/shard_map/all_to_all | solution.py:273
  81.7 0.9 scan.1
  82.6 0.0 copy-start.10
  82.6 0.0 copy-start.13
  82.6 6.7 %all-to-all-start.2 = ((bf16[16,128,128]{2,1,0:T(8,128)(2,1)}), bf16[16,128,128]{2,1,0:T(8,128)(2,1)S(1)}, u32[]{:S(2)}, u32[]{:S(2)}) async-start(bf16[16,128,128]{2,1,0:T(8,128)(2,1)} %scan.1), calls=%async_computation.2 | async-start | bytes 1048576 | tf_op jit(solution)/shard_map/all_to_all | solution.py:311
  89.3 0.0 copy-done.5
  89.3 0.0 copy-done.12
  89.3 4.1 %inner.1 = (bf16[128,1024]{1,0:T(8,128)(2,1)S(1)}, f32[128,2048]{1,0:T(8,128)S(1)}) custom-call(bf16[128,1024]{1,0:T(8,128)(2,1)S(1)} %bitcast.16, bf16[4,4096]{1,0:T(4,128)(2,1)S(1)} %collective-permute-done.hx_ref.hb_ref.hc_ref, bf16[4,1024]{1,0:T(4,128)(2,1)S(1)} %copy-done.12, bf16[128,1024]{1,0:T(8,128)(2,1)S(1)} %get-tuple-element.18.bin_ref, ...), custom_call_target="tpu_custom_call" | custom-call | flops 4000000000 | bytes 2000000 | tf_op jit(solution)/shard_map/inner/pallas_call | solution.py:275
  93.4 23.6 %all-to-all-done.2.ent_ref = bf16[16,128,128]{2,1,0:T(8,128)(2,1)S(1)} async-done(((bf16[16,128,128]{2,1,0:T(8,128)(2,1)}), bf16[16,128,128]{2,1,0:T(8,128)(2,1)S(1)}, u32[]{:S(2)}, u32[]{:S(2)}) %all-to-all-start.2) | async-done | bytes 524320 | tf_op jit(solution)/shard_map/all_to_all | solution.py:311
  117.1 0.0 all-gather.2.cloned.1.call-done.w_ref
  117.1 0.0 copy-done.10
  117.1 0.0 copy-done.13
  117.1 0.0 copy-start.9
  117.1 3.4 %copy-done.9 = bf16[2048,2048]{1,0:T(8,128)(2,1)S(1)} copy-done((bf16[2048,2048]{1,0:T(8,128)(2,1)S(1)}, bf16[2048,2048]{1,0:T(8,128)(2,1)}, u32[]{:S(2)}) %copy-start.9) | copy-done | bytes 8388632
  120.4 5.7 %project.1 = bf16[128,2048]{1,0:T(8,128)(2,1)} custom-call(bf16[16,128,128]{2,1,0:T(8,128)(2,1)S(1)} %all-to-all-done.2.ent_ref, bf16[128,1024]{1,0:T(8,128)(2,1)S(1)} %get-tuple-element.21.cin_ref, f32[128,2048]{1,0:T(8,128)S(1)} %get-tuple-element.22.inner_ref, f32[8,8,128]{2,1,0:T(8,128)S(1)} %get-tuple-element.20.cum_ref, ...), custom_call_target="tpu_custom_call" | custom-call | flops 4000000000 | bytes 10000000 | tf_op jit(solution)/shard_map/project/pallas_call | solution.py:313
  (2 shorter events, 0.0 us)
Async XLA Ops:
  6.5 110.5 %all-gather.2.cloned.1.call-start = ((), (), s32[]{:S(2)}) async-start(), calls=%async_computation.3 | async-start | bytes 8650752 | tf_op jit(solution)/shard_map/all_gather | solution.py:208
  8.1 1.0 copy-start
  9.1 0.9 copy-start.2
  10.1 0.9 copy-start.4
  11.0 0.7 copy-start.6
  11.7 0.7 copy-start.7
  12.4 42.2 %copy-start.8 = (f32[2]{0:T(128)S(1)}, f32[2]{0:T(128)}, u32[]{:S(2)}) copy-start(f32[2]{0:T(128)} %decay_ref.1) | copy-start | bytes 28
  13.8 26.7 %all-to-all-start = ((f32[16,8,128]{2,1,0:T(8,128)}), f32[16,8,128]{2,1,0:T(8,128)S(1)}, u32[]{:S(2)}, u32[]{:S(2)}) async-start(f32[16,8,128]{2,1,0:T(8,128)} %get-tuple-element.14), calls=%async_computation | async-start | bytes 131072 | tf_op jit(solution)/shard_map/all_to_all | solution.py:235
  29.0 6.0 %collective-permute-start = (bf16[4,4096]{1,0:T(4,128)(2,1)S(1)}, bf16[4,4096]{1,0:T(4,128)(2,1)S(1)}, u32[]{:S(2)}, u32[]{:S(2)}) collective-permute-start(bf16[4,4096]{1,0:T(4,128)(2,1)S(1)} %get-tuple-element.15), channel_id=1, source_target_pairs={{0,32},{32,64},{64,96},{96,128},{128,160},{160,192},{192,224},{224... | collective-permute-start | bytes 98312 | tf_op jit(solution)/shard_map/ppermute | solution.py:236
  40.5 1.0 copy-start.1
  41.6 0.9 copy-start.3
  42.5 0.7 copy-start.11
  43.2 46.0 %copy-start.5 = (bf16[1,128,1024]{2,1,0:T(8,128)(2,1)S(1)}, bf16[1,128,1024]{2,1,0:T(8,128)(2,1)}, u32[]{:S(2)}) copy-start(bf16[1,128,1024]{2,1,0:T(8,128)(2,1)} %param.13) | copy-start | bytes 786436
  43.2 46.0 %copy-start.12 = (bf16[4,1024]{1,0:T(4,128)(2,1)S(1)}, bf16[4,1024]{1,0:T(4,128)(2,1)}, u32[]{:S(2)}) copy-start(bf16[4,1024]{1,0:T(4,128)(2,1)} %tc_ref.1) | copy-start | bytes 24580
  47.0 34.7 %all-to-all-start.1 = ((bf16[16,128,128]{2,1,0:T(8,128)(2,1)}), bf16[16,128,128]{2,1,0:T(8,128)(2,1)S(1)}, u32[]{:S(2)}, u32[]{:S(2)}) async-start(bf16[16,128,128]{2,1,0:T(8,128)(2,1)} %get-tuple-element.17), calls=%async_computation.1 | async-start | bytes 1048576 | tf_op jit(solution)/shard_map/all_to_all | solution.py:273
  82.6 34.5 %copy-start.10 = (bf16[1,128,2048]{2,1,0:T(8,128)(2,1)S(1)}, bf16[1,128,2048]{2,1,0:T(8,128)(2,1)}, u32[]{:S(2)}) copy-start(bf16[1,128,2048]{2,1,0:T(8,128)(2,1)} %param.14) | copy-start | bytes 1572868
  82.6 34.5 %copy-start.13 = (f32[2048]{0:T(1024)S(1)}, f32[2048]{0:T(1024)}, u32[]{:S(2)}) copy-start(f32[2048]{0:T(1024)} %param.20) | copy-start | bytes 24580
  82.6 34.5 %all-to-all-start.2 = ((bf16[16,128,128]{2,1,0:T(8,128)(2,1)}), bf16[16,128,128]{2,1,0:T(8,128)(2,1)S(1)}, u32[]{:S(2)}, u32[]{:S(2)}) async-start(bf16[16,128,128]{2,1,0:T(8,128)(2,1)} %scan.1), calls=%async_computation.2 | async-start | bytes 1048576 | tf_op jit(solution)/shard_map/all_to_all | solution.py:311
  117.1 3.4 %copy-start.9 = (bf16[2048,2048]{1,0:T(8,128)(2,1)S(1)}, bf16[2048,2048]{1,0:T(8,128)(2,1)}, u32[]{:S(2)}) copy-start(bf16[2048,2048]{1,0:T(8,128)(2,1)} %all-gather.2.cloned.1.call-done.w_ref) | copy-start | bytes 25165828
Sparse Core Ops, SparseCore 0:
  10.5 70.2 all-gather.1

commit v2 on v1

--- a/solution.py
+++ b/solution.py
@@ -15,8 +15,9 @@
 BF16 = jnp.bfloat16
 HALO = 4
 PAD = 8
-CHUNKS = 4
 MIB = 1 << 20
+WHOLE = 16 * MIB
+OUT_LIMIT = 20 * MIB
 
 
 def silu(u):
@@ -43,9 +44,9 @@
 
 
 def share_kernel(decay_ref, raw_ref, taps_ref, x_ref, b_ref, c_ref, small_ref, ends_ref, dt_ref):
-    tokens, heads = raw_ref.shape
+    heads, tokens = raw_ref.shape
     ranks = small_ref.shape[0]
-    raw = jnp.transpose(raw_ref[...].astype(F32))
+    raw = raw_ref[...].astype(F32)
     dt = jnp.maximum(raw, 0.0) + jnp.log1p(jnp.exp(-jnp.abs(raw)))
     src = lax.broadcasted_iota(jnp.int32, (tokens, tokens), 0)
     dst = lax.broadcasted_iota(jnp.int32, (tokens, tokens), 1)
@@ -131,30 +132,43 @@
         inner_ref[:, cols] = jnp.dot(weights, xin_ref[:, cols], preferred_element_type=F32)
 
 
-def scan_kernel(decay_ref, local_ref, out_ref):
+def scan_kernel(decay_ref, shared_ref, local_ref, out_ref):
     count = local_ref.shape[0]
+    me = lax.axis_index("sp")
+    sums = shared_ref[:, 6, :]
+    lane = lax.broadcasted_iota(jnp.int32, sums.shape, 1)
+    ends = []
+    for head in range(2):
+        mine = jnp.sum(jnp.where(lane == 2 * me + head, sums, 0.0), axis=1, keepdims=True)
+        rate = jnp.exp(jnp.full(sums.shape, decay_ref[head], F32))
+        ends.append(jnp.exp(-rate * mine))
+    decay = jnp.where(lane < HEAD_DIM, ends[0], ends[1])
     for part in range(STATE // 32):
         rows = slice(part * 32, (part + 1) * 32)
         entering = jnp.zeros((32, 2 * HEAD_DIM), F32)
         for step in range(count):
             out_ref[step, rows, :] = entering.astype(BF16)
             if step + 1 < count:
-                entering = entering * decay_ref[step : step + 1, :] + local_ref[
+                entering = entering * decay[step : step + 1, :] + local_ref[
                     step, rows, :
                 ].astype(F32)
 
 
 def out_kernel(
-    ent_ref, cin_ref, inner_ref, cum_ref, z_ref, gain_ref, w_ref, out_ref, normed_ref, held_ref, sems
+    ent_ref, cin_ref, inner_ref, cum_ref, z_ref, gain_ref,
+    m0_ref, m1_ref, m2_ref, m3_ref, o0_ref, o1_ref, o2_ref, o3_ref,
+    out_ref, normed_ref, ordered_ref, held_ref, acc_ref, sems,
 ):
-    chunk = w_ref.shape[1] // CHUNKS
-    copies = []
-    for k in range(CHUNKS):
-        cols = slice(k * chunk, (k + 1) * chunk)
-        copies.append(
-            pltpu.make_async_copy(w_ref.at[:, cols], held_ref.at[:, cols], sems.at[k])
-        )
-        copies[k].start()
+    rank = lax.axis_index("dp")
+    y, x, core = rank // 8, lax.rem(rank // 2, 4), lax.rem(rank, 2)
+    pieces = (m0_ref, m1_ref, m2_ref, m3_ref, o0_ref, o1_ref, o2_ref, o3_ref)
+    deep = m0_ref.shape[0]
+    copies = [
+        pltpu.make_async_copy(ref, held_ref.at[k * deep : (k + 1) * deep, :], sems.at[k])
+        for k, ref in enumerate(pieces)
+    ]
+    for copy in copies:
+        copy.start()
     row_id = lax.broadcasted_iota(jnp.int32, (STATE, STATE), 0) // HEAD_DIM
     col_id = lax.broadcasted_iota(jnp.int32, (STATE, STATE), 1) // HEAD_DIM
     average = jnp.where(row_id == col_id, 1.0 / HEAD_DIM, 0.0).astype(BF16)
@@ -165,30 +179,85 @@
             pair = 2 * group + half
             cols = slice(pair * STATE, (pair + 1) * STATE)
             carried = jnp.dot(cin, ent_ref[pair], preferred_element_type=F32)
-            core = inner_ref[:, cols] + carried * per_head(columns, 2 * half)
-            v = core.astype(BF16).astype(F32) * silu(z_ref[:, cols].astype(F32))
+            core_out = inner_ref[:, cols] + carried * per_head(columns, 2 * half)
+            v = core_out.astype(BF16).astype(F32) * silu(z_ref[:, cols].astype(F32))
             squares = v * v
             high = squares.astype(BF16)
             low = (squares - high.astype(F32)).astype(BF16)
             mean = jnp.dot(high, average, preferred_element_type=F32) + jnp.dot(
                 low, average, preferred_element_type=F32
             )
-            normed = v * lax.rsqrt(mean + NORM_EPS) * gain_ref[:, cols]
-            normed_ref[:, cols] = normed.astype(BF16)
-    for k in range(CHUNKS):
-        cols = slice(k * chunk, (k + 1) * chunk)
-        copies[k].wait()
-        out_ref[:, cols] = jnp.dot(
-            normed_ref[...], held_ref[:, cols], preferred_element_type=F32
-        ).astype(BF16)
+            normed_ref[pair] = v * lax.rsqrt(mean + NORM_EPS) * gain_ref[:, cols]
+    tokens = out_ref.shape[0]
+    lane = lax.broadcasted_iota(jnp.int32, (tokens, STATE), 1)
+
+    def chip(side, position):
+        major, minor = position // 4, position % 4
+        ry = jnp.where(side == 0, major, minor)
+        rx = jnp.where(side == 0, minor, major)
+        return lax.rem(y + 4 - ry, 4) * 4 + lax.rem(x + 4 - rx, 4)
+
+    for half, side in enumerate((core, 1 - core)):
+        for k in range(8):
+            left = normed_ref[chip(side, 2 * k)]
+            right = normed_ref[chip(side, 2 * k + 1)]
+            turned = pltpu.roll(jnp.where(side == 0, right, left), HEAD_DIM, 1)
+            left = jnp.where(side == 0, left, turned)
+            right = jnp.where(side == 0, turned, right)
+            first = (half * 8 + k) * STATE
+            ordered_ref[:, first : first + STATE] = jnp.where(
+                lane < HEAD_DIM, left, right
+            ).astype(BF16)
+    chunk = 512
+    stages = 4
+    depth = held_ref.shape[0] // stages
+    for stage in range(stages):
+        for copy in copies[stage * 8 // stages : (stage + 1) * 8 // stages]:
+            copy.wait()
+        rows = slice(stage * depth, (stage + 1) * depth)
+        for first in range(0, out_ref.shape[1], chunk):
+            cols = slice(first, first + chunk)
+            part = jnp.dot(
+                ordered_ref[:, rows], held_ref[rows, cols], preferred_element_type=F32
+            )
+            if stage:
+                part = part + acc_ref[:, cols]
+            if stage < stages - 1:
+                acc_ref[:, cols] = part
+            else:
+                out_ref[:, cols] = part.astype(BF16)
 
 
 def vmem():
     return pl.BlockSpec(memory_space=pltpu.VMEM)
 
 
+def in_hbm(*values):
+    return [pltpu.with_memory_space_constraint(v, pltpu.HBM) for v in values]
+
+
 def cost(flops, moved, special):
     return pl.CostEstimate(flops=flops, bytes_accessed=moved, transcendentals=special)
+
+
+def first_step(y, x, core, d):
+    return (y, x + d, core) if core == 0 else (y + d, x, core)
+
+
+def second_step(y, x, core, d):
+    return (y + d, x, core) if core == 0 else (y, x + d, core)
+
+
+def swap_step(y, x, core, d):
+    return y, x, 1 - core
+
+
+def torus(step, d):
+    pairs = []
+    for rank in range(32):
+        y, x, core = step(rank // 8, rank // 2 % 4, rank % 2, d)
+        pairs.append((rank, ((y % 4) * 4 + x % 4) * 2 + core))
+    return pairs
 
 
 def body(
@@ -196,23 +265,24 @@
     conv_x, conv_b, conv_c, decay_log, norm_gain, w_out,
 ):
     ranks = lax.axis_size("sp")
-    me = lax.axis_index("sp")
     x, b, c, z, raw = (v[0] for v in (stream_x, stream_b, stream_c, gate_z, step_raw))
     tokens, inner_width = x.shape
     groups = b.shape[1] // STATE
     heads = raw.shape[1]
-    own = heads // ranks
     thin = groups * STATE
     last = tokens // 8 - 1
 
-    w_full = lax.all_gather(w_out, "dp", axis=0, tiled=True)
+    near = [lax.ppermute(w_out, "dp", torus(first_step, d)) for d in (1, 2, 3)]
+    row = jnp.concatenate([w_out] + near)
+    mine = [row] + [lax.ppermute(row, "dp", torus(second_step, d)) for d in (1, 2, 3)]
+    other = [lax.ppermute(v, "dp", torus(swap_step, 0)) for v in mine]
 
     small, ends, dt = pl.pallas_call(
         share_kernel,
         grid=(1,),
         in_specs=[
             pl.BlockSpec(memory_space=pltpu.SMEM),
-            pl.BlockSpec((tokens, heads), lambda i: (0, 0)),
+            pl.BlockSpec((heads, tokens), lambda i: (0, 0)),
             pl.BlockSpec((4, 128), lambda i: (0, 0)),
             pl.BlockSpec((8, inner_width), lambda i: (last, 0)),
             pl.BlockSpec((8, thin), lambda i: (last, 0)),
@@ -228,10 +298,10 @@
             jax.ShapeDtypeStruct((HALO, inner_width + 2 * thin), BF16),
             jax.ShapeDtypeStruct((groups, 2 * RATIO, tokens), F32),
         ],
-        compiler_params=pltpu.CompilerParams(vmem_limit_bytes=8 * MIB),
+        compiler_params=pltpu.CompilerParams(vmem_limit_bytes=WHOLE),
         cost_estimate=cost(10_000_000, 200_000, 10_000),
         name="share",
-    )(decay_log, raw, conv_x, x, b, c)
+    )(decay_log, jnp.transpose(raw), conv_x, *in_hbm(x, b, c))
     shared = lax.all_to_all(small, "sp", 0, 0, tiled=True)
     halo = lax.ppermute(ends, "sp", [(i, i + 1) for i in range(ranks - 1)])
 
@@ -265,10 +335,10 @@
             pltpu.VMEM((per, PAD + tokens, WIDTH), F32),
             pltpu.VMEM((per, PAD + tokens, STATE), F32),
         ],
-        compiler_params=pltpu.CompilerParams(vmem_limit_bytes=16 * MIB),
+        compiler_params=pltpu.CompilerParams(vmem_limit_bytes=WHOLE),
         cost_estimate=cost(4_000_000_000, 2_000_000, 400_000),
         name="state",
-    )(x, b, halo, halo, shared, conv_b, dt)
+    )(*in_hbm(x, b), halo, halo, shared, conv_b, dt)
 
     local = lax.all_to_all(state, "sp", 0, 0, tiled=True)
 
@@ -297,33 +367,33 @@
         name="inner",
     )(c, halo, conv_c, bin_, xin, cum)
 
-    own_sums = lax.dynamic_slice_in_dim(shared[:, 6, :], me * own, own, 1)
-    decay = jnp.repeat(jnp.exp(own_sums * -jnp.exp(decay_log)[None, :]), HEAD_DIM, axis=1)
     entering = pl.pallas_call(
         scan_kernel,
-        in_specs=[vmem(), vmem()],
+        in_specs=[pl.BlockSpec(memory_space=pltpu.SMEM), vmem(), vmem()],
         out_specs=vmem(),
         out_shape=jax.ShapeDtypeStruct(local.shape, BF16),
         compiler_params=pltpu.CompilerParams(vmem_limit_bytes=8 * MIB),
         cost_estimate=cost(1_000_000_000, 1_000_000, 0),
         name="scan",
-    )(decay, local)
+    )(decay_log, shared, local)
     entering = lax.all_to_all(entering, "sp", 0, 0, tiled=True)
 
     mixed = pl.pallas_call(
         out_kernel,
-        in_specs=[vmem()] * 6 + [pl.BlockSpec(memory_space=pltpu.HBM)],
+        in_specs=[vmem()] * 6 + [pl.BlockSpec(memory_space=pltpu.HBM)] * 8,
         out_specs=vmem(),
-        out_shape=jax.ShapeDtypeStruct((tokens, w_full.shape[1]), BF16),
+        out_shape=jax.ShapeDtypeStruct((tokens, w_out.shape[1]), BF16),
         scratch_shapes=[
+            pltpu.VMEM((inner_width // STATE, tokens, STATE), F32),
             pltpu.VMEM((tokens, inner_width), BF16),
-            pltpu.VMEM(w_full.shape, BF16),
-            pltpu.SemaphoreType.DMA((CHUNKS,)),
-        ],
-        compiler_params=pltpu.CompilerParams(vmem_limit_bytes=24 * MIB),
+            pltpu.VMEM((inner_width, w_out.shape[1]), BF16),
+            pltpu.VMEM((tokens, w_out.shape[1]), F32),
+            pltpu.SemaphoreType.DMA((8,)),
+        ],
+        compiler_params=pltpu.CompilerParams(vmem_limit_bytes=OUT_LIMIT),
         cost_estimate=cost(4_000_000_000, 10_000_000, 300_000),
         name="project",
-    )(entering, cin, inner, cum, z, norm_gain[None], w_full)
+    )(entering, cin, inner, cum, z, norm_gain[None], *in_hbm(*mine, *other))
     return mixed[None]
 
 

time: 134 us -> 117 us (0.87)
  the two profiles are of different devices: /device:TPU:54 before, /device:TPU:2 now
where the time goes in v2:
time: 117 us; the launch traced here: 116 us
  starting transfers between devices  67.1 us (57%)
  waiting for transfers between devices  22.9 us (20%)
  Pallas kernels  18.9 us (16%)
  local copies, waits for them, and re-layouts  6.61 us (6%)
    all_to_all x1, starting transfers between devices, body(): shared = lax.all_to_all(small, 'sp', 0, 0, tiled=True)  15.3 us
    all_to_all x1, starting transfers between devices, body(): entering = lax.all_to_all(entering, 'sp', 0, 0, tiled=True)  12.2 us
    ppermute x3, starting transfers between devices, body(): lax.ppermute(row, 'dp', torus(second_step, d))  10.9 us
    ppermute x3, starting transfers between devices, body(): near = [lax.ppermute(w_out, 'dp', torus(first_step, d)) for d in (1, 2, 3)]  10.5 us
    ppermute x4, starting transfers between devices, body(): other = [lax.ppermute(v, 'dp', torus(swap_step, 0)) for v in mine]  8.14 us
    all_to_all x1, waiting for transfers between devices, body(): shared = lax.all_to_all(small, 'sp', 0, 0, tiled=True)  7.46 us
    pallas_call x1, Pallas kernels, body(): pl.pallas_call(out_kernel, in_specs=[vmem()] * 6 + [pl.BlockSpec(memory_s...  6.82 us
    all_to_all x1, starting transfers between devices, body(): local = lax.all_to_all(state, 'sp', 0, 0, tiled=True)  6.21 us
  transfers between devices with their start and end apart: 14, of which 7 were waited for; matrix products, arithmetic and copies ran while one was open for 3% of the time, Pallas kernels for 5%

profile of v2, /device:TPU:2, one launch (start us, length us, event | category | flops | bytes accessed | tf_op | source)
XLA Modules:
  0.0 115.8 jit_solution(11887120227575216184)
XLA Ops:
  0.0 0.0 copy-start.2
  0.0 0.0 copy-start.3
  0.0 0.7 copy-done.2
  0.7 0.0 copy-done.3
  0.7 0.0 copy-start.1
  0.7 0.7 copy-done.1
  1.4 1.6 %share.1 = (f32[16,8,128]{2,1,0:T(8,128)}, bf16[4,4096]{1,0:T(4,128)(2,1)S(1)}, f32[8,8,128]{2,1,0:T(8,128)S(1)}) custom-call(f32[2]{0:T(128)S(1)} %copy-done.3, bf16[32,128]{1,0:T(8,128)(2,1)S(1)} %bitcast.11, bf16[4,128]{1,0:T(4,128)(2,1)S(1)} %copy-done.2, bf16[128,2048]{1,0:T(8,128)(2,1)} %bitcast.14, bf16[128,1024]{1,0:T(8,128)(2,1)} %bitcast.16, ...), custom_call_target="tpu_custom_call" | custom-call | flops 10000000 | bytes 200000 | tf_op jit(solution)/shard_map/share/pallas_call | solution.py:280
  3.0 0.0 copy-start.5
  3.0 15.3 %all-to-all-start = ((f32[16,8,128]{2,1,0:T(8,128)}), f32[16,8,128]{2,1,0:T(8,128)S(1)}, u32[]{:S(2)}, u32[]{:S(2)}) async-start(f32[16,8,128]{2,1,0:T(8,128)} %get-tuple-element.14), calls=%async_computation | async-start | bytes 131072 | tf_op jit(solution)/shard_map/all_to_all | solution.py:305
  18.3 3.8 %collective-permute-start = (bf16[4,4096]{1,0:T(4,128)(2,1)S(1)}, bf16[4,4096]{1,0:T(4,128)(2,1)S(1)}, u32[]{:S(2)}, u32[]{:S(2)}) collective-permute-start(bf16[4,4096]{1,0:T(4,128)(2,1)S(1)} %get-tuple-element.15), channel_id=1, source_target_pairs={{0,32},{32,64},{64,96},{96,128},{128,160},{160,192},{192,224},{224... | collective-permute-start | bytes 98312 | tf_op jit(solution)/shard_map/ppermute | solution.py:306
  22.2 1.7 %collective-permute-done.hx_ref.hb_ref.hc_ref = bf16[4,4096]{1,0:T(4,128)(2,1)S(1)} collective-permute-done((bf16[4,4096]{1,0:T(4,128)(2,1)S(1)}, bf16[4,4096]{1,0:T(4,128)(2,1)S(1)}, u32[]{:S(2)}, u32[]{:S(2)}) %collective-permute-start) | collective-permute-done | bytes 32800 | tf_op jit(solution)/shard_map/ppermute | solution.py:306
  23.8 7.5 %all-to-all-done.shared_ref = f32[16,8,128]{2,1,0:T(8,128)S(1)} async-done(((f32[16,8,128]{2,1,0:T(8,128)}), f32[16,8,128]{2,1,0:T(8,128)S(1)}, u32[]{:S(2)}, u32[]{:S(2)}) %all-to-all-start) | async-done | bytes 65568 | tf_op jit(solution)/shard_map/all_to_all | solution.py:305
  31.3 0.0 copy-done.5
  31.3 4.8 %state.1 = (bf16[16,128,128]{2,1,0:T(8,128)(2,1)}, bf16[128,2048]{1,0:T(8,128)(2,1)S(1)}, bf16[128,1024]{1,0:T(8,128)(2,1)S(1)}, f32[8,8,128]{2,1,0:T(8,128)S(1)}) custom-call(bf16[128,2048]{1,0:T(8,128)(2,1)} %bitcast.15, bf16[128,1024]{1,0:T(8,128)(2,1)} %bitcast.17, bf16[4,4096]{1,0:T(4,128)(2,1)S(1)} %collective-permute-done.hx_ref.hb_ref.hc_ref, ...), custom_call_target="tpu_custom_call" | custom-call | flops 4000000000 | bytes 2000000 | tf_op jit(solution)/shard_map/state/pallas_call | solution.py:310
  36.1 0.0 copy-start.8
  36.1 6.2 %all-to-all-start.1 = ((bf16[16,128,128]{2,1,0:T(8,128)(2,1)}), bf16[16,128,128]{2,1,0:T(8,128)(2,1)S(1)}, u32[]{:S(2)}, u32[]{:S(2)}) async-start(bf16[16,128,128]{2,1,0:T(8,128)(2,1)} %get-tuple-element.17), calls=%async_computation.1 | async-start | bytes 1048576 | tf_op jit(solution)/shard_map/all_to_all | solution.py:343
  42.3 0.0 copy-done.8
  42.3 3.4 %collective-permute-start.1 = (bf16[64,2048]{1,0:T(8,128)(2,1)S(1)}, bf16[64,2048]{1,0:T(8,128)(2,1)S(1)}, u32[]{:S(2)}, u32[]{:S(2)}) collective-permute-start(bf16[64,2048]{1,0:T(8,128)(2,1)S(1)} %copy-done.8), channel_id=1, source_target_pairs={{0,2},{1,9},{2,4},{3,11},{4,6},{5,13},{6,0},{7,15},{8,10},{9,17},{... | collective-permute-start | bytes 786440 | tf_op jit(solution)/shard_map/ppermute | solution.py:275
  45.7 3.0 %collective-permute-start.2 = (bf16[64,2048]{1,0:T(8,128)(2,1)S(1)}, bf16[64,2048]{1,0:T(8,128)(2,1)S(1)}, u32[]{:S(2)}, u32[]{:S(2)}) collective-permute-start(bf16[64,2048]{1,0:T(8,128)(2,1)S(1)} %copy-done.8), channel_id=1, source_target_pairs={{0,4},{1,17},{2,6},{3,19},{4,0},{5,21},{6,2},{7,23},{8,12},{9,25},... | collective-permute-start | bytes 786440 | tf_op jit(solution)/shard_map/ppermute | solution.py:275
  48.8 4.1 %collective-permute-start.3 = (bf16[64,2048]{1,0:T(8,128)(2,1)S(1)}, bf16[64,2048]{1,0:T(8,128)(2,1)S(1)}, u32[]{:S(2)}, u32[]{:S(2)}) collective-permute-start(bf16[64,2048]{1,0:T(8,128)(2,1)S(1)} %copy-done.8), channel_id=1, source_target_pairs={{0,6},{1,25},{2,0},{3,27},{4,2},{5,29},{6,4},{7,31},{8,14},{9,1},{... | collective-permute-start | bytes 786440 | tf_op jit(solution)/shard_map/ppermute | solution.py:275
  52.8 0.7 constant_dynamic-update-slice_fusion.3
  53.5 0.0 collective-permute-done.1
  53.5 0.7 constant_dynamic-update-slice_fusion.2
  54.3 1.3 %collective-permute-done.2 = bf16[64,2048]{1,0:T(8,128)(2,1)S(1)} collective-permute-done((bf16[64,2048]{1,0:T(8,128)(2,1)S(1)}, bf16[64,2048]{1,0:T(8,128)(2,1)S(1)}, u32[]{:S(2)}, u32[]{:S(2)}) %collective-permute-start.2) | collective-permute-done | bytes 262176 | tf_op jit(solution)/shard_map/ppermute | solution.py:275
  55.6 0.7 constant_dynamic-update-slice_fusion.1
  56.3 2.0 %collective-permute-done.3 = bf16[64,2048]{1,0:T(8,128)(2,1)S(1)} collective-permute-done((bf16[64,2048]{1,0:T(8,128)(2,1)S(1)}, bf16[64,2048]{1,0:T(8,128)(2,1)S(1)}, u32[]{:S(2)}, u32[]{:S(2)}) %collective-permute-start.3) | collective-permute-done | bytes 262176 | tf_op jit(solution)/shard_map/ppermute | solution.py:275
  58.3 0.7 constant_dynamic-update-slice_fusion.m0_ref
  59.0 4.9 %collective-permute-start.6 = (bf16[256,2048]{1,0:T(8,128)(2,1)}, bf16[256,2048]{1,0:T(8,128)(2,1)}, u32[]{:S(2)}, u32[]{:S(2)}) collective-permute-start(bf16[256,2048]{1,0:T(8,128)(2,1)} %constant_dynamic-update-slice_fusion.m0_ref), channel_id=1, source_target_pairs={{0,24},{1,7},{2,26},{3,1},{4,28},{5,3},{6,30},{7,5},{8,0},{9,15},{... | collective-permute-start | bytes 3145736 | tf_op jit(solution)/shard_map/ppermute | solution.py:277
  63.9 1.9 %collective-permute-start.4 = (bf16[256,2048]{1,0:T(8,128)(2,1)}, bf16[256,2048]{1,0:T(8,128)(2,1)}, u32[]{:S(2)}, u32[]{:S(2)}) collective-permute-start(bf16[256,2048]{1,0:T(8,128)(2,1)} %constant_dynamic-update-slice_fusion.m0_ref), channel_id=1, source_target_pairs={{0,8},{1,3},{2,10},{3,5},{4,12},{5,7},{6,14},{7,1},{8,16},{9,11},{... | collective-permute-start | bytes 3145736 | tf_op jit(solution)/shard_map/ppermute | solution.py:277
  65.9 4.1 %collective-permute-start.5 = (bf16[256,2048]{1,0:T(8,128)(2,1)}, bf16[256,2048]{1,0:T(8,128)(2,1)}, u32[]{:S(2)}, u32[]{:S(2)}) collective-permute-start(bf16[256,2048]{1,0:T(8,128)(2,1)} %constant_dynamic-update-slice_fusion.m0_ref), channel_id=1, source_target_pairs={{0,16},{1,5},{2,18},{3,7},{4,20},{5,1},{6,22},{7,3},{8,24},{9,13},... | collective-permute-start | bytes 3145736 | tf_op jit(solution)/shard_map/ppermute | solution.py:277
  70.0 0.0 all-to-all-done.1.local_ref
  70.0 1.5 %scan.1 = bf16[16,128,128]{2,1,0:T(8,128)(2,1)} custom-call(f32[2]{0:T(128)S(1)} %copy-done.3, f32[16,8,128]{2,1,0:T(8,128)S(1)} %all-to-all-done.shared_ref, bf16[16,128,128]{2,1,0:T(8,128)(2,1)S(1)} %all-to-all-done.1.local_ref), custom_call_target="tpu_custom_call" | custom-call | flops 1000000000 | bytes 1000000 | tf_op jit(solution)/shard_map/scan/pallas_call | solution.py:370
  71.5 0.0 copy-start
  71.5 0.0 copy-start.6
  71.6 12.2 %all-to-all-start.2 = ((bf16[16,128,128]{2,1,0:T(8,128)(2,1)}), bf16[16,128,128]{2,1,0:T(8,128)(2,1)S(1)}, u32[]{:S(2)}, u32[]{:S(2)}) async-start(bf16[16,128,128]{2,1,0:T(8,128)(2,1)} %scan.1), calls=%async_computation.2 | async-start | bytes 1048576 | tf_op jit(solution)/shard_map/all_to_all | solution.py:379
  83.7 1.9 %collective-permute-start.7 = (bf16[256,2048]{1,0:T(8,128)(2,1)}, bf16[256,2048]{1,0:T(8,128)(2,1)S(1)}, u32[]{:S(2)}, u32[]{:S(2)}) collective-permute-start(bf16[256,2048]{1,0:T(8,128)(2,1)} %constant_dynamic-update-slice_fusion.m0_ref), channel_id=1, source_target_pairs={{0,1},{1,0},{2,3},{3,2},{4,5},{5,4},{6,7},{7,6},{8,9},{9,8},{10,11... | collective-permute-start | bytes 3145736 | tf_op jit(solution)/shard_map/ppermute | solution.py:278
  85.6 2.2 %collective-permute-done.6.m3_ref = bf16[256,2048]{1,0:T(8,128)(2,1)} collective-permute-done((bf16[256,2048]{1,0:T(8,128)(2,1)}, bf16[256,2048]{1,0:T(8,128)(2,1)}, u32[]{:S(2)}, u32[]{:S(2)}) %collective-permute-start.6) | collective-permute-done | bytes 1048608 | tf_op jit(solution)/shard_map/ppermute | solution.py:277
  87.8 1.9 %collective-permute-start.10 = (bf16[256,2048]{1,0:T(8,128)(2,1)}, bf16[256,2048]{1,0:T(8,128)(2,1)S(1)}, u32[]{:S(2)}, u32[]{:S(2)}) collective-permute-start(bf16[256,2048]{1,0:T(8,128)(2,1)} %collective-permute-done.6.m3_ref), channel_id=1, source_target_pairs={{0,1},{1,0},{2,3},{3,2},{4,5},{5,4},{6,7},{7,6},{8,9},{9,8},{10,11... | collective-permute-start | bytes 3145736 | tf_op jit(solution)/shard_map/ppermute | solution.py:278
  89.7 3.7 %collective-permute-done.4.m1_ref = bf16[256,2048]{1,0:T(8,128)(2,1)} collective-permute-done((bf16[256,2048]{1,0:T(8,128)(2,1)}, bf16[256,2048]{1,0:T(8,128)(2,1)}, u32[]{:S(2)}, u32[]{:S(2)}) %collective-permute-start.4) | collective-permute-done | bytes 1048608 | tf_op jit(solution)/shard_map/ppermute | solution.py:277
  93.4 1.9 %collective-permute-start.8 = (bf16[256,2048]{1,0:T(8,128)(2,1)}, bf16[256,2048]{1,0:T(8,128)(2,1)S(1)}, u32[]{:S(2)}, u32[]{:S(2)}) collective-permute-start(bf16[256,2048]{1,0:T(8,128)(2,1)} %collective-permute-done.4.m1_ref), channel_id=1, source_target_pairs={{0,1},{1,0},{2,3},{3,2},{4,5},{5,4},{6,7},{7,6},{8,9},{9,8},{10,11... | collective-permute-start | bytes 3145736 | tf_op jit(solution)/shard_map/ppermute | solution.py:278
  95.3 0.0 collective-permute-done.5.m2_ref
  95.3 2.4 %collective-permute-start.9 = (bf16[256,2048]{1,0:T(8,128)(2,1)}, bf16[256,2048]{1,0:T(8,128)(2,1)}, u32[]{:S(2)}, u32[]{:S(2)}) collective-permute-start(bf16[256,2048]{1,0:T(8,128)(2,1)} %collective-permute-done.5.m2_ref), channel_id=1, source_target_pairs={{0,1},{1,0},{2,3},{3,2},{4,5},{5,4},{6,7},{7,6},{8,9},{9,8},{10,11... | collective-permute-start | bytes 3145736 | tf_op jit(solution)/shard_map/ppermute | solution.py:278
  97.7 0.0 copy-done
  97.8 0.0 copy-done.6
  97.8 0.0 copy-start.4
  97.8 0.0 copy-start.7
  97.8 4.1 %inner.1 = (bf16[128,1024]{1,0:T(8,128)(2,1)S(1)}, f32[128,2048]{1,0:T(8,128)S(1)}) custom-call(bf16[128,1024]{1,0:T(8,128)(2,1)S(1)} %bitcast.10, bf16[4,4096]{1,0:T(4,128)(2,1)S(1)} %collective-permute-done.hx_ref.hb_ref.hc_ref, bf16[4,1024]{1,0:T(4,128)(2,1)S(1)} %copy-done.6, bf16[128,1024]{1,0:T(8,128)(2,1)S(1)} %get-tuple-element.18.bin_ref, ...), custom_call_target="tpu_custom_call" | custom-call | flops 4000000000 | bytes 2000000 | tf_op jit(solution)/shard_map/inner/pallas_call | solution.py:345
  101.9 0.0 collective-permute-done.7.o0_ref
  101.9 0.0 copy-start.9
  102.0 0.0 collective-permute-done.10.o3_ref
  102.0 0.0 copy-start.10
  102.0 0.0 collective-permute-done.8.o1_ref
  102.0 0.9 copy-done.9
  102.9 0.4 copy-done.10
  103.3 0.0 copy-start.11
  103.3 1.0 copy-done.11
  104.3 0.0 collective-permute-done.9.o2_ref
  104.3 4.6 %all-to-all-done.2.ent_ref = bf16[16,128,128]{2,1,0:T(8,128)(2,1)S(1)} async-done(((bf16[16,128,128]{2,1,0:T(8,128)(2,1)}), bf16[16,128,128]{2,1,0:T(8,128)(2,1)S(1)}, u32[]{:S(2)}, u32[]{:S(2)}) %all-to-all-start.2) | async-done | bytes 524320 | tf_op jit(solution)/shard_map/all_to_all | solution.py:379
  108.9 0.0 copy-done.4
  108.9 0.0 copy-done.7
  108.9 6.8 %project.1 = bf16[128,2048]{1,0:T(8,128)(2,1)} custom-call(bf16[16,128,128]{2,1,0:T(8,128)(2,1)S(1)} %all-to-all-done.2.ent_ref, bf16[128,1024]{1,0:T(8,128)(2,1)S(1)} %get-tuple-element.21.cin_ref, f32[128,2048]{1,0:T(8,128)S(1)} %get-tuple-element.22.inner_ref, f32[8,8,128]{2,1,0:T(8,128)S(1)} %get-tuple-element.20.cum_ref, ...), custom_call_target="tpu_custom_call" | custom-call | flops 4000000000 | bytes 10000000 | tf_op jit(solution)/shard_map/project/pallas_call | solution.py:381
Async XLA Ops:
  0.0 0.7 copy-start.2
  0.0 0.7 copy-start.3
  0.7 0.7 copy-start.1
  3.0 28.3 %copy-start.5 = (bf16[4,1024]{1,0:T(4,128)(2,1)S(1)}, bf16[4,1024]{1,0:T(4,128)(2,1)}, u32[]{:S(2)}) copy-start(bf16[4,1024]{1,0:T(4,128)(2,1)} %tb_ref.1) | copy-start | bytes 24580
  3.0 28.3 %all-to-all-start = ((f32[16,8,128]{2,1,0:T(8,128)}), f32[16,8,128]{2,1,0:T(8,128)S(1)}, u32[]{:S(2)}, u32[]{:S(2)}) async-start(f32[16,8,128]{2,1,0:T(8,128)} %get-tuple-element.14), calls=%async_computation | async-start | bytes 131072 | tf_op jit(solution)/shard_map/all_to_all | solution.py:305
  18.3 5.5 %collective-permute-start = (bf16[4,4096]{1,0:T(4,128)(2,1)S(1)}, bf16[4,4096]{1,0:T(4,128)(2,1)S(1)}, u32[]{:S(2)}, u32[]{:S(2)}) collective-permute-start(bf16[4,4096]{1,0:T(4,128)(2,1)S(1)} %get-tuple-element.15), channel_id=1, source_target_pairs={{0,32},{32,64},{64,96},{96,128},{128,160},{160,192},{192,224},{224... | collective-permute-start | bytes 98312 | tf_op jit(solution)/shard_map/ppermute | solution.py:306
  36.1 6.2 %copy-start.8 = (bf16[64,2048]{1,0:T(8,128)(2,1)S(1)}, bf16[64,2048]{1,0:T(8,128)(2,1)}, u32[]{:S(2)}) copy-start(bf16[64,2048]{1,0:T(8,128)(2,1)} %param.21) | copy-start | bytes 786436
  36.1 33.9 %all-to-all-start.1 = ((bf16[16,128,128]{2,1,0:T(8,128)(2,1)}), bf16[16,128,128]{2,1,0:T(8,128)(2,1)S(1)}, u32[]{:S(2)}, u32[]{:S(2)}) async-start(bf16[16,128,128]{2,1,0:T(8,128)(2,1)} %get-tuple-element.17), calls=%async_computation.1 | async-start | bytes 1048576 | tf_op jit(solution)/shard_map/all_to_all | solution.py:343
  42.3 11.2 %collective-permute-start.1 = (bf16[64,2048]{1,0:T(8,128)(2,1)S(1)}, bf16[64,2048]{1,0:T(8,128)(2,1)S(1)}, u32[]{:S(2)}, u32[]{:S(2)}) collective-permute-start(bf16[64,2048]{1,0:T(8,128)(2,1)S(1)} %copy-done.8), channel_id=1, source_target_pairs={{0,2},{1,9},{2,4},{3,11},{4,6},{5,13},{6,0},{7,15},{8,10},{9,17},{... | collective-permute-start | bytes 786440 | tf_op jit(solution)/shard_map/ppermute | solution.py:275
  45.7 9.9 %collective-permute-start.2 = (bf16[64,2048]{1,0:T(8,128)(2,1)S(1)}, bf16[64,2048]{1,0:T(8,128)(2,1)S(1)}, u32[]{:S(2)}, u32[]{:S(2)}) collective-permute-start(bf16[64,2048]{1,0:T(8,128)(2,1)S(1)} %copy-done.8), channel_id=1, source_target_pairs={{0,4},{1,17},{2,6},{3,19},{4,0},{5,21},{6,2},{7,23},{8,12},{9,25},... | collective-permute-start | bytes 786440 | tf_op jit(solution)/shard_map/ppermute | solution.py:275
  48.8 9.6 %collective-permute-start.3 = (bf16[64,2048]{1,0:T(8,128)(2,1)S(1)}, bf16[64,2048]{1,0:T(8,128)(2,1)S(1)}, u32[]{:S(2)}, u32[]{:S(2)}) collective-permute-start(bf16[64,2048]{1,0:T(8,128)(2,1)S(1)} %copy-done.8), channel_id=1, source_target_pairs={{0,6},{1,25},{2,0},{3,27},{4,2},{5,29},{6,4},{7,31},{8,14},{9,1},{... | collective-permute-start | bytes 786440 | tf_op jit(solution)/shard_map/ppermute | solution.py:275
  59.0 28.8 %collective-permute-start.6 = (bf16[256,2048]{1,0:T(8,128)(2,1)}, bf16[256,2048]{1,0:T(8,128)(2,1)}, u32[]{:S(2)}, u32[]{:S(2)}) collective-permute-start(bf16[256,2048]{1,0:T(8,128)(2,1)} %constant_dynamic-update-slice_fusion.m0_ref), channel_id=1, source_target_pairs={{0,24},{1,7},{2,26},{3,1},{4,28},{5,3},{6,30},{7,5},{8,0},{9,15},{... | collective-permute-start | bytes 3145736 | tf_op jit(solution)/shard_map/ppermute | solution.py:277
  63.9 29.5 %collective-permute-start.4 = (bf16[256,2048]{1,0:T(8,128)(2,1)}, bf16[256,2048]{1,0:T(8,128)(2,1)}, u32[]{:S(2)}, u32[]{:S(2)}) collective-permute-start(bf16[256,2048]{1,0:T(8,128)(2,1)} %constant_dynamic-update-slice_fusion.m0_ref), channel_id=1, source_target_pairs={{0,8},{1,3},{2,10},{3,5},{4,12},{5,7},{6,14},{7,1},{8,16},{9,11},{... | collective-permute-start | bytes 3145736 | tf_op jit(solution)/shard_map/ppermute | solution.py:277
  65.9 29.4 %collective-permute-start.5 = (bf16[256,2048]{1,0:T(8,128)(2,1)}, bf16[256,2048]{1,0:T(8,128)(2,1)}, u32[]{:S(2)}, u32[]{:S(2)}) collective-permute-start(bf16[256,2048]{1,0:T(8,128)(2,1)} %constant_dynamic-update-slice_fusion.m0_ref), channel_id=1, source_target_pairs={{0,16},{1,5},{2,18},{3,7},{4,20},{5,1},{6,22},{7,3},{8,24},{9,13},... | collective-permute-start | bytes 3145736 | tf_op jit(solution)/shard_map/ppermute | solution.py:277
  71.5 26.2 %copy-start = (bf16[1,128,1024]{2,1,0:T(8,128)(2,1)S(1)}, bf16[1,128,1024]{2,1,0:T(8,128)(2,1)}, u32[]{:S(2)}) copy-start(bf16[1,128,1024]{2,1,0:T(8,128)(2,1)} %param.13) | copy-start | bytes 786436
  71.5 26.2 %copy-start.6 = (bf16[4,1024]{1,0:T(4,128)(2,1)S(1)}, bf16[4,1024]{1,0:T(4,128)(2,1)}, u32[]{:S(2)}) copy-start(bf16[4,1024]{1,0:T(4,128)(2,1)} %tc_ref.1) | copy-start | bytes 24580
  71.6 37.4 %all-to-all-start.2 = ((bf16[16,128,128]{2,1,0:T(8,128)(2,1)}), bf16[16,128,128]{2,1,0:T(8,128)(2,1)S(1)}, u32[]{:S(2)}, u32[]{:S(2)}) async-start(bf16[16,128,128]{2,1,0:T(8,128)(2,1)} %scan.1), calls=%async_computation.2 | async-start | bytes 1048576 | tf_op jit(solution)/shard_map/all_to_all | solution.py:379
  83.7 18.2 %collective-permute-start.7 = (bf16[256,2048]{1,0:T(8,128)(2,1)}, bf16[256,2048]{1,0:T(8,128)(2,1)S(1)}, u32[]{:S(2)}, u32[]{:S(2)}) collective-permute-start(bf16[256,2048]{1,0:T(8,128)(2,1)} %constant_dynamic-update-slice_fusion.m0_ref), channel_id=1, source_target_pairs={{0,1},{1,0},{2,3},{3,2},{4,5},{5,4},{6,7},{7,6},{8,9},{9,8},{10,11... | collective-permute-start | bytes 3145736 | tf_op jit(solution)/shard_map/ppermute | solution.py:278
  87.8 14.2 %collective-permute-start.10 = (bf16[256,2048]{1,0:T(8,128)(2,1)}, bf16[256,2048]{1,0:T(8,128)(2,1)S(1)}, u32[]{:S(2)}, u32[]{:S(2)}) collective-permute-start(bf16[256,2048]{1,0:T(8,128)(2,1)} %collective-permute-done.6.m3_ref), channel_id=1, source_target_pairs={{0,1},{1,0},{2,3},{3,2},{4,5},{5,4},{6,7},{7,6},{8,9},{9,8},{10,11... | collective-permute-start | bytes 3145736 | tf_op jit(solution)/shard_map/ppermute | solution.py:278
  93.4 8.6 %collective-permute-start.8 = (bf16[256,2048]{1,0:T(8,128)(2,1)}, bf16[256,2048]{1,0:T(8,128)(2,1)S(1)}, u32[]{:S(2)}, u32[]{:S(2)}) collective-permute-start(bf16[256,2048]{1,0:T(8,128)(2,1)} %collective-permute-done.4.m1_ref), channel_id=1, source_target_pairs={{0,1},{1,0},{2,3},{3,2},{4,5},{5,4},{6,7},{7,6},{8,9},{9,8},{10,11... | collective-permute-start | bytes 3145736 | tf_op jit(solution)/shard_map/ppermute | solution.py:278
  95.3 9.0 %collective-permute-start.9 = (bf16[256,2048]{1,0:T(8,128)(2,1)}, bf16[256,2048]{1,0:T(8,128)(2,1)}, u32[]{:S(2)}, u32[]{:S(2)}) collective-permute-start(bf16[256,2048]{1,0:T(8,128)(2,1)} %collective-permute-done.5.m2_ref), channel_id=1, source_target_pairs={{0,1},{1,0},{2,3},{3,2},{4,5},{5,4},{6,7},{7,6},{8,9},{9,8},{10,11... | collective-permute-start | bytes 3145736 | tf_op jit(solution)/shard_map/ppermute | solution.py:278
  97.8 11.2 %copy-start.4 = (bf16[1,128,2048]{2,1,0:T(8,128)(2,1)S(1)}, bf16[1,128,2048]{2,1,0:T(8,128)(2,1)}, u32[]{:S(2)}) copy-start(bf16[1,128,2048]{2,1,0:T(8,128)(2,1)} %param.14) | copy-start | bytes 1572868
  97.8 11.2 %copy-start.7 = (f32[2048]{0:T(1024)S(1)}, f32[2048]{0:T(1024)}, u32[]{:S(2)}) copy-start(f32[2048]{0:T(1024)} %param.20) | copy-start | bytes 24580
  101.9 1.0 copy-start.9
  102.0 1.3 %copy-start.10 = (bf16[256,2048]{1,0:T(8,128)(2,1)}, bf16[256,2048]{1,0:T(8,128)(2,1)S(1)}, u32[]{:S(2)}) copy-start(bf16[256,2048]{1,0:T(8,128)(2,1)S(1)} %collective-permute-done.10.o3_ref) | copy-start | bytes 3145732
  103.3 1.0 copy-start.11

commit v3 on v2

v3 whole, which is shorter than its diff:
```python
import jax
import jax.numpy as jnp
from jax import lax
from jax.experimental import pallas as pl
from jax.experimental.pallas import tpu as pltpu
from jax.sharding import PartitionSpec as P


HEAD_DIM = 64
STATE = 128
RATIO = 4
WIDTH = RATIO * HEAD_DIM
NORM_EPS = 1.0
HIGHEST = lax.Precision.HIGHEST
F32 = jnp.float32
BF16 = jnp.bfloat16
HALO = 4
EXTRA = 8
REACH = 3
COMMON = 16
PAD = 8
MIB = 1 << 20
OUT_LIMIT = 20 * MIB


def silu(u):
    half = 0.5 * u
    return half + half * jnp.tanh(half)


def lanes(first, size):
    return pl.ds(pl.multiple_of(first, STATE), size)


def conv_silu(pad_ref, halo, own, given, side, taps):
    tokens = own.shape[0]
    rows = 2 * tokens
    pad_ref[PAD - HALO : PAD, :] = halo.astype(F32)
    pad_ref[pl.ds(pl.multiple_of(PAD + side * tokens, 8), tokens), :] = own.astype(F32)
    pad_ref[pl.ds(pl.multiple_of(PAD + (1 - side) * tokens, 8), tokens), :] = given.astype(F32)
    total = taps[3:4, :] * pad_ref[PAD : PAD + rows, :]
    for back in range(1, 4):
        total = total + taps[3 - back : 4 - back, :] * pad_ref[PAD - back : PAD - back + rows, :]
    return silu(total)


def per_head(columns, first):
    tokens = columns.shape[0]
    lane = lax.broadcasted_iota(jnp.int32, (tokens, 128), 1)
    left = jnp.broadcast_to(columns[:, first : first + 1], (tokens, 128))
    right = jnp.broadcast_to(columns[:, first + 1 : first + 2], (tokens, 128))
    return jnp.where(lane < HEAD_DIM, left, right)


def head_row(values):
    lane = lax.broadcasted_iota(jnp.int32, (1, WIDTH), 1)
    row = jnp.broadcast_to(values[0:1], (1, WIDTH))
    for head in range(1, RATIO):
        row = jnp.where(
            lane >= head * HEAD_DIM, jnp.broadcast_to(values[head : head + 1], (1, WIDTH)), row
        )
    return row


def steps_of(raw):
    tokens = raw.shape[1]
    raw = raw.astype(F32)
    dt = jnp.maximum(raw, 0.0) + jnp.log1p(jnp.exp(-jnp.abs(raw)))
    src = lax.broadcasted_iota(jnp.int32, (tokens, tokens), 0)
    dst = lax.broadcasted_iota(jnp.int32, (tokens, tokens), 1)
    upper = (src <= dst).astype(F32)
    return dt, jnp.dot(dt, upper, precision=HIGHEST, preferred_element_type=F32)


def thirds(value):
    high = value.astype(BF16).astype(F32)
    rest = value - high
    middle = rest.astype(BF16).astype(F32)
    return [high, middle, rest - middle]


def share_kernel(
    decay_ref, raw_ref, taps_ref, x_ref, b_ref, c_ref,
    small_ref, dt_ref, own_ref, give_ref, own_c_ref, give_c_ref,
):
    heads, tokens = raw_ref.shape
    side = lax.rem(lax.axis_index("sp"), 2)
    other = 1 - side
    raw = raw_ref[...].astype(F32)
    left = 0
    for source in (x_ref, b_ref):
        half = source.shape[1] // 2
        own_ref[:, left : left + half] = source[:, lanes(side * half, half)]
        give_ref[0:tokens, left : left + half] = source[:, lanes(other * half, half)]
        left += half
    half = c_ref.shape[1] // 2
    own_c_ref[...] = c_ref[:, lanes(side * half, half)]
    give_c_ref[...] = c_ref[:, lanes(other * half, half)]
    theirs = jnp.where(other == 0, raw[0 : heads // 2], raw[heads // 2 :])
    per = left // tokens
    flats = []
    for first in range(0, heads // 2, per):
        held = min(per, heads // 2 - first)
        flats.append(
            jnp.concatenate(
                [theirs[first + k : first + k + 1] for k in range(held)]
                + [jnp.zeros((1, tokens), F32)] * (per - held),
                axis=1,
            )
        )
    flats.append(jnp.zeros((EXTRA - len(flats), left), F32))
    give_ref[tokens : tokens + EXTRA, :] = jnp.concatenate(flats, axis=0).astype(BF16)

    dt, prefix = steps_of(raw)
    for group in range(heads // RATIO):
        rows = slice(group * RATIO, (group + 1) * RATIO)
        dt_ref[group, 0:RATIO, :] = prefix[rows]
        dt_ref[group, RATIO:, :] = dt[rows]
    ones = jnp.ones((8, tokens), F32)
    sums = lax.dot_general(
        ones, dt, (((1,), (1,)), ((), ())), precision=HIGHEST, preferred_element_type=F32
    )
    sums = jnp.concatenate([sums[0:1], jnp.zeros((1, 128 - heads), F32)], axis=1)
    common = jnp.concatenate(
        [taps_ref[...].astype(F32)]
        + thirds(jnp.full((1, 128), decay_ref[0], F32))
        + thirds(jnp.full((1, 128), decay_ref[1], F32))
        + thirds(sums)
        + [jnp.zeros((3, 128), F32)],
        axis=0,
    ).astype(BF16)
    ends = []
    for part in range(2):
        rows = []
        tails = [ref[tokens - 8 :, :].astype(F32) for ref in (x_ref, b_ref, c_ref)]
        for token in range(8 - REACH, 8):
            for tail in tails:
                half = tail.shape[1] // 2
                for first in range(part * half, (part + 1) * half, STATE):
                    rows.append(tail[token : token + 1, first : first + STATE])
        ends.append(jnp.concatenate(rows, axis=0).astype(BF16))
    for rank in range(small_ref.shape[0]):
        small_ref[rank, 0:COMMON, :] = common
        small_ref[rank, COMMON:, :] = ends[rank % 2]


def halo_of(shared_ref, first, count):
    pair = lax.axis_index("sp") // 2
    source = jnp.maximum(2 * pair - 1, 0)
    ends = shared_ref[source, COMMON:, :].astype(F32)
    ends = jnp.where(pair == 0, 0.0, ends)
    stride = ends.shape[0] // REACH
    row_id = lax.broadcasted_iota(jnp.int32, ends.shape, 0)
    rows = [jnp.zeros((HALO - REACH, count * STATE), F32)]
    for token in range(REACH):
        picked = [
            jnp.sum(
                jnp.where(row_id == token * stride + first + k, ends, 0.0), axis=0, keepdims=True
            )
            for k in range(count)
        ]
        rows.append(jnp.concatenate(picked, axis=1))
    return jnp.concatenate(rows, axis=0)


def early_kernel(got_ref, dt_ref, steps_ref):
    side = lax.rem(lax.axis_index("sp"), 2)
    groups, _, tokens = steps_ref.shape
    flat = got_ref[...].astype(F32)
    per = flat.shape[1] // tokens
    raw = jnp.concatenate(
        [
            flat[k // per : k // per + 1, k % per * tokens : (k % per + 1) * tokens]
            for k in range(groups * RATIO)
        ],
        axis=0,
    )
    dt, prefix = steps_of(raw)
    for group in range(groups):
        rows = slice(group * RATIO, (group + 1) * RATIO)
        given = jnp.concatenate([prefix[rows], dt[rows]], axis=0)
        own = dt_ref[side * groups + group]
        steps_ref[group, 0 : 2 * RATIO, :] = jnp.where(side == 0, own, given)
        steps_ref[group, 2 * RATIO :, :] = jnp.where(side == 0, given, own)


def state_kernel(
    own_ref, own_b_ref, got_ref, got_b_ref, shared_ref, tb_ref, steps_ref,
    state_ref, first_ref, xin_ref, bin_ref, cum_ref, pad_ref, pad_b_ref,
):
    side = lax.rem(lax.axis_index("sp"), 2)
    tokens = own_ref.shape[0]
    end = tokens - 1
    per = steps_ref.shape[0]
    for k in range(per):
        wide = slice(k * WIDTH, (k + 1) * WIDTH)
        thin = slice(k * STATE, (k + 1) * STATE)
        group = per * pl.program_id(0) + k
        piece = 8 * side + 2 * group
        lower = shared_ref[piece, 0:COMMON, :].astype(F32)
        upper = shared_ref[piece + 1, 0:COMMON, :].astype(F32)
        rows = steps_ref[k]
        logs = []
        for part in (lower, upper):
            for row in (4, 7):
                logs.append(part[row : row + 1] + part[row + 1 : row + 2] + part[row + 2 : row + 3])
        rate = jnp.exp(jnp.concatenate(logs, axis=0))
        cums, tails = [], []
        for block in range(2):
            prefix = rows[8 * block : 8 * block + RATIO]
            dt = rows[8 * block + RATIO : 8 * block + 2 * RATIO]
            cum = -rate * prefix
            cums += [cum, dt]
            tails.append(jnp.exp(cum[:, end : end + 1] - cum) * dt)
        cum_ref[k] = jnp.concatenate(cums, axis=0)
        columns = jnp.transpose(jnp.concatenate(tails, axis=0))
        xin = conv_silu(
            pad_ref.at[k],
            halo_of(shared_ref, 2 * group, 2),
            own_ref[:, wide],
            got_ref[0:tokens, wide],
            side,
            jnp.concatenate([lower[0:4], upper[0:4]], axis=1),
        ).astype(BF16)
        bin_ = conv_silu(
            pad_b_ref.at[k],
            halo_of(shared_ref, 8 + group, 1),
            own_b_ref[:, thin],
            got_b_ref[0:tokens, thin],
            side,
            tb_ref[:, lanes((side * 4 + group) * STATE, STATE)].astype(F32),
        ).astype(BF16)
        bin_ref[:, thin] = bin_
        xin_ref[:, wide] = xin
        states = []
        for block in range(2):
            part = slice(block * tokens, (block + 1) * tokens)
            scale = jnp.concatenate(
                [per_head(columns, 4 * block), per_head(columns, 4 * block + 2)], axis=1
            )
            scaled = (xin[part].astype(F32) * scale).astype(BF16)
            states.append(
                lax.dot_general(
                    bin_[part],
                    scaled,
                    (((0,), (0,)), ((), ())),
                    preferred_element_type=F32,
                )
            )
        both = (states[1] + states[0] * head_row(jnp.exp(cums[2][:, end : end + 1]))).astype(BF16)
        for half in range(2):
            cols = slice(half * STATE, (half + 1) * STATE)
            first_ref[2 * k + half] = states[0][:, cols]
            for part in range(2):
                state_ref[4 * k + 2 * half + part] = both[
                    part * HEAD_DIM : (part + 1) * HEAD_DIM, cols
                ]


def inner_kernel(
    own_ref, got_ref, shared_ref, tc_ref, bin_ref, xin_ref, cum_ref,
    cin_ref, inner_ref, pad_ref,
):
    side = lax.rem(lax.axis_index("sp"), 2)
    group = pl.program_id(0)
    groups = pl.num_programs(0)
    tokens = own_ref.shape[0]
    cin = conv_silu(
        pad_ref,
        halo_of(shared_ref, 12 + group, 1),
        own_ref[...],
        got_ref[...],
        side,
        tc_ref[:, lanes((side * groups + group) * STATE, STATE)].astype(F32),
    ).astype(BF16)
    cin_ref[...] = cin
    row_id = lax.broadcasted_iota(jnp.int32, (tokens, tokens), 0)
    col_id = lax.broadcasted_iota(jnp.int32, (tokens, tokens), 1)
    causal = row_id >= col_id
    for block in range(2):
        part = slice(block * tokens, (block + 1) * tokens)
        scores = lax.dot_general(
            cin[part], bin_ref[part, :], (((1,), (1,)), ((), ())), preferred_element_type=F32
        )
        rows = cum_ref[0, 8 * block : 8 * block + 8, :]
        columns = jnp.transpose(rows)
        for head in range(RATIO):
            spread = columns[:, head : head + 1] - rows[head : head + 1, :]
            decay = jnp.exp(jnp.where(causal, spread, -jnp.inf))
            weights = (scores * decay * rows[RATIO + head : RATIO + head + 1, :]).astype(BF16)
            cols = slice(head * HEAD_DIM, (head + 1) * HEAD_DIM)
            inner_ref[part, cols] = jnp.dot(
                weights, xin_ref[part, cols], preferred_element_type=F32
            )


def scan_kernel(shared_ref, local_ref, out_ref):
    me = lax.axis_index("sp")
    pair = me // 2
    count = local_ref.shape[0]
    sums = jnp.concatenate(
        [
            jnp.sum(shared_ref[rank, 0:COMMON, :].astype(F32)[10:13], axis=0, keepdims=True)
            for rank in range(count)
        ],
        axis=0,
    )
    lane = lax.broadcasted_iota(jnp.int32, sums.shape, 1)
    for upper in range(2):
        ends = []
        for head in range(2):
            mine = jnp.sum(
                jnp.where(lane == count * upper + 2 * pair + head, sums, 0.0),
                axis=1,
                keepdims=True,
            )
            logs = shared_ref[8 * upper + pair, 0:COMMON, :].astype(F32)
            logs = logs[4 + 3 * head : 7 + 3 * head]
            rate = jnp.exp(logs[0:1] + logs[1:2] + logs[2:3])
            ends.append(jnp.exp(-rate * mine))
        decay = jnp.where(lane < HEAD_DIM, ends[0], ends[1])
        entering = jnp.zeros(local_ref.shape[1:], F32)
        for step in range(count // 2):
            slot = 2 * step + upper
            out_ref[slot] = entering.astype(BF16)
            if step + 1 < count // 2:
                passed = decay[2 * step : 2 * step + 1, :] * decay[2 * step + 1 : 2 * step + 2, :]
                entering = entering * passed + local_ref[slot].astype(F32)


def core_of(block, pair, ent_ref, first_ref, cin_ref, inner_ref, cum_ref):
    tokens = cin_ref.shape[0] // 2
    group, half = pair // 2, pair % 2
    rows = cum_ref[group]
    picked = jnp.where(block == 0, rows[0:8], rows[8:16])
    columns = jnp.transpose(jnp.exp(picked))
    cols = slice(half * STATE, (half + 1) * STATE)
    passed = head_row(jnp.exp(rows[0:RATIO, tokens - 1 : tokens]))[:, cols]
    entering = ent_ref[pair].astype(F32) * jnp.where(block == 0, 1.0, passed) + jnp.where(
        block == 0, 0.0, first_ref[pair]
    )
    part = pl.ds(pl.multiple_of(block * tokens, tokens), tokens)
    carried = jnp.dot(
        cin_ref[part, group * STATE : (group + 1) * STATE],
        entering.astype(BF16),
        preferred_element_type=F32,
    )
    inner = inner_ref[part, pair * STATE : (pair + 1) * STATE]
    return (inner + carried * per_head(columns, 2 * half)).astype(BF16)


def average_of():
    row_id = lax.broadcasted_iota(jnp.int32, (STATE, STATE), 0) // HEAD_DIM
    col_id = lax.broadcasted_iota(jnp.int32, (STATE, STATE), 1) // HEAD_DIM
    return jnp.where(row_id == col_id, 1.0 / HEAD_DIM, 0.0).astype(BF16)


def gate_norm(core, gate, gain, average):
    v = core.astype(F32) * silu(gate.astype(F32))
    squares = v * v
    high = squares.astype(BF16)
    low = (squares - high.astype(F32)).astype(BF16)
    mean = jnp.dot(high, average, preferred_element_type=F32) + jnp.dot(
        low, average, preferred_element_type=F32
    )
    return v * lax.rsqrt(mean + NORM_EPS) * gain


def give_kernel(ent_ref, first_ref, cin_ref, inner_ref, cum_ref, core_ref):
    block = 1 - lax.rem(lax.axis_index("sp"), 2)
    for pair in range(ent_ref.shape[0]):
        core_ref[:, pair * STATE : (pair + 1) * STATE] = core_of(
            block, pair, ent_ref, first_ref, cin_ref, inner_ref, cum_ref
        )


def mine_kernel(
    ent_ref, first_ref, cin_ref, inner_ref, cum_ref, z_ref, gain_ref, normed_ref
):
    side = lax.rem(lax.axis_index("sp"), 2)
    average = average_of()
    pairs = ent_ref.shape[0]
    for pair in range(pairs):
        core = core_of(side, pair, ent_ref, first_ref, cin_ref, inner_ref, cum_ref)
        cols = lanes((side * pairs + pair) * STATE, STATE)
        normed_ref[pair] = gate_norm(core, z_ref[:, cols], gain_ref[:, cols], average).astype(BF16)


def join_kernel(a_ref, b_ref, c_ref, d_ref, out_ref):
    rows = a_ref.shape[0]
    for k, ref in enumerate((a_ref, b_ref, c_ref, d_ref)):
        out_ref[k * rows : (k + 1) * rows, :] = ref[...]


def out_kernel(
    core_ref, near_ref, z_ref, gain_ref,
    m0_ref, m1_ref, m2_ref, m3_ref, o0_ref, o1_ref, o2_ref, o3_ref,
    out_ref, normed_ref, ordered_ref, held_ref, acc_ref, sems,
):
    rank = lax.axis_index("dp")
    y, x, core = rank // 8, lax.rem(rank // 2, 4), lax.rem(rank, 2)
    side = lax.rem(lax.axis_index("sp"), 2)
    pieces = (m0_ref, m1_ref, m2_ref, m3_ref, o0_ref, o1_ref, o2_ref, o3_ref)
    deep = m0_ref.shape[0]
    copies = [
        pltpu.make_async_copy(ref, held_ref.at[k * deep : (k + 1) * deep, :], sems.at[k])
        for k, ref in enumerate(pieces)
    ]
    for copy in copies:
        copy.start()
    average = average_of()
    pairs = near_ref.shape[0]
    for pair in range(pairs):
        normed_ref[side * pairs + pair] = near_ref[pair].astype(F32)
        far = (1 - side) * pairs + pair
        cols = lanes(far * STATE, STATE)
        value = gate_norm(
            core_ref[:, pair * STATE : (pair + 1) * STATE],
            z_ref[:, cols],
            gain_ref[:, cols],
            average,
        )
        normed_ref[far] = value
    tokens = out_ref.shape[0]
    lane = lax.broadcasted_iota(jnp.int32, (tokens, STATE), 1)

    def chip(side, position):
        major, minor = position // 4, position % 4
        ry = jnp.where(side == 0, major, minor)
        rx = jnp.where(side == 0, minor, major)
        return lax.rem(y + 4 - ry, 4) * 4 + lax.rem(x + 4 - rx, 4)

    for half, side in enumerate((core, 1 - core)):
        for k in range(8):
            left = normed_ref[chip(side, 2 * k)]
            right = normed_ref[chip(side, 2 * k + 1)]
            turned = pltpu.roll(jnp.where(side == 0, right, left), HEAD_DIM, 1)
            left = jnp.where(side == 0, left, turned)
            right = jnp.where(side == 0, turned, right)
            first = (half * 8 + k) * STATE
            ordered_ref[:, first : first + STATE] = jnp.where(
                lane < HEAD_DIM, left, right
            ).astype(BF16)
    chunk = 512
    stages = 4
    depth = held_ref.shape[0] // stages
    for stage in range(stages):
        for copy in copies[stage * 8 // stages : (stage + 1) * 8 // stages]:
            copy.wait()
        rows = slice(stage * depth, (stage + 1) * depth)
        for first in range(0, out_ref.shape[1], chunk):
            cols = slice(first, first + chunk)
            part = jnp.dot(
                ordered_ref[:, rows], held_ref[rows, cols], preferred_element_type=F32
            )
            if stage:
                part = part + acc_ref[:, cols]
            if stage < stages - 1:
                acc_ref[:, cols] = part
            else:
                out_ref[:, cols] = part.astype(BF16)


def vmem():
    return pl.BlockSpec(memory_space=pltpu.VMEM)


def in_hbm(*values):
    return [pltpu.with_memory_space_constraint(v, pltpu.HBM) for v in values]


def cost(flops, moved, special):
    return pl.CostEstimate(flops=flops, bytes_accessed=moved, transcendentals=special)


def first_step(y, x, core, d):
    return (y, x + d, core) if core == 0 else (y + d, x, core)


def second_step(y, x, core, d):
    return (y + d, x, core) if core == 0 else (y, x + d, core)


def swap_step(y, x, core, d):
    return y, x, 1 - core


def torus(step, d):
    pairs = []
    for rank in range(32):
        y, x, core = step(rank // 8, rank // 2 % 4, rank % 2, d)
        pairs.append((rank, ((y % 4) * 4 + x % 4) * 2 + core))
    return pairs


def step(
    stream_x, stream_b, stream_c, gate_z, step_raw,
    conv_x, conv_b, conv_c, decay_log, norm_gain, w_out,
):
    ranks = lax.axis_size("sp")
    x, b, c, z, raw = (v[0] for v in (stream_x, stream_b, stream_c, gate_z, step_raw))
    tokens, inner_width = x.shape
    wide, thin = inner_width // 2, b.shape[1] // 2
    groups = thin // STATE
    pairs = wide // STATE
    swap = [(i, i ^ 1) for i in range(ranks)]
    x, b, c, raw, taps = in_hbm(x, b, c, jnp.transpose(raw), conv_x)

    cols = wide + thin
    small, dt, own, give, own_c, give_c = pl.pallas_call(
        share_kernel,
        in_specs=[pl.BlockSpec(memory_space=pltpu.SMEM)] + [vmem()] * 5,
        out_specs=[vmem()] * 6,
        out_shape=[
            jax.ShapeDtypeStruct((ranks, COMMON + REACH * (cols + thin) // STATE, STATE), BF16),
            jax.ShapeDtypeStruct((2 * groups, 2 * RATIO, tokens), F32),
            jax.ShapeDtypeStruct((tokens, cols), BF16),
            jax.ShapeDtypeStruct((tokens + EXTRA, cols), BF16),
            jax.ShapeDtypeStruct((tokens, thin), BF16),
            jax.ShapeDtypeStruct((tokens, thin), BF16),
        ],
        compiler_params=pltpu.CompilerParams(vmem_limit_bytes=8 * MIB),
        cost_estimate=cost(10_000_000, 2_000_000, 10_000),
        name="share",
    )(decay_log, raw, taps, x, b, c)
    shared = lax.all_to_all(small, "sp", 0, 0, tiled=True)
    got = lax.ppermute(give, "sp", swap)
    got_c = lax.ppermute(give_c, "sp", swap)

    w1, w2, w3 = (lax.ppermute(w_out, "dp", torus(first_step, d)) for d in (1, 2, 3))
    row = pl.pallas_call(
        join_kernel,
        in_specs=[vmem()] * 4,
        out_specs=vmem(),
        out_shape=jax.ShapeDtypeStruct((4 * w_out.shape[0], w_out.shape[1]), BF16),
        compiler_params=pltpu.CompilerParams(vmem_limit_bytes=8 * MIB),
        cost_estimate=cost(1_000_000, 2_000_000, 0),
        name="join",
    )(w_out, w1, w2, w3)
    mine = [row] + [lax.ppermute(row, "dp", torus(second_step, d)) for d in (1, 2, 3)]
    other = [lax.ppermute(v, "dp", torus(swap_step, 0)) for v in mine]

    steps = pl.pallas_call(
        early_kernel,
        grid=(1,),
        in_specs=[
            pl.BlockSpec((EXTRA, cols), lambda i: (tokens // EXTRA, 0)),
            pl.BlockSpec(dt.shape, lambda i: (0, 0, 0)),
        ],
        out_specs=pl.BlockSpec((groups, 4 * RATIO, tokens), lambda i: (0, 0, 0)),
        out_shape=jax.ShapeDtypeStruct((groups, 4 * RATIO, tokens), F32),
        compiler_params=pltpu.CompilerParams(vmem_limit_bytes=8 * MIB),
        cost_estimate=cost(100_000_000, 100_000, 20_000),
        name="early",
    )(got, dt)

    per = 2
    away = wide // (per * STATE)
    state, first, xin, bin_, cum = pl.pallas_call(
        state_kernel,
        grid=(groups // per,),
        in_specs=[
            pl.BlockSpec((tokens, per * WIDTH), lambda g: (0, g)),
            pl.BlockSpec((tokens, per * STATE), lambda g: (0, away + g)),
            pl.BlockSpec((tokens + EXTRA, per * WIDTH), lambda g: (0, g)),
            pl.BlockSpec((tokens + EXTRA, per * STATE), lambda g: (0, away + g)),
            pl.BlockSpec(shared.shape, lambda g: (0, 0, 0)),
            pl.BlockSpec((4, 2 * thin), lambda g: (0, 0)),
            pl.BlockSpec((per, 4 * RATIO, tokens), lambda g: (g, 0, 0)),
        ],
        out_specs=[
            pl.BlockSpec((4 * per, HEAD_DIM, STATE), lambda g: (g, 0, 0)),
            pl.BlockSpec((2 * per, STATE, STATE), lambda g: (g, 0, 0)),
            pl.BlockSpec((2 * tokens, per * WIDTH), lambda g: (0, g)),
            pl.BlockSpec((2 * tokens, per * STATE), lambda g: (0, g)),
            pl.BlockSpec((per, 4 * RATIO, tokens), lambda g: (g, 0, 0)),
        ],
        out_shape=[
            jax.ShapeDtypeStruct((ranks, HEAD_DIM, STATE), BF16),
            pltpu.HBM((pairs, STATE, STATE), F32),
            pltpu.HBM((2 * tokens, wide), BF16),
            pltpu.HBM((2 * tokens, thin), BF16),
            pltpu.HBM((groups, 4 * RATIO, tokens), F32),
        ],
        scratch_shapes=[
            pltpu.VMEM((per, PAD + 2 * tokens, WIDTH), F32),
            pltpu.VMEM((per, PAD + 2 * tokens, STATE), F32),
        ],
        compiler_params=pltpu.CompilerParams(vmem_limit_bytes=16 * MIB),
        cost_estimate=cost(4_000_000_000, 2_000_000, 400_000),
        name="state",
    )(own, own, got, got, shared, conv_b, steps)

    local = lax.all_to_all(state, "sp", 0, 0, tiled=True)

    cin, inner = pl.pallas_call(
        inner_kernel,
        grid=(groups,),
        in_specs=[
            pl.BlockSpec((tokens, STATE), lambda g: (0, g)),
            pl.BlockSpec((tokens, STATE), lambda g: (0, g)),
            pl.BlockSpec(shared.shape, lambda g: (0, 0, 0)),
            pl.BlockSpec((4, 2 * thin), lambda g: (0, 0)),
            pl.BlockSpec((2 * tokens, STATE), lambda g: (0, g)),
            pl.BlockSpec((2 * tokens, WIDTH), lambda g: (0, g)),
            pl.BlockSpec((1, 4 * RATIO, tokens), lambda g: (g, 0, 0)),
        ],
        out_specs=[
            pl.BlockSpec((2 * tokens, STATE), lambda g: (0, g)),
            pl.BlockSpec((2 * tokens, WIDTH), lambda g: (0, g)),
        ],
        out_shape=[
            pltpu.HBM((2 * tokens, thin), BF16),
            pltpu.HBM((2 * tokens, wide), F32),
        ],
        scratch_shapes=[pltpu.VMEM((PAD + 2 * tokens, STATE), F32)],
        compiler_params=pltpu.CompilerParams(vmem_limit_bytes=16 * MIB),
        cost_estimate=cost(4_000_000_000, 2_000_000, 700_000),
        name="inner",
    )(own_c, got_c, shared, conv_c, *in_hbm(bin_, xin, cum))

    entering = pl.pallas_call(
        scan_kernel,
        in_specs=[vmem(), vmem()],
        out_specs=vmem(),
        out_shape=jax.ShapeDtypeStruct(local.shape, BF16),
        compiler_params=pltpu.CompilerParams(vmem_limit_bytes=8 * MIB),
        cost_estimate=cost(1_000_000_000, 1_000_000, 0),
        name="scan",
    )(shared, local)
    entering = lax.all_to_all(entering, "sp", 0, 0, tiled=True)
    entering = entering.reshape(pairs, STATE, STATE)

    mixer = (entering, *in_hbm(first, cin, inner, cum))
    core = pl.pallas_call(
        give_kernel,
        in_specs=[vmem()] * 5,
        out_specs=vmem(),
        out_shape=jax.ShapeDtypeStruct((tokens, wide), BF16),
        compiler_params=pltpu.CompilerParams(vmem_limit_bytes=8 * MIB),
        cost_estimate=cost(1_000_000_000, 1_000_000, 0),
        name="give",
    )(*mixer)
    got_core = lax.ppermute(core, "sp", swap)
    gain = norm_gain[None]
    normed = pl.pallas_call(
        mine_kernel,
        in_specs=[vmem()] * 7,
        out_specs=vmem(),
        out_shape=jax.ShapeDtypeStruct((pairs, tokens, STATE), BF16),
        compiler_params=pltpu.CompilerParams(vmem_limit_bytes=8 * MIB),
        cost_estimate=cost(2_000_000_000, 1_000_000, 0),
        name="mine",
    )(*mixer, z, gain)
    mixed = pl.pallas_call(
        out_kernel,
        in_specs=[vmem()] * 4 + [pl.BlockSpec(memory_space=pltpu.HBM)] * 4 + [pl.BlockSpec(memory_space=pl.ANY)] * 4,
        out_specs=vmem(),
        out_shape=jax.ShapeDtypeStruct((tokens, w_out.shape[1]), BF16),
        scratch_shapes=[
            pltpu.VMEM((2 * pairs, tokens, STATE), F32),
            pltpu.VMEM((tokens, inner_width), BF16),
            pltpu.VMEM((inner_width, w_out.shape[1]), BF16),
            pltpu.VMEM((tokens, w_out.shape[1]), F32),
            pltpu.SemaphoreType.DMA((8,)),
        ],
        compiler_params=pltpu.CompilerParams(vmem_limit_bytes=OUT_LIMIT),
        cost_estimate=cost(4_000_000_000, 10_000_000, 300_000),
        name="project",
    )(got_core, normed, z, gain, *in_hbm(*mine), *other)
    return mixed[None]


def solution(mesh):
    placed = (
        P("dp", "sp", None),
        P("dp", "sp", None),
        P("dp", "sp", None),
        P("dp", "sp", None),
        P("dp", "sp", None),
        P(None, "sp"),
        P(),
        P(),
        P("sp"),
        P(),
        P("dp", None),
    )
    return jax.shard_map(
        step, mesh=mesh, in_specs=placed, out_specs=P("dp", "sp", None), check_vma=False
    )
```

time: 117 us -> 137 us (1.17)
  the two profiles are of different devices: /device:TPU:2 before, /device:TPU:8 now
where the time goes in v3:
time: 137 us; the launch traced here: 136 us
  starting transfers between devices  79.5 us (58%)
  waiting for transfers between devices  34.4 us (25%)
  Pallas kernels  20.5 us (15%)
    ppermute x1, waiting for transfers between devices, step(): got = lax.ppermute(give, 'sp', swap)  18.7 us
    all_to_all x1, starting transfers between devices, step(): shared = lax.all_to_all(small, 'sp', 0, 0, tiled=True)  15.2 us
    all_to_all x1, starting transfers between devices, step(): entering = lax.all_to_all(entering, 'sp', 0, 0, tiled=True)  12 us
    ppermute x3, starting transfers between devices, step(): lax.ppermute(w_out, 'dp', torus(first_step, d))  11.4 us
    all_to_all x1, starting transfers between devices, step(): local = lax.all_to_all(state, 'sp', 0, 0, tiled=True)  10.8 us
    ppermute x3, starting transfers between devices, step(): lax.ppermute(row, 'dp', torus(second_step, d))  10.7 us
    ppermute x4, starting transfers between devices, step(): other = [lax.ppermute(v, 'dp', torus(swap_step, 0)) for v in mine]  8.16 us
    ppermute x3, waiting for transfers between devices, step(): lax.ppermute(w_out, 'dp', torus(first_step, d))  4.91 us
  transfers between devices with their start and end apart: 16, of which 6 were waited for; matrix products, arithmetic and copies ran while one was open for 0% of the time, Pallas kernels for 8%

profile of v3, /device:TPU:8, one launch (start us, length us, event | category | flops | bytes accessed | tf_op | source)
XLA Modules:
  0.0 135.8 jit_solution(14476140988717065793)
XLA Ops:
  0.0 0.0 copy-start.2
  0.0 0.7 copy-done.2
  0.7 2.2 %share.1 = (bf16[16,64,128]{2,1,0:T(8,128)(2,1)}, f32[8,8,128]{2,1,0:T(8,128)S(1)}, bf16[128,1536]{1,0:T(8,128)(2,1)S(1)}, bf16[136,1536]{1,0:T(8,128)(2,1)S(1)}...) custom-call(f32[2]{0:T(128)S(1)} %copy-done.2, bf16[32,128]{1,0:T(8,128)(2,1)} %bitcast.19, ...), custom_call_target="tpu_custom_call" | custom-call | flops 10000000 | bytes 2000000 | tf_op jit(solution)/shard_map/share/pallas_call | solution.py:510
  2.8 15.2 %all-to-all-start = ((bf16[16,64,128]{2,1,0:T(8,128)(2,1)}), bf16[16,64,128]{2,1,0:T(8,128)(2,1)S(1)}, u32[]{:S(2)}, u32[]{:S(2)}) async-start(bf16[16,64,128]{2,1,0:T(8,128)(2,1)} %get-tuple-element.18), calls=%async_computation | async-start | bytes 524288 | tf_op jit(solution)/shard_map/all_to_all | solution.py:526
  18.0 3.8 %collective-permute-start = (bf16[136,1536]{1,0:T(8,128)(2,1)S(1)}, bf16[136,1536]{1,0:T(8,128)(2,1)S(1)}, u32[]{:S(2)}, u32[]{:S(2)}) collective-permute-start(bf16[136,1536]{1,0:T(8,128)(2,1)S(1)} %get-tuple-element.20), channel_id=1, source_target_pairs={{0,32},{32,0},{64,96},{96,64},{128,160},{160,128},{192,224},{224,1... | collective-permute-start | bytes 1253384 | tf_op jit(solution)/shard_map/ppermute | solution.py:527
  21.9 18.7 %collective-permute-done.got_ref.got_b_ref = bf16[136,1536]{1,0:T(8,128)(2,1)S(1)} collective-permute-done((bf16[136,1536]{1,0:T(8,128)(2,1)S(1)}, bf16[136,1536]{1,0:T(8,128)(2,1)S(1)}, u32[]{:S(2)}, u32[]{:S(2)}) %collective-permute-start) | collective-permute-done | bytes 417824 | tf_op jit(solution)/shard_map/ppermute | solution.py:527
  40.5 0.0 copy-start.4
  40.5 0.2 early.1.steps_ref
  40.7 0.0 all-to-all-done.shared_ref
  40.7 0.5 copy-done.4
  41.2 3.0 %state.1 = (bf16[16,64,128]{2,1,0:T(8,128)(2,1)}, f32[8,128,128]{2,1,0:T(8,128)}, bf16[256,1024]{1,0:T(8,128)(2,1)}, bf16[256,512]{1,0:T(8,128)(2,1)}, f32[4,16,128]{2,1,0:T(8,128)}) custom-call(bf16[128,1536]{1,0:T(8,128)(2,1)S(1)} %get-tuple-element.19.own_ref.own_b_ref, bf16[128,1536]{1,0:T(8,128)(2,1)S(1)} %get-tuple-element.19.own_ref.own_b_ref, ...), custom_call_target="tpu_custom_call" | custom-call | flops 4000000000 | bytes 2000000 | tf_op jit(solution)/shard_map/state/pallas_call | solution.py:559
  44.2 0.0 copy-start.1
  44.2 10.8 %all-to-all-start.1 = ((bf16[16,64,128]{2,1,0:T(8,128)(2,1)}), bf16[16,64,128]{2,1,0:T(8,128)(2,1)S(1)}, u32[]{:S(2)}, u32[]{:S(2)}) async-start(bf16[16,64,128]{2,1,0:T(8,128)(2,1)} %get-tuple-element.22), calls=%async_computation.1 | async-start | bytes 524288 | tf_op jit(solution)/shard_map/all_to_all | solution.py:594
  55.0 0.0 copy-done.1
  55.0 3.4 %collective-permute-start.3 = (bf16[64,2048]{1,0:T(8,128)(2,1)S(1)}, bf16[64,2048]{1,0:T(8,128)(2,1)S(1)}, u32[]{:S(2)}, u32[]{:S(2)}) collective-permute-start(bf16[64,2048]{1,0:T(8,128)(2,1)S(1)} %copy-done.1), channel_id=1, source_target_pairs={{0,2},{1,9},{2,4},{3,11},{4,6},{5,13},{6,0},{7,15},{8,10},{9,17},{... | collective-permute-start | bytes 786440 | tf_op jit(solution)/shard_map/ppermute | solution.py:530
  58.4 4.6 %collective-permute-start.4 = (bf16[64,2048]{1,0:T(8,128)(2,1)S(1)}, bf16[64,2048]{1,0:T(8,128)(2,1)S(1)}, u32[]{:S(2)}, u32[]{:S(2)}) collective-permute-start(bf16[64,2048]{1,0:T(8,128)(2,1)S(1)} %copy-done.1), channel_id=1, source_target_pairs={{0,4},{1,17},{2,6},{3,19},{4,0},{5,21},{6,2},{7,23},{8,12},{9,25},... | collective-permute-start | bytes 786440 | tf_op jit(solution)/shard_map/ppermute | solution.py:530
  63.0 3.3 %collective-permute-start.5 = (bf16[64,2048]{1,0:T(8,128)(2,1)S(1)}, bf16[64,2048]{1,0:T(8,128)(2,1)S(1)}, u32[]{:S(2)}, u32[]{:S(2)}) collective-permute-start(bf16[64,2048]{1,0:T(8,128)(2,1)S(1)} %copy-done.1), channel_id=1, source_target_pairs={{0,6},{1,25},{2,0},{3,27},{4,2},{5,29},{6,4},{7,31},{8,14},{9,1},{... | collective-permute-start | bytes 786440 | tf_op jit(solution)/shard_map/ppermute | solution.py:530
  66.4 0.0 collective-permute-done.3.b_ref
  66.4 1.9 %collective-permute-done.4.c_ref = bf16[64,2048]{1,0:T(8,128)(2,1)S(1)} collective-permute-done((bf16[64,2048]{1,0:T(8,128)(2,1)S(1)}, bf16[64,2048]{1,0:T(8,128)(2,1)S(1)}, u32[]{:S(2)}, u32[]{:S(2)}) %collective-permute-start.4) | collective-permute-done | bytes 262176 | tf_op jit(solution)/shard_map/ppermute | solution.py:530
  68.3 3.0 %collective-permute-done.5.d_ref = bf16[64,2048]{1,0:T(8,128)(2,1)S(1)} collective-permute-done((bf16[64,2048]{1,0:T(8,128)(2,1)S(1)}, bf16[64,2048]{1,0:T(8,128)(2,1)S(1)}, u32[]{:S(2)}, u32[]{:S(2)}) %collective-permute-start.5) | collective-permute-done | bytes 262176 | tf_op jit(solution)/shard_map/ppermute | solution.py:530
  71.3 0.1 join.1.m0_ref
  71.4 0.0 copy-start
  71.4 3.5 %collective-permute-start.6 = (bf16[256,2048]{1,0:T(8,128)(2,1)S(1)}, bf16[256,2048]{1,0:T(8,128)(2,1)}, u32[]{:S(2)}, u32[]{:S(2)}) collective-permute-start(bf16[256,2048]{1,0:T(8,128)(2,1)S(1)} %join.1.m0_ref), channel_id=1, source_target_pairs={{0,8},{1,3},{2,10},{3,5},{4,12},{5,7},{6,14},{7,1},{8,16},{9,11},{... | collective-permute-start | bytes 3145736 | tf_op jit(solution)/shard_map/ppermute | solution.py:540
  74.9 2.8 %collective-permute-start.7 = (bf16[256,2048]{1,0:T(8,128)(2,1)S(1)}, bf16[256,2048]{1,0:T(8,128)(2,1)}, u32[]{:S(2)}, u32[]{:S(2)}) collective-permute-start(bf16[256,2048]{1,0:T(8,128)(2,1)S(1)} %join.1.m0_ref), channel_id=1, source_target_pairs={{0,16},{1,5},{2,18},{3,7},{4,20},{5,1},{6,22},{7,3},{8,24},{9,13},... | collective-permute-start | bytes 3145736 | tf_op jit(solution)/shard_map/ppermute | solution.py:540
  77.7 4.3 %collective-permute-start.8 = (bf16[256,2048]{1,0:T(8,128)(2,1)S(1)}, bf16[256,2048]{1,0:T(8,128)(2,1)}, u32[]{:S(2)}, u32[]{:S(2)}) collective-permute-start(bf16[256,2048]{1,0:T(8,128)(2,1)S(1)} %join.1.m0_ref), channel_id=1, source_target_pairs={{0,24},{1,7},{2,26},{3,1},{4,28},{5,3},{6,30},{7,5},{8,0},{9,15},{... | collective-permute-start | bytes 3145736 | tf_op jit(solution)/shard_map/ppermute | solution.py:540
  82.1 0.0 all-to-all-done.1.local_ref
  82.1 0.9 scan.1
  83.0 12.0 %all-to-all-start.2 = ((bf16[16,64,128]{2,1,0:T(8,128)(2,1)}), bf16[16,64,128]{2,1,0:T(8,128)(2,1)S(1)}, u32[]{:S(2)}, u32[]{:S(2)}) async-start(bf16[16,64,128]{2,1,0:T(8,128)(2,1)} %scan.1), calls=%async_computation.2 | async-start | bytes 524288 | tf_op jit(solution)/shard_map/all_to_all | solution.py:631
  95.0 0.0 copy-done
  95.0 0.0 copy-start.5
  95.0 1.9 %collective-permute-start.9 = (bf16[256,2048]{1,0:T(8,128)(2,1)S(1)}, bf16[256,2048]{1,0:T(8,128)(2,1)S(1)}, u32[]{:S(2)}, u32[]{:S(2)}) collective-permute-start(bf16[256,2048]{1,0:T(8,128)(2,1)S(1)} %join.1.m0_ref), channel_id=1, source_target_pairs={{0,1},{1,0},{2,3},{3,2},{4,5},{5,4},{6,7},{7,6},{8,9},{9,8},{10,11... | collective-permute-start | bytes 3145736 | tf_op jit(solution)/shard_map/ppermute | solution.py:541
  96.9 0.0 collective-permute-done.6.m1_ref
  97.0 2.4 %collective-permute-start.10 = (bf16[256,2048]{1,0:T(8,128)(2,1)}, bf16[256,2048]{1,0:T(8,128)(2,1)}, u32[]{:S(2)}, u32[]{:S(2)}) collective-permute-start(bf16[256,2048]{1,0:T(8,128)(2,1)} %collective-permute-done.6.m1_ref), channel_id=1, source_target_pairs={{0,1},{1,0},{2,3},{3,2},{4,5},{5,4},{6,7},{7,6},{8,9},{9,8},{10,11... | collective-permute-start | bytes 3145736 | tf_op jit(solution)/shard_map/ppermute | solution.py:541
  99.4 0.0 collective-permute-done.7.m2_ref
  99.4 1.9 %collective-permute-start.11 = (bf16[256,2048]{1,0:T(8,128)(2,1)}, bf16[256,2048]{1,0:T(8,128)(2,1)}, u32[]{:S(2)}, u32[]{:S(2)}) collective-permute-start(bf16[256,2048]{1,0:T(8,128)(2,1)} %collective-permute-done.7.m2_ref), channel_id=1, source_target_pairs={{0,1},{1,0},{2,3},{3,2},{4,5},{5,4},{6,7},{7,6},{8,9},{9,8},{10,11... | collective-permute-start | bytes 3145736 | tf_op jit(solution)/shard_map/ppermute | solution.py:541
  101.3 3.1 %collective-permute-done.8.m3_ref = bf16[256,2048]{1,0:T(8,128)(2,1)} collective-permute-done((bf16[256,2048]{1,0:T(8,128)(2,1)S(1)}, bf16[256,2048]{1,0:T(8,128)(2,1)}, u32[]{:S(2)}, u32[]{:S(2)}) %collective-permute-start.8) | collective-permute-done | bytes 1048608 | tf_op jit(solution)/shard_map/ppermute | solution.py:540
  104.4 1.9 %collective-permute-start.12 = (bf16[256,2048]{1,0:T(8,128)(2,1)}, bf16[256,2048]{1,0:T(8,128)(2,1)}, u32[]{:S(2)}, u32[]{:S(2)}) collective-permute-start(bf16[256,2048]{1,0:T(8,128)(2,1)} %collective-permute-done.8.m3_ref), channel_id=1, source_target_pairs={{0,1},{1,0},{2,3},{3,2},{4,5},{5,4},{6,7},{7,6},{8,9},{9,8},{10,11... | collective-permute-start | bytes 3145736 | tf_op jit(solution)/shard_map/ppermute | solution.py:541
  106.3 3.8 %collective-permute-start.1 = (bf16[128,512]{1,0:T(8,128)(2,1)S(1)}, bf16[128,512]{1,0:T(8,128)(2,1)S(1)}, u32[]{:S(2)}, u32[]{:S(2)}) collective-permute-start(bf16[128,512]{1,0:T(8,128)(2,1)S(1)} %get-tuple-element.25), channel_id=1, source_target_pairs={{0,32},{32,0},{64,96},{96,64},{128,160},{160,128},{192,224},{224,1... | collective-permute-start | bytes 393224 | tf_op jit(solution)/shard_map/ppermute | solution.py:528
  110.2 4.1 %collective-permute-done.1.got_ref = bf16[128,512]{1,0:T(8,128)(2,1)S(1)} collective-permute-done((bf16[128,512]{1,0:T(8,128)(2,1)S(1)}, bf16[128,512]{1,0:T(8,128)(2,1)S(1)}, u32[]{:S(2)}, u32[]{:S(2)}) %collective-permute-start.1) | collective-permute-done | bytes 131104 | tf_op jit(solution)/shard_map/ppermute | solution.py:528
  114.3 0.0 copy-done.5
  114.3 4.7 %inner.1 = (bf16[256,512]{1,0:T(8,128)(2,1)}, f32[256,1024]{1,0:T(8,128)}) custom-call(bf16[128,512]{1,0:T(8,128)(2,1)S(1)} %get-tuple-element.24.own_ref, bf16[128,512]{1,0:T(8,128)(2,1)S(1)} %collective-permute-done.1.got_ref, bf16[16,64,128]{2,1,0:T(8,128)(2,1)S(1)} %all-to-all-done.shared_ref, bf16[4,1024]{1,0:T(4,128)(2,1)S(1)} %copy-done.5, ...), custom_call_target="tpu_custom_call" | custom-call | flops 4000000000 | bytes 2000000 | tf_op jit(solution)/shard_map/inner/pallas_call | solution.py:596
  119.0 0.0 all-to-all-done.2
  119.0 0.0 copy-start.3
  119.0 0.0 copy-start.6
  119.0 2.2 %give.1 = bf16[128,1024]{1,0:T(8,128)(2,1)S(1)} custom-call(bf16[8,128,128]{2,1,0:T(8,128)(2,1)S(1)} %bitcast.10, f32[8,128,128]{2,1,0:T(8,128)} %get-tuple-element.23.first_ref, bf16[256,512]{1,0:T(8,128)(2,1)} %get-tuple-element.29.cin_ref, f32[256,1024]{1,0:T(8,128)} %get-tuple-element.30.inner_ref, f32[4,16,128]{2,1,0:T(8,128)} %get-tuple-element.28.cum_ref), custom_call_target="tpu_custom_call" | custom-call | flops 1000000000 | bytes 1000000 | tf_op jit(solution)/shard_map/give/pallas_call | solution.py:635
  121.3 3.6 %collective-permute-start.2 = (bf16[128,1024]{1,0:T(8,128)(2,1)S(1)}, bf16[128,1024]{1,0:T(8,128)(2,1)S(1)}, u32[]{:S(2)}, u32[]{:S(2)}) collective-permute-start(bf16[128,1024]{1,0:T(8,128)(2,1)S(1)} %give.1), channel_id=1, source_target_pairs={{0,32},{32,0},{64,96},{96,64},{128,160},{160,128},{192,224},{224,1... | collective-permute-start | bytes 786440 | tf_op jit(solution)/shard_map/ppermute | solution.py:644
  124.9 0.0 copy-done.3
  124.9 0.0 copy-done.6
  124.9 2.7 %mine.1.near_ref = bf16[8,128,128]{2,1,0:T(8,128)(2,1)S(1)} custom-call(bf16[8,128,128]{2,1,0:T(8,128)(2,1)S(1)} %bitcast.11, f32[8,128,128]{2,1,0:T(8,128)} %get-tuple-element.23.first_ref, bf16[256,512]{1,0:T(8,128)(2,1)} %get-tuple-element.29.cin_ref, f32[256,1024]{1,0:T(8,128)} %get-tuple-element.30.inner_ref, f32[4,16,128]{2,1,0:T(8,128)} %get-tuple-element.28.cum_ref, ...), custom_call_target="tpu_custom_call" | custom-call | flops 2000000000 | bytes 1000000 | tf_op jit(solution)/shard_map/mine/pallas_call | solution.py:646
  127.6 0.0 collective-permute-done.9.o0_ref
  127.7 0.0 collective-permute-done.10.o1_ref
  127.7 0.0 collective-permute-done.11.o2_ref
  127.7 0.0 collective-permute-done.12.o3_ref
  127.7 3.5 %collective-permute-done.2.core_ref = bf16[128,1024]{1,0:T(8,128)(2,1)S(1)} collective-permute-done((bf16[128,1024]{1,0:T(8,128)(2,1)S(1)}, bf16[128,1024]{1,0:T(8,128)(2,1)S(1)}, u32[]{:S(2)}, u32[]{:S(2)}) %collective-permute-start.2) | collective-permute-done | bytes 262176 | tf_op jit(solution)/shard_map/ppermute | solution.py:644
  131.2 4.6 %project.1 = bf16[128,2048]{1,0:T(8,128)(2,1)} custom-call(bf16[128,1024]{1,0:T(8,128)(2,1)S(1)} %collective-permute-done.2.core_ref, bf16[8,128,128]{2,1,0:T(8,128)(2,1)S(1)} %mine.1.near_ref, bf16[128,2048]{1,0:T(8,128)(2,1)S(1)} %bitcast.13, f32[1,2048]{1,0:T(1,128)S(1)} %bitcast.15, bf16[256,2048]{1,0:T(8,128)(2,1)} %copy-done, ...), custom_call_target="tpu_custom_call" | custom-call | flops 4000000000 | bytes 10000000 | tf_op jit(solution)/shard_map/project/pallas_call | solution.py:655
Async XLA Ops:
  0.0 0.7 copy-start.2
  2.8 37.9 %all-to-all-start = ((bf16[16,64,128]{2,1,0:T(8,128)(2,1)}), bf16[16,64,128]{2,1,0:T(8,128)(2,1)S(1)}, u32[]{:S(2)}, u32[]{:S(2)}) async-start(bf16[16,64,128]{2,1,0:T(8,128)(2,1)} %get-tuple-element.18), calls=%async_computation | async-start | bytes 524288 | tf_op jit(solution)/shard_map/all_to_all | solution.py:526
  18.0 22.5 %collective-permute-start = (bf16[136,1536]{1,0:T(8,128)(2,1)S(1)}, bf16[136,1536]{1,0:T(8,128)(2,1)S(1)}, u32[]{:S(2)}, u32[]{:S(2)}) collective-permute-start(bf16[136,1536]{1,0:T(8,128)(2,1)S(1)} %get-tuple-element.20), channel_id=1, source_target_pairs={{0,32},{32,0},{64,96},{96,64},{128,160},{160,128},{192,224},{224,1... | collective-permute-start | bytes 1253384 | tf_op jit(solution)/shard_map/ppermute | solution.py:527
  40.5 0.7 copy-start.4
  44.2 10.8 %copy-start.1 = (bf16[64,2048]{1,0:T(8,128)(2,1)S(1)}, bf16[64,2048]{1,0:T(8,128)(2,1)}, u32[]{:S(2)}) copy-start(bf16[64,2048]{1,0:T(8,128)(2,1)} %a_ref.1) | copy-start | bytes 786436
  44.2 37.9 %all-to-all-start.1 = ((bf16[16,64,128]{2,1,0:T(8,128)(2,1)}), bf16[16,64,128]{2,1,0:T(8,128)(2,1)S(1)}, u32[]{:S(2)}, u32[]{:S(2)}) async-start(bf16[16,64,128]{2,1,0:T(8,128)(2,1)} %get-tuple-element.22), calls=%async_computation.1 | async-start | bytes 524288 | tf_op jit(solution)/shard_map/all_to_all | solution.py:594
  55.0 11.4 %collective-permute-start.3 = (bf16[64,2048]{1,0:T(8,128)(2,1)S(1)}, bf16[64,2048]{1,0:T(8,128)(2,1)S(1)}, u32[]{:S(2)}, u32[]{:S(2)}) collective-permute-start(bf16[64,2048]{1,0:T(8,128)(2,1)S(1)} %copy-done.1), channel_id=1, source_target_pairs={{0,2},{1,9},{2,4},{3,11},{4,6},{5,13},{6,0},{7,15},{8,10},{9,17},{... | collective-permute-start | bytes 786440 | tf_op jit(solution)/shard_map/ppermute | solution.py:530
  58.4 9.9 %collective-permute-start.4 = (bf16[64,2048]{1,0:T(8,128)(2,1)S(1)}, bf16[64,2048]{1,0:T(8,128)(2,1)S(1)}, u32[]{:S(2)}, u32[]{:S(2)}) collective-permute-start(bf16[64,2048]{1,0:T(8,128)(2,1)S(1)} %copy-done.1), channel_id=1, source_target_pairs={{0,4},{1,17},{2,6},{3,19},{4,0},{5,21},{6,2},{7,23},{8,12},{9,25},... | collective-permute-start | bytes 786440 | tf_op jit(solution)/shard_map/ppermute | solution.py:530
  63.0 8.3 %collective-permute-start.5 = (bf16[64,2048]{1,0:T(8,128)(2,1)S(1)}, bf16[64,2048]{1,0:T(8,128)(2,1)S(1)}, u32[]{:S(2)}, u32[]{:S(2)}) collective-permute-start(bf16[64,2048]{1,0:T(8,128)(2,1)S(1)} %copy-done.1), channel_id=1, source_target_pairs={{0,6},{1,25},{2,0},{3,27},{4,2},{5,29},{6,4},{7,31},{8,14},{9,1},{... | collective-permute-start | bytes 786440 | tf_op jit(solution)/shard_map/ppermute | solution.py:530
  71.4 23.6 %copy-start = (bf16[256,2048]{1,0:T(8,128)(2,1)}, bf16[256,2048]{1,0:T(8,128)(2,1)S(1)}, u32[]{:S(2)}) copy-start(bf16[256,2048]{1,0:T(8,128)(2,1)S(1)} %join.1.m0_ref) | copy-start | bytes 3145732
  71.4 25.5 %collective-permute-start.6 = (bf16[256,2048]{1,0:T(8,128)(2,1)S(1)}, bf16[256,2048]{1,0:T(8,128)(2,1)}, u32[]{:S(2)}, u32[]{:S(2)}) collective-permute-start(bf16[256,2048]{1,0:T(8,128)(2,1)S(1)} %join.1.m0_ref), channel_id=1, source_target_pairs={{0,8},{1,3},{2,10},{3,5},{4,12},{5,7},{6,14},{7,1},{8,16},{9,11},{... | collective-permute-start | bytes 3145736 | tf_op jit(solution)/shard_map/ppermute | solution.py:540
  74.9 24.5 %collective-permute-start.7 = (bf16[256,2048]{1,0:T(8,128)(2,1)S(1)}, bf16[256,2048]{1,0:T(8,128)(2,1)}, u32[]{:S(2)}, u32[]{:S(2)}) collective-permute-start(bf16[256,2048]{1,0:T(8,128)(2,1)S(1)} %join.1.m0_ref), channel_id=1, source_target_pairs={{0,16},{1,5},{2,18},{3,7},{4,20},{5,1},{6,22},{7,3},{8,24},{9,13},... | collective-permute-start | bytes 3145736 | tf_op jit(solution)/shard_map/ppermute | solution.py:540
  77.7 26.7 %collective-permute-start.8 = (bf16[256,2048]{1,0:T(8,128)(2,1)S(1)}, bf16[256,2048]{1,0:T(8,128)(2,1)}, u32[]{:S(2)}, u32[]{:S(2)}) collective-permute-start(bf16[256,2048]{1,0:T(8,128)(2,1)S(1)} %join.1.m0_ref), channel_id=1, source_target_pairs={{0,24},{1,7},{2,26},{3,1},{4,28},{5,3},{6,30},{7,5},{8,0},{9,15},{... | collective-permute-start | bytes 3145736 | tf_op jit(solution)/shard_map/ppermute | solution.py:540
  83.0 36.1 %all-to-all-start.2 = ((bf16[16,64,128]{2,1,0:T(8,128)(2,1)}), bf16[16,64,128]{2,1,0:T(8,128)(2,1)S(1)}, u32[]{:S(2)}, u32[]{:S(2)}) async-start(bf16[16,64,128]{2,1,0:T(8,128)(2,1)} %scan.1), calls=%async_computation.2 | async-start | bytes 524288 | tf_op jit(solution)/shard_map/all_to_all | solution.py:631
  95.0 19.3 %copy-start.5 = (bf16[4,1024]{1,0:T(4,128)(2,1)S(1)}, bf16[4,1024]{1,0:T(4,128)(2,1)}, u32[]{:S(2)}) copy-start(bf16[4,1024]{1,0:T(4,128)(2,1)} %tc_ref.1) | copy-start | bytes 24580
  95.0 32.6 %collective-permute-start.9 = (bf16[256,2048]{1,0:T(8,128)(2,1)S(1)}, bf16[256,2048]{1,0:T(8,128)(2,1)S(1)}, u32[]{:S(2)}, u32[]{:S(2)}) collective-permute-start(bf16[256,2048]{1,0:T(8,128)(2,1)S(1)} %join.1.m0_ref), channel_id=1, source_target_pairs={{0,1},{1,0},{2,3},{3,2},{4,5},{5,4},{6,7},{7,6},{8,9},{9,8},{10,11... | collective-permute-start | bytes 3145736 | tf_op jit(solution)/shard_map/ppermute | solution.py:541
  97.0 30.7 %collective-permute-start.10 = (bf16[256,2048]{1,0:T(8,128)(2,1)}, bf16[256,2048]{1,0:T(8,128)(2,1)}, u32[]{:S(2)}, u32[]{:S(2)}) collective-permute-start(bf16[256,2048]{1,0:T(8,128)(2,1)} %collective-permute-done.6.m1_ref), channel_id=1, source_target_pairs={{0,1},{1,0},{2,3},{3,2},{4,5},{5,4},{6,7},{7,6},{8,9},{9,8},{10,11... | collective-permute-start | bytes 3145736 | tf_op jit(solution)/shard_map/ppermute | solution.py:541
  99.4 28.3 %collective-permute-start.11 = (bf16[256,2048]{1,0:T(8,128)(2,1)}, bf16[256,2048]{1,0:T(8,128)(2,1)}, u32[]{:S(2)}, u32[]{:S(2)}) collective-permute-start(bf16[256,2048]{1,0:T(8,128)(2,1)} %collective-permute-done.7.m2_ref), channel_id=1, source_target_pairs={{0,1},{1,0},{2,3},{3,2},{4,5},{5,4},{6,7},{7,6},{8,9},{9,8},{10,11... | collective-permute-start | bytes 3145736 | tf_op jit(solution)/shard_map/ppermute | solution.py:541
  104.4 23.2 %collective-permute-start.12 = (bf16[256,2048]{1,0:T(8,128)(2,1)}, bf16[256,2048]{1,0:T(8,128)(2,1)}, u32[]{:S(2)}, u32[]{:S(2)}) collective-permute-start(bf16[256,2048]{1,0:T(8,128)(2,1)} %collective-permute-done.8.m3_ref), channel_id=1, source_target_pairs={{0,1},{1,0},{2,3},{3,2},{4,5},{5,4},{6,7},{7,6},{8,9},{9,8},{10,11... | collective-permute-start | bytes 3145736 | tf_op jit(solution)/shard_map/ppermute | solution.py:541
  106.3 8.0 %collective-permute-start.1 = (bf16[128,512]{1,0:T(8,128)(2,1)S(1)}, bf16[128,512]{1,0:T(8,128)(2,1)S(1)}, u32[]{:S(2)}, u32[]{:S(2)}) collective-permute-start(bf16[128,512]{1,0:T(8,128)(2,1)S(1)} %get-tuple-element.25), channel_id=1, source_target_pairs={{0,32},{32,0},{64,96},{96,64},{128,160},{160,128},{192,224},{224,1... | collective-permute-start | bytes 393224 | tf_op jit(solution)/shard_map/ppermute | solution.py:528
  119.0 5.9 %copy-start.3 = (bf16[1,128,2048]{2,1,0:T(8,128)(2,1)S(1)}, bf16[1,128,2048]{2,1,0:T(8,128)(2,1)}, u32[]{:S(2)}) copy-start(bf16[1,128,2048]{2,1,0:T(8,128)(2,1)} %param.14) | copy-start | bytes 1572868
  119.0 5.9 %copy-start.6 = (f32[2048]{0:T(1024)S(1)}, f32[2048]{0:T(1024)}, u32[]{:S(2)}) copy-start(f32[2048]{0:T(1024)} %param.20) | copy-start | bytes 24580
  121.3 9.9 %collective-permute-start.2 = (bf16[128,1024]{1,0:T(8,128)(2,1)S(1)}, bf16[128,1024]{1,0:T(8,128)(2,1)S(1)}, u32[]{:S(2)}, u32[]{:S(2)}) collective-permute-start(bf16[128,1024]{1,0:T(8,128)(2,1)S(1)} %give.1), channel_id=1, source_target_pairs={{0,32},{32,0},{64,96},{96,64},{128,160},{160,128},{192,224},{224,1... | collective-permute-start | bytes 786440 | tf_op jit(solution)/shard_map/ppermute | solution.py:644

commit v4 on v3

--- a/solution.py
+++ b/solution.py
@@ -80,7 +80,7 @@
 
 
 def share_kernel(
-    decay_ref, raw_ref, taps_ref, x_ref, b_ref, c_ref,
+    logs_ref, raw_ref, taps_ref, x_ref, b_ref, c_ref,
     small_ref, dt_ref, own_ref, give_ref, own_c_ref, give_c_ref,
 ):
     heads, tokens = raw_ref.shape
@@ -123,8 +123,8 @@
     sums = jnp.concatenate([sums[0:1], jnp.zeros((1, 128 - heads), F32)], axis=1)
     common = jnp.concatenate(
         [taps_ref[...].astype(F32)]
-        + thirds(jnp.full((1, 128), decay_ref[0], F32))
-        + thirds(jnp.full((1, 128), decay_ref[1], F32))
+        + thirds(jnp.broadcast_to(logs_ref[:, 0:1], (1, 128)))
+        + thirds(jnp.broadcast_to(logs_ref[:, 1:2], (1, 128)))
         + thirds(sums)
         + [jnp.zeros((3, 128), F32)],
         axis=0,
@@ -250,7 +250,7 @@
         both = (states[1] + states[0] * head_row(jnp.exp(cums[2][:, end : end + 1]))).astype(BF16)
         for half in range(2):
             cols = slice(half * STATE, (half + 1) * STATE)
-            first_ref[2 * k + half] = states[0][:, cols]
+            first_ref[2 * k + half] = states[0][:, cols].astype(BF16)
             for part in range(2):
                 state_ref[4 * k + 2 * half + part] = both[
                     part * HEAD_DIM : (part + 1) * HEAD_DIM, cols
@@ -329,7 +329,7 @@
 
 
 def core_of(block, pair, ent_ref, first_ref, cin_ref, inner_ref, cum_ref):
-    tokens = cin_ref.shape[0] // 2
+    tokens = cin_ref.shape[0]
     group, half = pair // 2, pair % 2
     rows = cum_ref[group]
     picked = jnp.where(block == 0, rows[0:8], rows[8:16])
@@ -337,15 +337,14 @@
     cols = slice(half * STATE, (half + 1) * STATE)
     passed = head_row(jnp.exp(rows[0:RATIO, tokens - 1 : tokens]))[:, cols]
     entering = ent_ref[pair].astype(F32) * jnp.where(block == 0, 1.0, passed) + jnp.where(
-        block == 0, 0.0, first_ref[pair]
-    )
-    part = pl.ds(pl.multiple_of(block * tokens, tokens), tokens)
+        block == 0, 0.0, first_ref[pair].astype(F32)
+    )
     carried = jnp.dot(
-        cin_ref[part, group * STATE : (group + 1) * STATE],
+        cin_ref[:, group * STATE : (group + 1) * STATE],
         entering.astype(BF16),
         preferred_element_type=F32,
     )
-    inner = inner_ref[part, pair * STATE : (pair + 1) * STATE]
+    inner = inner_ref[:, pair * STATE : (pair + 1) * STATE]
     return (inner + carried * per_head(columns, 2 * half)).astype(BF16)
 
 
@@ -504,12 +503,14 @@
     groups = thin // STATE
     pairs = wide // STATE
     swap = [(i, i ^ 1) for i in range(ranks)]
-    x, b, c, raw, taps = in_hbm(x, b, c, jnp.transpose(raw), conv_x)
+    x, b, c, raw, taps, logs = in_hbm(
+        x, b, c, jnp.transpose(raw), conv_x, decay_log[None]
+    )
 
     cols = wide + thin
     small, dt, own, give, own_c, give_c = pl.pallas_call(
         share_kernel,
-        in_specs=[pl.BlockSpec(memory_space=pltpu.SMEM)] + [vmem()] * 5,
+        in_specs=[vmem()] * 6,
         out_specs=[vmem()] * 6,
         out_shape=[
             jax.ShapeDtypeStruct((ranks, COMMON + REACH * (cols + thin) // STATE, STATE), BF16),
@@ -522,7 +523,7 @@
         compiler_params=pltpu.CompilerParams(vmem_limit_bytes=8 * MIB),
         cost_estimate=cost(10_000_000, 2_000_000, 10_000),
         name="share",
-    )(decay_log, raw, taps, x, b, c)
+    )(logs, raw, taps, x, b, c)
     shared = lax.all_to_all(small, "sp", 0, 0, tiled=True)
     got = lax.ppermute(give, "sp", swap)
     got_c = lax.ppermute(give_c, "sp", swap)
@@ -577,7 +578,7 @@
         ],
         out_shape=[
             jax.ShapeDtypeStruct((ranks, HEAD_DIM, STATE), BF16),
-            pltpu.HBM((pairs, STATE, STATE), F32),
+            pltpu.HBM((pairs, STATE, STATE), BF16),
             pltpu.HBM((2 * tokens, wide), BF16),
             pltpu.HBM((2 * tokens, thin), BF16),
             pltpu.HBM((groups, 4 * RATIO, tokens), F32),
@@ -632,10 +633,31 @@
     entering = entering.reshape(pairs, STATE, STATE)
 
     mixer = (entering, *in_hbm(first, cin, inner, cum))
+
+    def whole(value):
+        return pl.BlockSpec(value.shape, lambda i: (0,) * value.ndim)
+
+    def half_of(value, theirs):
+        def index(i):
+            side = lax.rem(lax.axis_index("sp"), 2)
+            return (1 - side if theirs else side, 0)
+
+        return pl.BlockSpec((value.shape[0] // 2, value.shape[1]), index)
+
+    def mixer_specs(theirs):
+        return [
+            whole(entering),
+            whole(first),
+            half_of(cin, theirs),
+            half_of(inner, theirs),
+            whole(cum),
+        ]
+
     core = pl.pallas_call(
         give_kernel,
-        in_specs=[vmem()] * 5,
-        out_specs=vmem(),
+        grid=(1,),
+        in_specs=mixer_specs(True),
+        out_specs=pl.BlockSpec((tokens, wide), lambda i: (0, 0)),
         out_shape=jax.ShapeDtypeStruct((tokens, wide), BF16),
         compiler_params=pltpu.CompilerParams(vmem_limit_bytes=8 * MIB),
         cost_estimate=cost(1_000_000_000, 1_000_000, 0),
@@ -645,8 +667,9 @@
     gain = norm_gain[None]
     normed = pl.pallas_call(
         mine_kernel,
-        in_specs=[vmem()] * 7,
-        out_specs=vmem(),
+        grid=(1,),
+        in_specs=mixer_specs(False) + [whole(z), whole(gain)],
+        out_specs=pl.BlockSpec((pairs, tokens, STATE), lambda i: (0, 0, 0)),
         out_shape=jax.ShapeDtypeStruct((pairs, tokens, STATE), BF16),
         compiler_params=pltpu.CompilerParams(vmem_limit_bytes=8 * MIB),
         cost_estimate=cost(2_000_000_000, 1_000_000, 0),

time: 137 us -> 136 us (level)
  no operation moved by 1% of the time
where the time goes in v4:
time: 136 us; the launch traced here: 135 us
  starting transfers between devices  79.5 us (58%)
  waiting for transfers between devices  34.6 us (25%)
  Pallas kernels  19.9 us (15%)
    ppermute x1, waiting for transfers between devices, step(): got = lax.ppermute(give, 'sp', swap)  18.7 us
    all_to_all x1, starting transfers between devices, step(): shared = lax.all_to_all(small, 'sp', 0, 0, tiled=True)  15.2 us
    all_to_all x1, starting transfers between devices, step(): entering = lax.all_to_all(entering, 'sp', 0, 0, tiled=True)  12 us
    ppermute x3, starting transfers between devices, step(): lax.ppermute(w_out, 'dp', torus(first_step, d))  11.4 us
    all_to_all x1, starting transfers between devices, step(): local = lax.all_to_all(state, 'sp', 0, 0, tiled=True)  10.8 us
    ppermute x3, starting transfers between devices, step(): lax.ppermute(row, 'dp', torus(second_step, d))  10.7 us
    ppermute x4, starting transfers between devices, step(): other = [lax.ppermute(v, 'dp', torus(swap_step, 0)) for v in mine]  8.16 us
    ppermute x3, waiting for transfers between devices, step(): lax.ppermute(w_out, 'dp', torus(first_step, d))  4.91 us
  transfers between devices with their start and end apart: 16, of which 6 were waited for; matrix products, arithmetic and copies ran while one was open for 0% of the time, Pallas kernels for 8%

profile of v4, /device:TPU:8, one launch (start us, length us, event | category | flops | bytes accessed | tf_op | source)
XLA Modules:
  0.0 134.8 jit_solution(15640285213159077752)
XLA Ops:
  0.0 2.2 %share.1 = (bf16[16,64,128]{2,1,0:T(8,128)(2,1)}, f32[8,8,128]{2,1,0:T(8,128)S(1)}, bf16[128,1536]{1,0:T(8,128)(2,1)S(1)}, bf16[136,1536]{1,0:T(8,128)(2,1)S(1)}...) custom-call(f32[1,2]{1,0:T(1,128)} %bitcast.21, bf16[32,128]{1,0:T(8,128)(2,1)} %bitcast.20, ...), custom_call_target="tpu_custom_call" | custom-call | flops 10000000 | bytes 2000000 | tf_op jit(solution)/shard_map/share/pallas_call | solution.py:511
  2.2 15.2 %all-to-all-start = ((bf16[16,64,128]{2,1,0:T(8,128)(2,1)}), bf16[16,64,128]{2,1,0:T(8,128)(2,1)S(1)}, u32[]{:S(2)}, u32[]{:S(2)}) async-start(bf16[16,64,128]{2,1,0:T(8,128)(2,1)} %get-tuple-element.18), calls=%async_computation | async-start | bytes 524288 | tf_op jit(solution)/shard_map/all_to_all | solution.py:527
  17.4 3.8 %collective-permute-start = (bf16[136,1536]{1,0:T(8,128)(2,1)S(1)}, bf16[136,1536]{1,0:T(8,128)(2,1)S(1)}, u32[]{:S(2)}, u32[]{:S(2)}) collective-permute-start(bf16[136,1536]{1,0:T(8,128)(2,1)S(1)} %get-tuple-element.20), channel_id=1, source_target_pairs={{0,32},{32,0},{64,96},{96,64},{128,160},{160,128},{192,224},{224,1... | collective-permute-start | bytes 1253384 | tf_op jit(solution)/shard_map/ppermute | solution.py:528
  21.2 18.7 %collective-permute-done.got_ref.got_b_ref = bf16[136,1536]{1,0:T(8,128)(2,1)S(1)} collective-permute-done((bf16[136,1536]{1,0:T(8,128)(2,1)S(1)}, bf16[136,1536]{1,0:T(8,128)(2,1)S(1)}, u32[]{:S(2)}, u32[]{:S(2)}) %collective-permute-start) | collective-permute-done | bytes 417824 | tf_op jit(solution)/shard_map/ppermute | solution.py:528
  39.9 0.0 copy-start.3
  39.9 0.2 early.1.steps_ref
  40.1 0.0 all-to-all-done.shared_ref
  40.1 0.5 copy-done.3
  40.6 2.9 %state.1 = (bf16[16,64,128]{2,1,0:T(8,128)(2,1)}, bf16[8,128,128]{2,1,0:T(8,128)(2,1)}, bf16[256,1024]{1,0:T(8,128)(2,1)}, bf16[256,512]{1,0:T(8,128)(2,1)}, f32[4,16,128]{2,1,0:T(8,128)}) custom-call(bf16[128,1536]{1,0:T(8,128)(2,1)S(1)} %get-tuple-element.19.own_ref.own_b_ref, bf16[128,1536]{1,0:T(8,128)(2,1)S(1)} %get-tuple-element.19.own_ref.own_b_ref, ...), custom_call_target="tpu_custom_call" | custom-call | flops 4000000000 | bytes 2000000 | tf_op jit(solution)/shard_map/state/pallas_call | solution.py:560
  43.5 0.0 copy-start.1
  43.5 10.8 %all-to-all-start.1 = ((bf16[16,64,128]{2,1,0:T(8,128)(2,1)}), bf16[16,64,128]{2,1,0:T(8,128)(2,1)S(1)}, u32[]{:S(2)}, u32[]{:S(2)}) async-start(bf16[16,64,128]{2,1,0:T(8,128)(2,1)} %get-tuple-element.22), calls=%async_computation.1 | async-start | bytes 524288 | tf_op jit(solution)/shard_map/all_to_all | solution.py:595
  54.3 0.0 copy-done.1
  54.3 3.4 %collective-permute-start.3 = (bf16[64,2048]{1,0:T(8,128)(2,1)S(1)}, bf16[64,2048]{1,0:T(8,128)(2,1)S(1)}, u32[]{:S(2)}, u32[]{:S(2)}) collective-permute-start(bf16[64,2048]{1,0:T(8,128)(2,1)S(1)} %copy-done.1), channel_id=1, source_target_pairs={{0,2},{1,9},{2,4},{3,11},{4,6},{5,13},{6,0},{7,15},{8,10},{9,17},{... | collective-permute-start | bytes 786440 | tf_op jit(solution)/shard_map/ppermute | solution.py:531
  57.7 4.6 %collective-permute-start.4 = (bf16[64,2048]{1,0:T(8,128)(2,1)S(1)}, bf16[64,2048]{1,0:T(8,128)(2,1)S(1)}, u32[]{:S(2)}, u32[]{:S(2)}) collective-permute-start(bf16[64,2048]{1,0:T(8,128)(2,1)S(1)} %copy-done.1), channel_id=1, source_target_pairs={{0,4},{1,17},{2,6},{3,19},{4,0},{5,21},{6,2},{7,23},{8,12},{9,25},... | collective-permute-start | bytes 786440 | tf_op jit(solution)/shard_map/ppermute | solution.py:531
  62.4 3.3 %collective-permute-start.5 = (bf16[64,2048]{1,0:T(8,128)(2,1)S(1)}, bf16[64,2048]{1,0:T(8,128)(2,1)S(1)}, u32[]{:S(2)}, u32[]{:S(2)}) collective-permute-start(bf16[64,2048]{1,0:T(8,128)(2,1)S(1)} %copy-done.1), channel_id=1, source_target_pairs={{0,6},{1,25},{2,0},{3,27},{4,2},{5,29},{6,4},{7,31},{8,14},{9,1},{... | collective-permute-start | bytes 786440 | tf_op jit(solution)/shard_map/ppermute | solution.py:531
  65.7 0.0 collective-permute-done.3.b_ref
  65.7 1.9 %collective-permute-done.4.c_ref = bf16[64,2048]{1,0:T(8,128)(2,1)S(1)} collective-permute-done((bf16[64,2048]{1,0:T(8,128)(2,1)S(1)}, bf16[64,2048]{1,0:T(8,128)(2,1)S(1)}, u32[]{:S(2)}, u32[]{:S(2)}) %collective-permute-start.4) | collective-permute-done | bytes 262176 | tf_op jit(solution)/shard_map/ppermute | solution.py:531
  67.6 3.0 %collective-permute-done.5.d_ref = bf16[64,2048]{1,0:T(8,128)(2,1)S(1)} collective-permute-done((bf16[64,2048]{1,0:T(8,128)(2,1)S(1)}, bf16[64,2048]{1,0:T(8,128)(2,1)S(1)}, u32[]{:S(2)}, u32[]{:S(2)}) %collective-permute-start.5) | collective-permute-done | bytes 262176 | tf_op jit(solution)/shard_map/ppermute | solution.py:531
  70.6 0.1 join.1.m0_ref
  70.7 0.0 copy-start
  70.7 3.5 %collective-permute-start.6 = (bf16[256,2048]{1,0:T(8,128)(2,1)S(1)}, bf16[256,2048]{1,0:T(8,128)(2,1)}, u32[]{:S(2)}, u32[]{:S(2)}) collective-permute-start(bf16[256,2048]{1,0:T(8,128)(2,1)S(1)} %join.1.m0_ref), channel_id=1, source_target_pairs={{0,8},{1,3},{2,10},{3,5},{4,12},{5,7},{6,14},{7,1},{8,16},{9,11},{... | collective-permute-start | bytes 3145736 | tf_op jit(solution)/shard_map/ppermute | solution.py:541
  74.2 2.9 %collective-permute-start.7 = (bf16[256,2048]{1,0:T(8,128)(2,1)S(1)}, bf16[256,2048]{1,0:T(8,128)(2,1)}, u32[]{:S(2)}, u32[]{:S(2)}) collective-permute-start(bf16[256,2048]{1,0:T(8,128)(2,1)S(1)} %join.1.m0_ref), channel_id=1, source_target_pairs={{0,16},{1,5},{2,18},{3,7},{4,20},{5,1},{6,22},{7,3},{8,24},{9,13},... | collective-permute-start | bytes 3145736 | tf_op jit(solution)/shard_map/ppermute | solution.py:541
  77.1 4.3 %collective-permute-start.8 = (bf16[256,2048]{1,0:T(8,128)(2,1)S(1)}, bf16[256,2048]{1,0:T(8,128)(2,1)}, u32[]{:S(2)}, u32[]{:S(2)}) collective-permute-start(bf16[256,2048]{1,0:T(8,128)(2,1)S(1)} %join.1.m0_ref), channel_id=1, source_target_pairs={{0,24},{1,7},{2,26},{3,1},{4,28},{5,3},{6,30},{7,5},{8,0},{9,15},{... | collective-permute-start | bytes 3145736 | tf_op jit(solution)/shard_map/ppermute | solution.py:541
  81.4 0.0 all-to-all-done.1.local_ref
  81.4 0.9 scan.1
  82.3 12.0 %all-to-all-start.2 = ((bf16[16,64,128]{2,1,0:T(8,128)(2,1)}), bf16[16,64,128]{2,1,0:T(8,128)(2,1)S(1)}, u32[]{:S(2)}, u32[]{:S(2)}) async-start(bf16[16,64,128]{2,1,0:T(8,128)(2,1)} %scan.1), calls=%async_computation.2 | async-start | bytes 524288 | tf_op jit(solution)/shard_map/all_to_all | solution.py:632
  94.3 0.0 copy-done
  94.3 0.0 copy-start.4
  94.3 1.9 %collective-permute-start.9 = (bf16[256,2048]{1,0:T(8,128)(2,1)S(1)}, bf16[256,2048]{1,0:T(8,128)(2,1)S(1)}, u32[]{:S(2)}, u32[]{:S(2)}) collective-permute-start(bf16[256,2048]{1,0:T(8,128)(2,1)S(1)} %join.1.m0_ref), channel_id=1, source_target_pairs={{0,1},{1,0},{2,3},{3,2},{4,5},{5,4},{6,7},{7,6},{8,9},{9,8},{10,11... | collective-permute-start | bytes 3145736 | tf_op jit(solution)/shard_map/ppermute | solution.py:542
  96.3 0.0 collective-permute-done.6.m1_ref
  96.3 2.4 %collective-permute-start.10 = (bf16[256,2048]{1,0:T(8,128)(2,1)}, bf16[256,2048]{1,0:T(8,128)(2,1)}, u32[]{:S(2)}, u32[]{:S(2)}) collective-permute-start(bf16[256,2048]{1,0:T(8,128)(2,1)} %collective-permute-done.6.m1_ref), channel_id=1, source_target_pairs={{0,1},{1,0},{2,3},{3,2},{4,5},{5,4},{6,7},{7,6},{8,9},{9,8},{10,11... | collective-permute-start | bytes 3145736 | tf_op jit(solution)/shard_map/ppermute | solution.py:542
  98.7 0.0 collective-permute-done.7.m2_ref
  98.7 1.9 %collective-permute-start.11 = (bf16[256,2048]{1,0:T(8,128)(2,1)}, bf16[256,2048]{1,0:T(8,128)(2,1)}, u32[]{:S(2)}, u32[]{:S(2)}) collective-permute-start(bf16[256,2048]{1,0:T(8,128)(2,1)} %collective-permute-done.7.m2_ref), channel_id=1, source_target_pairs={{0,1},{1,0},{2,3},{3,2},{4,5},{5,4},{6,7},{7,6},{8,9},{9,8},{10,11... | collective-permute-start | bytes 3145736 | tf_op jit(solution)/shard_map/ppermute | solution.py:542
  100.6 3.1 %collective-permute-done.8.m3_ref = bf16[256,2048]{1,0:T(8,128)(2,1)} collective-permute-done((bf16[256,2048]{1,0:T(8,128)(2,1)S(1)}, bf16[256,2048]{1,0:T(8,128)(2,1)}, u32[]{:S(2)}, u32[]{:S(2)}) %collective-permute-start.8) | collective-permute-done | bytes 1048608 | tf_op jit(solution)/shard_map/ppermute | solution.py:541
  103.8 1.9 %collective-permute-start.12 = (bf16[256,2048]{1,0:T(8,128)(2,1)}, bf16[256,2048]{1,0:T(8,128)(2,1)}, u32[]{:S(2)}, u32[]{:S(2)}) collective-permute-start(bf16[256,2048]{1,0:T(8,128)(2,1)} %collective-permute-done.8.m3_ref), channel_id=1, source_target_pairs={{0,1},{1,0},{2,3},{3,2},{4,5},{5,4},{6,7},{7,6},{8,9},{9,8},{10,11... | collective-permute-start | bytes 3145736 | tf_op jit(solution)/shard_map/ppermute | solution.py:542
  105.7 3.8 %collective-permute-start.1 = (bf16[128,512]{1,0:T(8,128)(2,1)S(1)}, bf16[128,512]{1,0:T(8,128)(2,1)S(1)}, u32[]{:S(2)}, u32[]{:S(2)}) collective-permute-start(bf16[128,512]{1,0:T(8,128)(2,1)S(1)} %get-tuple-element.25), channel_id=1, source_target_pairs={{0,32},{32,0},{64,96},{96,64},{128,160},{160,128},{192,224},{224,1... | collective-permute-start | bytes 393224 | tf_op jit(solution)/shard_map/ppermute | solution.py:529
  109.5 4.1 %collective-permute-done.1.got_ref = bf16[128,512]{1,0:T(8,128)(2,1)S(1)} collective-permute-done((bf16[128,512]{1,0:T(8,128)(2,1)S(1)}, bf16[128,512]{1,0:T(8,128)(2,1)S(1)}, u32[]{:S(2)}, u32[]{:S(2)}) %collective-permute-start.1) | collective-permute-done | bytes 131104 | tf_op jit(solution)/shard_map/ppermute | solution.py:529
  113.7 0.0 copy-done.4
  113.7 4.6 %inner.1 = (bf16[256,512]{1,0:T(8,128)(2,1)}, f32[256,1024]{1,0:T(8,128)}) custom-call(bf16[128,512]{1,0:T(8,128)(2,1)S(1)} %get-tuple-element.24.own_ref, bf16[128,512]{1,0:T(8,128)(2,1)S(1)} %collective-permute-done.1.got_ref, bf16[16,64,128]{2,1,0:T(8,128)(2,1)S(1)} %all-to-all-done.shared_ref, bf16[4,1024]{1,0:T(4,128)(2,1)S(1)} %copy-done.4, ...), custom_call_target="tpu_custom_call" | custom-call | flops 4000000000 | bytes 2000000 | tf_op jit(solution)/shard_map/inner/pallas_call | solution.py:597
  118.3 0.0 all-to-all-done.2
  118.3 0.0 copy-start.2
  118.3 0.0 copy-start.5
  118.3 2.0 %give.1 = bf16[128,1024]{1,0:T(8,128)(2,1)S(1)} custom-call(bf16[8,128,128]{2,1,0:T(8,128)(2,1)S(1)} %bitcast.11, bf16[8,128,128]{2,1,0:T(8,128)(2,1)} %get-tuple-element.23.first_ref, bf16[256,512]{1,0:T(8,128)(2,1)} %get-tuple-element.29.cin_ref, f32[256,1024]{1,0:T(8,128)} %get-tuple-element.30.inner_ref, f32[4,16,128]{2,1,0:T(8,128)} %get-tuple-element.28.cum_ref), custom_call_target="tpu_custom_call" | custom-call | flops 1000000000 | bytes 1000000 | tf_op jit(solution)/shard_map/give/pallas_call | solution.py:656
  120.3 3.6 %collective-permute-start.2 = (bf16[128,1024]{1,0:T(8,128)(2,1)S(1)}, bf16[128,1024]{1,0:T(8,128)(2,1)S(1)}, u32[]{:S(2)}, u32[]{:S(2)}) collective-permute-start(bf16[128,1024]{1,0:T(8,128)(2,1)S(1)} %give.1), channel_id=1, source_target_pairs={{0,32},{32,0},{64,96},{96,64},{128,160},{160,128},{192,224},{224,1... | collective-permute-start | bytes 786440 | tf_op jit(solution)/shard_map/ppermute | solution.py:666
  123.9 0.0 copy-done.2
  124.0 0.0 copy-done.5
  124.0 2.4 %mine.1.near_ref = bf16[8,128,128]{2,1,0:T(8,128)(2,1)S(1)} custom-call(bf16[8,128,128]{2,1,0:T(8,128)(2,1)S(1)} %bitcast.12, bf16[8,128,128]{2,1,0:T(8,128)(2,1)} %get-tuple-element.23.first_ref, bf16[256,512]{1,0:T(8,128)(2,1)} %get-tuple-element.29.cin_ref, f32[256,1024]{1,0:T(8,128)} %get-tuple-element.30.inner_ref, ...), custom_call_target="tpu_custom_call" | custom-call | flops 2000000000 | bytes 1000000 | tf_op jit(solution)/shard_map/mine/pallas_call | solution.py:668
  126.4 0.0 collective-permute-done.9.o0_ref
  126.4 0.0 collective-permute-done.10.o1_ref
  126.4 0.0 collective-permute-done.11.o2_ref
  126.5 0.0 collective-permute-done.12.o3_ref
  126.5 3.8 %collective-permute-done.2.core_ref = bf16[128,1024]{1,0:T(8,128)(2,1)S(1)} collective-permute-done((bf16[128,1024]{1,0:T(8,128)(2,1)S(1)}, bf16[128,1024]{1,0:T(8,128)(2,1)S(1)}, u32[]{:S(2)}, u32[]{:S(2)}) %collective-permute-start.2) | collective-permute-done | bytes 262176 | tf_op jit(solution)/shard_map/ppermute | solution.py:666
  130.2 4.6 %project.1 = bf16[128,2048]{1,0:T(8,128)(2,1)} custom-call(bf16[128,1024]{1,0:T(8,128)(2,1)S(1)} %collective-permute-done.2.core_ref, bf16[8,128,128]{2,1,0:T(8,128)(2,1)S(1)} %mine.1.near_ref, bf16[128,2048]{1,0:T(8,128)(2,1)S(1)} %bitcast.14, f32[1,2048]{1,0:T(1,128)S(1)} %bitcast.16, bf16[256,2048]{1,0:T(8,128)(2,1)} %copy-done, ...), custom_call_target="tpu_custom_call" | custom-call | flops 4000000000 | bytes 10000000 | tf_op jit(solution)/shard_map/project/pallas_call | solution.py:678
Async XLA Ops:
  2.2 37.9 %all-to-all-start = ((bf16[16,64,128]{2,1,0:T(8,128)(2,1)}), bf16[16,64,128]{2,1,0:T(8,128)(2,1)S(1)}, u32[]{:S(2)}, u32[]{:S(2)}) async-start(bf16[16,64,128]{2,1,0:T(8,128)(2,1)} %get-tuple-element.18), calls=%async_computation | async-start | bytes 524288 | tf_op jit(solution)/shard_map/all_to_all | solution.py:527
  17.4 22.5 %collective-permute-start = (bf16[136,1536]{1,0:T(8,128)(2,1)S(1)}, bf16[136,1536]{1,0:T(8,128)(2,1)S(1)}, u32[]{:S(2)}, u32[]{:S(2)}) collective-permute-start(bf16[136,1536]{1,0:T(8,128)(2,1)S(1)} %get-tuple-element.20), channel_id=1, source_target_pairs={{0,32},{32,0},{64,96},{96,64},{128,160},{160,128},{192,224},{224,1... | collective-permute-start | bytes 1253384 | tf_op jit(solution)/shard_map/ppermute | solution.py:528
  39.9 0.7 copy-start.3
  43.5 10.8 %copy-start.1 = (bf16[64,2048]{1,0:T(8,128)(2,1)S(1)}, bf16[64,2048]{1,0:T(8,128)(2,1)}, u32[]{:S(2)}) copy-start(bf16[64,2048]{1,0:T(8,128)(2,1)} %a_ref.1) | copy-start | bytes 786436
  43.5 37.9 %all-to-all-start.1 = ((bf16[16,64,128]{2,1,0:T(8,128)(2,1)}), bf16[16,64,128]{2,1,0:T(8,128)(2,1)S(1)}, u32[]{:S(2)}, u32[]{:S(2)}) async-start(bf16[16,64,128]{2,1,0:T(8,128)(2,1)} %get-tuple-element.22), calls=%async_computation.1 | async-start | bytes 524288 | tf_op jit(solution)/shard_map/all_to_all | solution.py:595
  54.3 11.4 %collective-permute-start.3 = (bf16[64,2048]{1,0:T(8,128)(2,1)S(1)}, bf16[64,2048]{1,0:T(8,128)(2,1)S(1)}, u32[]{:S(2)}, u32[]{:S(2)}) collective-permute-start(bf16[64,2048]{1,0:T(8,128)(2,1)S(1)} %copy-done.1), channel_id=1, source_target_pairs={{0,2},{1,9},{2,4},{3,11},{4,6},{5,13},{6,0},{7,15},{8,10},{9,17},{... | collective-permute-start | bytes 786440 | tf_op jit(solution)/shard_map/ppermute | solution.py:531
  57.7 9.9 %collective-permute-start.4 = (bf16[64,2048]{1,0:T(8,128)(2,1)S(1)}, bf16[64,2048]{1,0:T(8,128)(2,1)S(1)}, u32[]{:S(2)}, u32[]{:S(2)}) collective-permute-start(bf16[64,2048]{1,0:T(8,128)(2,1)S(1)} %copy-done.1), channel_id=1, source_target_pairs={{0,4},{1,17},{2,6},{3,19},{4,0},{5,21},{6,2},{7,23},{8,12},{9,25},... | collective-permute-start | bytes 786440 | tf_op jit(solution)/shard_map/ppermute | solution.py:531
  62.4 8.3 %collective-permute-start.5 = (bf16[64,2048]{1,0:T(8,128)(2,1)S(1)}, bf16[64,2048]{1,0:T(8,128)(2,1)S(1)}, u32[]{:S(2)}, u32[]{:S(2)}) collective-permute-start(bf16[64,2048]{1,0:T(8,128)(2,1)S(1)} %copy-done.1), channel_id=1, source_target_pairs={{0,6},{1,25},{2,0},{3,27},{4,2},{5,29},{6,4},{7,31},{8,14},{9,1},{... | collective-permute-start | bytes 786440 | tf_op jit(solution)/shard_map/ppermute | solution.py:531
  70.7 23.6 %copy-start = (bf16[256,2048]{1,0:T(8,128)(2,1)}, bf16[256,2048]{1,0:T(8,128)(2,1)S(1)}, u32[]{:S(2)}) copy-start(bf16[256,2048]{1,0:T(8,128)(2,1)S(1)} %join.1.m0_ref) | copy-start | bytes 3145732
  70.7 25.5 %collective-permute-start.6 = (bf16[256,2048]{1,0:T(8,128)(2,1)S(1)}, bf16[256,2048]{1,0:T(8,128)(2,1)}, u32[]{:S(2)}, u32[]{:S(2)}) collective-permute-start(bf16[256,2048]{1,0:T(8,128)(2,1)S(1)} %join.1.m0_ref), channel_id=1, source_target_pairs={{0,8},{1,3},{2,10},{3,5},{4,12},{5,7},{6,14},{7,1},{8,16},{9,11},{... | collective-permute-start | bytes 3145736 | tf_op jit(solution)/shard_map/ppermute | solution.py:541
  74.2 24.5 %collective-permute-start.7 = (bf16[256,2048]{1,0:T(8,128)(2,1)S(1)}, bf16[256,2048]{1,0:T(8,128)(2,1)}, u32[]{:S(2)}, u32[]{:S(2)}) collective-permute-start(bf16[256,2048]{1,0:T(8,128)(2,1)S(1)} %join.1.m0_ref), channel_id=1, source_target_pairs={{0,16},{1,5},{2,18},{3,7},{4,20},{5,1},{6,22},{7,3},{8,24},{9,13},... | collective-permute-start | bytes 3145736 | tf_op jit(solution)/shard_map/ppermute | solution.py:541
  77.1 26.7 %collective-permute-start.8 = (bf16[256,2048]{1,0:T(8,128)(2,1)S(1)}, bf16[256,2048]{1,0:T(8,128)(2,1)}, u32[]{:S(2)}, u32[]{:S(2)}) collective-permute-start(bf16[256,2048]{1,0:T(8,128)(2,1)S(1)} %join.1.m0_ref), channel_id=1, source_target_pairs={{0,24},{1,7},{2,26},{3,1},{4,28},{5,3},{6,30},{7,5},{8,0},{9,15},{... | collective-permute-start | bytes 3145736 | tf_op jit(solution)/shard_map/ppermute | solution.py:541
  82.3 36.0 %all-to-all-start.2 = ((bf16[16,64,128]{2,1,0:T(8,128)(2,1)}), bf16[16,64,128]{2,1,0:T(8,128)(2,1)S(1)}, u32[]{:S(2)}, u32[]{:S(2)}) async-start(bf16[16,64,128]{2,1,0:T(8,128)(2,1)} %scan.1), calls=%async_computation.2 | async-start | bytes 524288 | tf_op jit(solution)/shard_map/all_to_all | solution.py:632
  94.3 19.3 %copy-start.4 = (bf16[4,1024]{1,0:T(4,128)(2,1)S(1)}, bf16[4,1024]{1,0:T(4,128)(2,1)}, u32[]{:S(2)}) copy-start(bf16[4,1024]{1,0:T(4,128)(2,1)} %tc_ref.1) | copy-start | bytes 24580
  94.3 32.1 %collective-permute-start.9 = (bf16[256,2048]{1,0:T(8,128)(2,1)S(1)}, bf16[256,2048]{1,0:T(8,128)(2,1)S(1)}, u32[]{:S(2)}, u32[]{:S(2)}) collective-permute-start(bf16[256,2048]{1,0:T(8,128)(2,1)S(1)} %join.1.m0_ref), channel_id=1, source_target_pairs={{0,1},{1,0},{2,3},{3,2},{4,5},{5,4},{6,7},{7,6},{8,9},{9,8},{10,11... | collective-permute-start | bytes 3145736 | tf_op jit(solution)/shard_map/ppermute | solution.py:542
  96.3 30.2 %collective-permute-start.10 = (bf16[256,2048]{1,0:T(8,128)(2,1)}, bf16[256,2048]{1,0:T(8,128)(2,1)}, u32[]{:S(2)}, u32[]{:S(2)}) collective-permute-start(bf16[256,2048]{1,0:T(8,128)(2,1)} %collective-permute-done.6.m1_ref), channel_id=1, source_target_pairs={{0,1},{1,0},{2,3},{3,2},{4,5},{5,4},{6,7},{7,6},{8,9},{9,8},{10,11... | collective-permute-start | bytes 3145736 | tf_op jit(solution)/shard_map/ppermute | solution.py:542
  98.7 27.7 %collective-permute-start.11 = (bf16[256,2048]{1,0:T(8,128)(2,1)}, bf16[256,2048]{1,0:T(8,128)(2,1)}, u32[]{:S(2)}, u32[]{:S(2)}) collective-permute-start(bf16[256,2048]{1,0:T(8,128)(2,1)} %collective-permute-done.7.m2_ref), channel_id=1, source_target_pairs={{0,1},{1,0},{2,3},{3,2},{4,5},{5,4},{6,7},{7,6},{8,9},{9,8},{10,11... | collective-permute-start | bytes 3145736 | tf_op jit(solution)/shard_map/ppermute | solution.py:542
  103.8 22.7 %collective-permute-start.12 = (bf16[256,2048]{1,0:T(8,128)(2,1)}, bf16[256,2048]{1,0:T(8,128)(2,1)}, u32[]{:S(2)}, u32[]{:S(2)}) collective-permute-start(bf16[256,2048]{1,0:T(8,128)(2,1)} %collective-permute-done.8.m3_ref), channel_id=1, source_target_pairs={{0,1},{1,0},{2,3},{3,2},{4,5},{5,4},{6,7},{7,6},{8,9},{9,8},{10,11... | collective-permute-start | bytes 3145736 | tf_op jit(solution)/shard_map/ppermute | solution.py:542
  105.7 8.0 %collective-permute-start.1 = (bf16[128,512]{1,0:T(8,128)(2,1)S(1)}, bf16[128,512]{1,0:T(8,128)(2,1)S(1)}, u32[]{:S(2)}, u32[]{:S(2)}) collective-permute-start(bf16[128,512]{1,0:T(8,128)(2,1)S(1)} %get-tuple-element.25), channel_id=1, source_target_pairs={{0,32},{32,0},{64,96},{96,64},{128,160},{160,128},{192,224},{224,1... | collective-permute-start | bytes 393224 | tf_op jit(solution)/shard_map/ppermute | solution.py:529
  118.3 5.6 %copy-start.2 = (bf16[1,128,2048]{2,1,0:T(8,128)(2,1)S(1)}, bf16[1,128,2048]{2,1,0:T(8,128)(2,1)}, u32[]{:S(2)}) copy-start(bf16[1,128,2048]{2,1,0:T(8,128)(2,1)} %param.14) | copy-start | bytes 1572868
  118.3 5.7 %copy-start.5 = (f32[2048]{0:T(1024)S(1)}, f32[2048]{0:T(1024)}, u32[]{:S(2)}) copy-start(f32[2048]{0:T(1024)} %param.20) | copy-start | bytes 24580
  120.3 9.9 %collective-permute-start.2 = (bf16[128,1024]{1,0:T(8,128)(2,1)S(1)}, bf16[128,1024]{1,0:T(8,128)(2,1)S(1)}, u32[]{:S(2)}, u32[]{:S(2)}) collective-permute-start(bf16[128,1024]{1,0:T(8,128)(2,1)S(1)} %give.1), channel_id=1, source_target_pairs={{0,32},{32,0},{64,96},{96,64},{128,160},{160,128},{192,224},{224,1... | collective-permute-start | bytes 786440 | tf_op jit(solution)/shard_map/ppermute | solution.py:666

commit v5 on v4

--- a/solution.py
+++ b/solution.py
@@ -391,22 +391,23 @@
         out_ref[k * rows : (k + 1) * rows, :] = ref[...]
 
 
-def out_kernel(
-    core_ref, near_ref, z_ref, gain_ref,
-    m0_ref, m1_ref, m2_ref, m3_ref, o0_ref, o1_ref, o2_ref, o3_ref,
-    out_ref, normed_ref, ordered_ref, held_ref, acc_ref, sems,
-):
-    rank = lax.axis_index("dp")
-    y, x, core = rank // 8, lax.rem(rank // 2, 4), lax.rem(rank, 2)
-    side = lax.rem(lax.axis_index("sp"), 2)
-    pieces = (m0_ref, m1_ref, m2_ref, m3_ref, o0_ref, o1_ref, o2_ref, o3_ref)
-    deep = m0_ref.shape[0]
+def hold_kernel(*refs):
+    pieces, held_ref, sems = refs[:8], refs[8], refs[9]
+    deep = pieces[0].shape[0]
     copies = [
         pltpu.make_async_copy(ref, held_ref.at[k * deep : (k + 1) * deep, :], sems.at[k])
         for k, ref in enumerate(pieces)
     ]
     for copy in copies:
         copy.start()
+    for copy in copies:
+        copy.wait()
+
+
+def out_kernel(core_ref, near_ref, z_ref, gain_ref, held_ref, out_ref, normed_ref, ordered_ref):
+    rank = lax.axis_index("dp")
+    y, x, core = rank // 8, lax.rem(rank // 2, 4), lax.rem(rank, 2)
+    side = lax.rem(lax.axis_index("sp"), 2)
     average = average_of()
     pairs = near_ref.shape[0]
     for pair in range(pairs):
@@ -441,23 +442,11 @@
                 lane < HEAD_DIM, left, right
             ).astype(BF16)
     chunk = 512
-    stages = 4
-    depth = held_ref.shape[0] // stages
-    for stage in range(stages):
-        for copy in copies[stage * 8 // stages : (stage + 1) * 8 // stages]:
-            copy.wait()
-        rows = slice(stage * depth, (stage + 1) * depth)
-        for first in range(0, out_ref.shape[1], chunk):
-            cols = slice(first, first + chunk)
-            part = jnp.dot(
-                ordered_ref[:, rows], held_ref[rows, cols], preferred_element_type=F32
-            )
-            if stage:
-                part = part + acc_ref[:, cols]
-            if stage < stages - 1:
-                acc_ref[:, cols] = part
-            else:
-                out_ref[:, cols] = part.astype(BF16)
+    for first in range(0, out_ref.shape[1], chunk):
+        cols = slice(first, first + chunk)
+        out_ref[:, cols] = jnp.dot(
+            ordered_ref[...], held_ref[:, cols], preferred_element_type=F32
+        ).astype(BF16)
 
 
 def vmem():
@@ -674,23 +663,30 @@
         compiler_params=pltpu.CompilerParams(vmem_limit_bytes=8 * MIB),
         cost_estimate=cost(2_000_000_000, 1_000_000, 0),
         name="mine",
-    )(*mixer, z, gain)
+    )(*mixer, *in_hbm(z, gain))
+    held = pl.pallas_call(
+        hold_kernel,
+        in_specs=[pl.BlockSpec(memory_space=pl.ANY)] * 8,
+        out_specs=pl.BlockSpec(memory_space=pltpu.VMEM),
+        out_shape=pltpu.VMEM((inner_width, w_out.shape[1]), BF16),
+        scratch_shapes=[pltpu.SemaphoreType.DMA((8,))],
+        compiler_params=pltpu.CompilerParams(vmem_limit_bytes=16 * MIB),
+        cost_estimate=cost(1_000_000, 16_000_000, 0),
+        name="hold",
+    )(*in_hbm(*mine), *other)
     mixed = pl.pallas_call(
         out_kernel,
-        in_specs=[vmem()] * 4 + [pl.BlockSpec(memory_space=pltpu.HBM)] * 4 + [pl.BlockSpec(memory_space=pl.ANY)] * 4,
+        in_specs=[vmem()] * 5,
         out_specs=vmem(),
         out_shape=jax.ShapeDtypeStruct((tokens, w_out.shape[1]), BF16),
         scratch_shapes=[
             pltpu.VMEM((2 * pairs, tokens, STATE), F32),
             pltpu.VMEM((tokens, inner_width), BF16),
-            pltpu.VMEM((inner_width, w_out.shape[1]), BF16),
-            pltpu.VMEM((tokens, w_out.shape[1]), F32),
-            pltpu.SemaphoreType.DMA((8,)),
         ],
         compiler_params=pltpu.CompilerParams(vmem_limit_bytes=OUT_LIMIT),
         cost_estimate=cost(4_000_000_000, 10_000_000, 300_000),
         name="project",
-    )(got_core, normed, z, gain, *in_hbm(*mine), *other)
+    )(got_core, normed, z, gain, held)
     return mixed[None]
 
 

time: 136 us -> 120 us (0.88)
  the two profiles are of different devices: /device:TPU:8 before, /device:TPU:2 now
where the time goes in v5:
time: 120 us; the launch traced here: 119 us
  starting transfers between devices  71.4 us (60%)
  waiting for transfers between devices  25.1 us (21%)
  Pallas kernels  21 us (18%)
  local copies, waits for them, and re-layouts  1.38 us (1%)
    all_to_all x1, starting transfers between devices, step(): shared = lax.all_to_all(small, 'sp', 0, 0, tiled=True)  15.3 us
    all_to_all x1, starting transfers between devices, step(): local = lax.all_to_all(state, 'sp', 0, 0, tiled=True)  10.6 us
    ppermute x3, starting transfers between devices, step(): lax.ppermute(row, 'dp', torus(second_step, d))  10.3 us
    ppermute x3, starting transfers between devices, step(): lax.ppermute(w_out, 'dp', torus(first_step, d))  9.88 us
    ppermute x1, waiting for transfers between devices, step(): got = lax.ppermute(give, 'sp', swap)  8.75 us
    ppermute x4, starting transfers between devices, step(): other = [lax.ppermute(v, 'dp', torus(swap_step, 0)) for v in mine]  8.15 us
    all_to_all x1, waiting for transfers between devices, step(): local = lax.all_to_all(state, 'sp', 0, 0, tiled=True)  8.03 us
    all_to_all x1, starting transfers between devices, step(): entering = lax.all_to_all(entering, 'sp', 0, 0, tiled=True)  5.61 us
  transfers between devices with their start and end apart: 16, of which 6 were waited for; matrix products, arithmetic and copies ran while one was open for 0% of the time, Pallas kernels for 14%

profile of v5, /device:TPU:2, one launch (start us, length us, event | category | flops | bytes accessed | tf_op | source)
XLA Modules:
  0.0 119.2 jit_solution(16113595947873920670)
XLA Ops:
  0.0 2.2 %share.1 = (bf16[16,64,128]{2,1,0:T(8,128)(2,1)}, f32[8,8,128]{2,1,0:T(8,128)S(1)}, bf16[128,1536]{1,0:T(8,128)(2,1)S(1)}, bf16[136,1536]{1,0:T(8,128)(2,1)S(1)}...) custom-call(f32[1,2]{1,0:T(1,128)} %bitcast.19, bf16[32,128]{1,0:T(8,128)(2,1)} %bitcast.18, ...), custom_call_target="tpu_custom_call" | custom-call | flops 10000000 | bytes 2000000 | tf_op jit(solution)/shard_map/share/pallas_call | solution.py:500
  2.2 0.0 copy-start.3
  2.2 0.7 copy-done.3
  2.8 0.0 copy-start.1
  2.8 15.3 %all-to-all-start = ((bf16[16,64,128]{2,1,0:T(8,128)(2,1)}), bf16[16,64,128]{2,1,0:T(8,128)(2,1)S(1)}, u32[]{:S(2)}, u32[]{:S(2)}) async-start(bf16[16,64,128]{2,1,0:T(8,128)(2,1)} %get-tuple-element.18), calls=%async_computation | async-start | bytes 524288 | tf_op jit(solution)/shard_map/all_to_all | solution.py:516
  18.2 3.8 %collective-permute-start = (bf16[136,1536]{1,0:T(8,128)(2,1)S(1)}, bf16[136,1536]{1,0:T(8,128)(2,1)S(1)}, u32[]{:S(2)}, u32[]{:S(2)}) collective-permute-start(bf16[136,1536]{1,0:T(8,128)(2,1)S(1)} %get-tuple-element.20), channel_id=1, source_target_pairs={{0,32},{32,0},{64,96},{96,64},{128,160},{160,128},{192,224},{224,1... | collective-permute-start | bytes 1253384 | tf_op jit(solution)/shard_map/ppermute | solution.py:517
  22.0 4.0 %collective-permute-start.4 = (bf16[64,2048]{1,0:T(8,128)(2,1)}, bf16[64,2048]{1,0:T(8,128)(2,1)S(1)}, u32[]{:S(2)}, u32[]{:S(2)}) collective-permute-start(bf16[64,2048]{1,0:T(8,128)(2,1)} %a_ref.1), channel_id=1, source_target_pairs={{0,4},{1,17},{2,6},{3,19},{4,0},{5,21},{6,2},{7,23},{8,12},{9,25},... | collective-permute-start | bytes 786440 | tf_op jit(solution)/shard_map/ppermute | solution.py:520
  26.1 1.9 %collective-permute-start.3 = (bf16[64,2048]{1,0:T(8,128)(2,1)}, bf16[64,2048]{1,0:T(8,128)(2,1)S(1)}, u32[]{:S(2)}, u32[]{:S(2)}) collective-permute-start(bf16[64,2048]{1,0:T(8,128)(2,1)} %a_ref.1), channel_id=1, source_target_pairs={{0,2},{1,9},{2,4},{3,11},{4,6},{5,13},{6,0},{7,15},{8,10},{9,17},{... | collective-permute-start | bytes 786440 | tf_op jit(solution)/shard_map/ppermute | solution.py:520
  28.0 3.9 %collective-permute-start.5 = (bf16[64,2048]{1,0:T(8,128)(2,1)}, bf16[64,2048]{1,0:T(8,128)(2,1)S(1)}, u32[]{:S(2)}, u32[]{:S(2)}) collective-permute-start(bf16[64,2048]{1,0:T(8,128)(2,1)} %a_ref.1), channel_id=1, source_target_pairs={{0,6},{1,25},{2,0},{3,27},{4,2},{5,29},{6,4},{7,31},{8,14},{9,1},{... | collective-permute-start | bytes 786440 | tf_op jit(solution)/shard_map/ppermute | solution.py:520
  31.9 8.8 %collective-permute-done.got_ref.got_b_ref = bf16[136,1536]{1,0:T(8,128)(2,1)S(1)} collective-permute-done((bf16[136,1536]{1,0:T(8,128)(2,1)S(1)}, bf16[136,1536]{1,0:T(8,128)(2,1)S(1)}, u32[]{:S(2)}, u32[]{:S(2)}) %collective-permute-start) | collective-permute-done | bytes 417824 | tf_op jit(solution)/shard_map/ppermute | solution.py:517
  40.7 0.2 early.1.steps_ref
  40.8 0.0 all-to-all-done.shared_ref
  40.9 0.0 copy-start.4
  40.9 0.7 copy-done.4
  41.6 0.0 copy-start.5
  41.6 3.0 %state.1 = (bf16[16,64,128]{2,1,0:T(8,128)(2,1)}, bf16[8,128,128]{2,1,0:T(8,128)(2,1)}, bf16[256,1024]{1,0:T(8,128)(2,1)}, bf16[256,512]{1,0:T(8,128)(2,1)}, f32[4,16,128]{2,1,0:T(8,128)}) custom-call(bf16[128,1536]{1,0:T(8,128)(2,1)S(1)} %get-tuple-element.19.own_ref.own_b_ref, bf16[128,1536]{1,0:T(8,128)(2,1)S(1)} %get-tuple-element.19.own_ref.own_b_ref, ...), custom_call_target="tpu_custom_call" | custom-call | flops 4000000000 | bytes 2000000 | tf_op jit(solution)/shard_map/state/pallas_call | solution.py:549
  44.5 10.6 %all-to-all-start.1 = ((bf16[16,64,128]{2,1,0:T(8,128)(2,1)}), bf16[16,64,128]{2,1,0:T(8,128)(2,1)S(1)}, u32[]{:S(2)}, u32[]{:S(2)}) async-start(bf16[16,64,128]{2,1,0:T(8,128)(2,1)} %get-tuple-element.22), calls=%async_computation.1 | async-start | bytes 524288 | tf_op jit(solution)/shard_map/all_to_all | solution.py:584
  55.2 0.0 collective-permute-done.4.c_ref
  55.2 0.0 collective-permute-done.3.b_ref
  55.2 0.0 collective-permute-done.5.d_ref
  55.2 0.0 copy-done.1
  55.2 0.1 join.1.refs_0_
  55.3 0.0 copy-start
  55.3 4.9 %collective-permute-start.8 = (bf16[256,2048]{1,0:T(8,128)(2,1)S(1)}, bf16[256,2048]{1,0:T(8,128)(2,1)}, u32[]{:S(2)}, u32[]{:S(2)}) collective-permute-start(bf16[256,2048]{1,0:T(8,128)(2,1)S(1)} %join.1.refs_0_), channel_id=1, source_target_pairs={{0,24},{1,7},{2,26},{3,1},{4,28},{5,3},{6,30},{7,5},{8,0},{9,15},{... | collective-permute-start | bytes 3145736 | tf_op jit(solution)/shard_map/ppermute | solution.py:530
  60.2 2.5 %collective-permute-start.7 = (bf16[256,2048]{1,0:T(8,128)(2,1)S(1)}, bf16[256,2048]{1,0:T(8,128)(2,1)}, u32[]{:S(2)}, u32[]{:S(2)}) collective-permute-start(bf16[256,2048]{1,0:T(8,128)(2,1)S(1)} %join.1.refs_0_), channel_id=1, source_target_pairs={{0,16},{1,5},{2,18},{3,7},{4,20},{5,1},{6,22},{7,3},{8,24},{9,13},... | collective-permute-start | bytes 3145736 | tf_op jit(solution)/shard_map/ppermute | solution.py:530
  62.8 2.9 %collective-permute-start.6 = (bf16[256,2048]{1,0:T(8,128)(2,1)S(1)}, bf16[256,2048]{1,0:T(8,128)(2,1)}, u32[]{:S(2)}, u32[]{:S(2)}) collective-permute-start(bf16[256,2048]{1,0:T(8,128)(2,1)S(1)} %join.1.refs_0_), channel_id=1, source_target_pairs={{0,8},{1,3},{2,10},{3,5},{4,12},{5,7},{6,14},{7,1},{8,16},{9,11},{... | collective-permute-start | bytes 3145736 | tf_op jit(solution)/shard_map/ppermute | solution.py:530
  65.7 8.0 %all-to-all-done.1.local_ref = bf16[16,64,128]{2,1,0:T(8,128)(2,1)S(1)} async-done(((bf16[16,64,128]{2,1,0:T(8,128)(2,1)}), bf16[16,64,128]{2,1,0:T(8,128)(2,1)S(1)}, u32[]{:S(2)}, u32[]{:S(2)}) %all-to-all-start.1) | async-done | bytes 262176 | tf_op jit(solution)/shard_map/all_to_all | solution.py:584
  73.7 0.9 scan.1
  74.6 5.6 %all-to-all-start.2 = ((bf16[16,64,128]{2,1,0:T(8,128)(2,1)}), bf16[16,64,128]{2,1,0:T(8,128)(2,1)}, u32[]{:S(2)}, u32[]{:S(2)}) async-start(bf16[16,64,128]{2,1,0:T(8,128)(2,1)} %scan.1), calls=%async_computation.2 | async-start | bytes 524288 | tf_op jit(solution)/shard_map/all_to_all | solution.py:621
  80.2 1.9 %collective-permute-start.9 = (bf16[256,2048]{1,0:T(8,128)(2,1)S(1)}, bf16[256,2048]{1,0:T(8,128)(2,1)S(1)}, u32[]{:S(2)}, u32[]{:S(2)}) collective-permute-start(bf16[256,2048]{1,0:T(8,128)(2,1)S(1)} %join.1.refs_0_), channel_id=1, source_target_pairs={{0,1},{1,0},{2,3},{3,2},{4,5},{5,4},{6,7},{7,6},{8,9},{9,8},{10,11... | collective-permute-start | bytes 3145736 | tf_op jit(solution)/shard_map/ppermute | solution.py:531
  82.1 1.6 %collective-permute-done.8.refs_3_ = bf16[256,2048]{1,0:T(8,128)(2,1)} collective-permute-done((bf16[256,2048]{1,0:T(8,128)(2,1)S(1)}, bf16[256,2048]{1,0:T(8,128)(2,1)}, u32[]{:S(2)}, u32[]{:S(2)}) %collective-permute-start.8) | collective-permute-done | bytes 1048608 | tf_op jit(solution)/shard_map/ppermute | solution.py:530
  83.8 1.9 %collective-permute-start.12 = (bf16[256,2048]{1,0:T(8,128)(2,1)}, bf16[256,2048]{1,0:T(8,128)(2,1)S(1)}, u32[]{:S(2)}, u32[]{:S(2)}) collective-permute-start(bf16[256,2048]{1,0:T(8,128)(2,1)} %collective-permute-done.8.refs_3_), channel_id=1, source_target_pairs={{0,1},{1,0},{2,3},{3,2},{4,5},{5,4},{6,7},{7,6},{8,9},{9,8},{10,11... | collective-permute-start | bytes 3145736 | tf_op jit(solution)/shard_map/ppermute | solution.py:531
  85.7 0.0 collective-permute-done.7.refs_2_
  85.7 2.4 %collective-permute-start.11 = (bf16[256,2048]{1,0:T(8,128)(2,1)}, bf16[256,2048]{1,0:T(8,128)(2,1)}, u32[]{:S(2)}, u32[]{:S(2)}) collective-permute-start(bf16[256,2048]{1,0:T(8,128)(2,1)} %collective-permute-done.7.refs_2_), channel_id=1, source_target_pairs={{0,1},{1,0},{2,3},{3,2},{4,5},{5,4},{6,7},{7,6},{8,9},{9,8},{10,11... | collective-permute-start | bytes 3145736 | tf_op jit(solution)/shard_map/ppermute | solution.py:531
  88.1 1.7 %collective-permute-done.6.refs_1_ = bf16[256,2048]{1,0:T(8,128)(2,1)} collective-permute-done((bf16[256,2048]{1,0:T(8,128)(2,1)S(1)}, bf16[256,2048]{1,0:T(8,128)(2,1)}, u32[]{:S(2)}, u32[]{:S(2)}) %collective-permute-start.6) | collective-permute-done | bytes 1048608 | tf_op jit(solution)/shard_map/ppermute | solution.py:530
  89.8 1.9 %collective-permute-start.10 = (bf16[256,2048]{1,0:T(8,128)(2,1)}, bf16[256,2048]{1,0:T(8,128)(2,1)}, u32[]{:S(2)}, u32[]{:S(2)}) collective-permute-start(bf16[256,2048]{1,0:T(8,128)(2,1)} %collective-permute-done.6.refs_1_), channel_id=1, source_target_pairs={{0,1},{1,0},{2,3},{3,2},{4,5},{5,4},{6,7},{7,6},{8,9},{9,8},{10,11... | collective-permute-start | bytes 3145736 | tf_op jit(solution)/shard_map/ppermute | solution.py:531
  91.7 3.8 %collective-permute-start.1 = (bf16[128,512]{1,0:T(8,128)(2,1)}, bf16[128,512]{1,0:T(8,128)(2,1)S(1)}, u32[]{:S(2)}, u32[]{:S(2)}) collective-permute-start(bf16[128,512]{1,0:T(8,128)(2,1)} %copy-done.3), channel_id=1, source_target_pairs={{0,32},{32,0},{64,96},{96,64},{128,160},{160,128},{192,224},{224,1... | collective-permute-start | bytes 393224 | tf_op jit(solution)/shard_map/ppermute | solution.py:518
  95.5 4.4 %collective-permute-done.1.got_ref = bf16[128,512]{1,0:T(8,128)(2,1)S(1)} collective-permute-done((bf16[128,512]{1,0:T(8,128)(2,1)}, bf16[128,512]{1,0:T(8,128)(2,1)S(1)}, u32[]{:S(2)}, u32[]{:S(2)}) %collective-permute-start.1) | collective-permute-done | bytes 131104 | tf_op jit(solution)/shard_map/ppermute | solution.py:518
  99.9 0.0 copy-done.5
  99.9 4.6 %inner.1 = (bf16[256,512]{1,0:T(8,128)(2,1)}, f32[256,1024]{1,0:T(8,128)}) custom-call(bf16[128,512]{1,0:T(8,128)(2,1)S(1)} %get-tuple-element.24.own_ref, bf16[128,512]{1,0:T(8,128)(2,1)S(1)} %collective-permute-done.1.got_ref, bf16[16,64,128]{2,1,0:T(8,128)(2,1)S(1)} %all-to-all-done.shared_ref, bf16[4,1024]{1,0:T(4,128)(2,1)S(1)} %copy-done.5, ...), custom_call_target="tpu_custom_call" | custom-call | flops 4000000000 | bytes 2000000 | tf_op jit(solution)/shard_map/inner/pallas_call | solution.py:586
  104.5 0.0 copy-done
  104.5 0.0 all-to-all-done.2
  104.5 1.9 %give.1 = bf16[128,1024]{1,0:T(8,128)(2,1)S(1)} custom-call(bf16[8,128,128]{2,1,0:T(8,128)(2,1)} %bitcast.6.ent_ref, bf16[8,128,128]{2,1,0:T(8,128)(2,1)} %get-tuple-element.23.first_ref, bf16[256,512]{1,0:T(8,128)(2,1)} %get-tuple-element.29.cin_ref, f32[256,1024]{1,0:T(8,128)} %get-tuple-element.30.inner_ref, f32[4,16,128]{2,1,0:T(8,128)} %get-tuple-element.28.cum_ref), custom_call_target="tpu_custom_call" | custom-call | flops 1000000000 | bytes 1000000 | tf_op jit(solution)/shard_map/give/pallas_call | solution.py:645
  106.5 0.0 copy-start.2
  106.5 0.0 copy-start.6
  106.5 3.8 %collective-permute-start.2 = (bf16[128,1024]{1,0:T(8,128)(2,1)S(1)}, bf16[128,1024]{1,0:T(8,128)(2,1)S(1)}, u32[]{:S(2)}, u32[]{:S(2)}) collective-permute-start(bf16[128,1024]{1,0:T(8,128)(2,1)S(1)} %give.1), channel_id=1, source_target_pairs={{0,32},{32,0},{64,96},{96,64},{128,160},{160,128},{192,224},{224,1... | collective-permute-start | bytes 786440 | tf_op jit(solution)/shard_map/ppermute | solution.py:655
  110.3 0.0 collective-permute-done.9.refs_4_
  110.3 0.0 collective-permute-done.12.refs_7_
  110.3 0.0 collective-permute-done.11.refs_6_
  110.3 0.0 collective-permute-done.10.refs_5_
  110.4 2.9 %hold.1.held_ref = bf16[2048,2048]{1,0:T(8,128)(2,1)S(1)} custom-call(bf16[256,2048]{1,0:T(8,128)(2,1)} %copy-done, bf16[256,2048]{1,0:T(8,128)(2,1)} %collective-permute-done.6.refs_1_, bf16[256,2048]{1,0:T(8,128)(2,1)} %collective-permute-done.7.refs_2_, bf16[256,2048]{1,0:T(8,128)(2,1)} %collective-permute-done.8.refs_3_, ...), custom_call_target="tpu_custom_call" | custom-call | flops 1000000 | bytes 16000000 | tf_op jit(solution)/shard_map/hold/pallas_call | solution.py:667
  113.3 2.6 %mine.1.near_ref = bf16[8,128,128]{2,1,0:T(8,128)(2,1)S(1)} custom-call(bf16[8,128,128]{2,1,0:T(8,128)(2,1)} %bitcast.6.ent_ref, bf16[8,128,128]{2,1,0:T(8,128)(2,1)} %get-tuple-element.23.first_ref, bf16[256,512]{1,0:T(8,128)(2,1)} %get-tuple-element.29.cin_ref, f32[256,1024]{1,0:T(8,128)} %get-tuple-element.30.inner_ref, ...), custom_call_target="tpu_custom_call" | custom-call | flops 2000000000 | bytes 1000000 | tf_op jit(solution)/shard_map/mine/pallas_call | solution.py:657
  115.9 0.7 collective-permute-done.2.core_ref
  116.5 0.0 copy-done.2
  116.5 0.0 copy-done.6
  116.5 2.6 %project.1 = bf16[128,2048]{1,0:T(8,128)(2,1)} custom-call(bf16[128,1024]{1,0:T(8,128)(2,1)S(1)} %collective-permute-done.2.core_ref, bf16[8,128,128]{2,1,0:T(8,128)(2,1)S(1)} %mine.1.near_ref, bf16[128,2048]{1,0:T(8,128)(2,1)S(1)} %bitcast.12, f32[1,2048]{1,0:T(1,128)S(1)} %bitcast.14, bf16[2048,2048]{1,0:T(8,128)(2,1)S(1)} %hold.1.held_ref), custom_call_target="tpu_custom_call" | custom-call | flops 4000000000 | bytes 10000000 | tf_op jit(solution)/shard_map/project/pallas_call | solution.py:677
Async XLA Ops:
  2.2 0.7 copy-start.3
  2.8 52.4 %copy-start.1 = (bf16[64,2048]{1,0:T(8,128)(2,1)S(1)}, bf16[64,2048]{1,0:T(8,128)(2,1)}, u32[]{:S(2)}) copy-start(bf16[64,2048]{1,0:T(8,128)(2,1)} %a_ref.1) | copy-start | bytes 786436
  2.8 38.0 %all-to-all-start = ((bf16[16,64,128]{2,1,0:T(8,128)(2,1)}), bf16[16,64,128]{2,1,0:T(8,128)(2,1)S(1)}, u32[]{:S(2)}, u32[]{:S(2)}) async-start(bf16[16,64,128]{2,1,0:T(8,128)(2,1)} %get-tuple-element.18), calls=%async_computation | async-start | bytes 524288 | tf_op jit(solution)/shard_map/all_to_all | solution.py:516
  18.2 22.5 %collective-permute-start = (bf16[136,1536]{1,0:T(8,128)(2,1)S(1)}, bf16[136,1536]{1,0:T(8,128)(2,1)S(1)}, u32[]{:S(2)}, u32[]{:S(2)}) collective-permute-start(bf16[136,1536]{1,0:T(8,128)(2,1)S(1)} %get-tuple-element.20), channel_id=1, source_target_pairs={{0,32},{32,0},{64,96},{96,64},{128,160},{160,128},{192,224},{224,1... | collective-permute-start | bytes 1253384 | tf_op jit(solution)/shard_map/ppermute | solution.py:517
  22.0 33.2 %collective-permute-start.4 = (bf16[64,2048]{1,0:T(8,128)(2,1)}, bf16[64,2048]{1,0:T(8,128)(2,1)S(1)}, u32[]{:S(2)}, u32[]{:S(2)}) collective-permute-start(bf16[64,2048]{1,0:T(8,128)(2,1)} %a_ref.1), channel_id=1, source_target_pairs={{0,4},{1,17},{2,6},{3,19},{4,0},{5,21},{6,2},{7,23},{8,12},{9,25},... | collective-permute-start | bytes 786440 | tf_op jit(solution)/shard_map/ppermute | solution.py:520
  26.1 29.1 %collective-permute-start.3 = (bf16[64,2048]{1,0:T(8,128)(2,1)}, bf16[64,2048]{1,0:T(8,128)(2,1)S(1)}, u32[]{:S(2)}, u32[]{:S(2)}) collective-permute-start(bf16[64,2048]{1,0:T(8,128)(2,1)} %a_ref.1), channel_id=1, source_target_pairs={{0,2},{1,9},{2,4},{3,11},{4,6},{5,13},{6,0},{7,15},{8,10},{9,17},{... | collective-permute-start | bytes 786440 | tf_op jit(solution)/shard_map/ppermute | solution.py:520
  28.0 27.2 %collective-permute-start.5 = (bf16[64,2048]{1,0:T(8,128)(2,1)}, bf16[64,2048]{1,0:T(8,128)(2,1)S(1)}, u32[]{:S(2)}, u32[]{:S(2)}) collective-permute-start(bf16[64,2048]{1,0:T(8,128)(2,1)} %a_ref.1), channel_id=1, source_target_pairs={{0,6},{1,25},{2,0},{3,27},{4,2},{5,29},{6,4},{7,31},{8,14},{9,1},{... | collective-permute-start | bytes 786440 | tf_op jit(solution)/shard_map/ppermute | solution.py:520
  40.9 0.7 copy-start.4
  41.6 58.3 %copy-start.5 = (bf16[4,1024]{1,0:T(4,128)(2,1)S(1)}, bf16[4,1024]{1,0:T(4,128)(2,1)}, u32[]{:S(2)}) copy-start(bf16[4,1024]{1,0:T(4,128)(2,1)} %tc_ref.1) | copy-start | bytes 24580
  44.5 29.2 %all-to-all-start.1 = ((bf16[16,64,128]{2,1,0:T(8,128)(2,1)}), bf16[16,64,128]{2,1,0:T(8,128)(2,1)S(1)}, u32[]{:S(2)}, u32[]{:S(2)}) async-start(bf16[16,64,128]{2,1,0:T(8,128)(2,1)} %get-tuple-element.22), calls=%async_computation.1 | async-start | bytes 524288 | tf_op jit(solution)/shard_map/all_to_all | solution.py:584
  55.3 49.2 %copy-start = (bf16[256,2048]{1,0:T(8,128)(2,1)}, bf16[256,2048]{1,0:T(8,128)(2,1)S(1)}, u32[]{:S(2)}) copy-start(bf16[256,2048]{1,0:T(8,128)(2,1)S(1)} %join.1.refs_0_) | copy-start | bytes 3145732
  55.3 28.5 %collective-permute-start.8 = (bf16[256,2048]{1,0:T(8,128)(2,1)S(1)}, bf16[256,2048]{1,0:T(8,128)(2,1)}, u32[]{:S(2)}, u32[]{:S(2)}) collective-permute-start(bf16[256,2048]{1,0:T(8,128)(2,1)S(1)} %join.1.refs_0_), channel_id=1, source_target_pairs={{0,24},{1,7},{2,26},{3,1},{4,28},{5,3},{6,30},{7,5},{8,0},{9,15},{... | collective-permute-start | bytes 3145736 | tf_op jit(solution)/shard_map/ppermute | solution.py:530
  60.2 25.4 %collective-permute-start.7 = (bf16[256,2048]{1,0:T(8,128)(2,1)S(1)}, bf16[256,2048]{1,0:T(8,128)(2,1)}, u32[]{:S(2)}, u32[]{:S(2)}) collective-permute-start(bf16[256,2048]{1,0:T(8,128)(2,1)S(1)} %join.1.refs_0_), channel_id=1, source_target_pairs={{0,16},{1,5},{2,18},{3,7},{4,20},{5,1},{6,22},{7,3},{8,24},{9,13},... | collective-permute-start | bytes 3145736 | tf_op jit(solution)/shard_map/ppermute | solution.py:530
  62.8 27.0 %collective-permute-start.6 = (bf16[256,2048]{1,0:T(8,128)(2,1)S(1)}, bf16[256,2048]{1,0:T(8,128)(2,1)}, u32[]{:S(2)}, u32[]{:S(2)}) collective-permute-start(bf16[256,2048]{1,0:T(8,128)(2,1)S(1)} %join.1.refs_0_), channel_id=1, source_target_pairs={{0,8},{1,3},{2,10},{3,5},{4,12},{5,7},{6,14},{7,1},{8,16},{9,11},{... | collective-permute-start | bytes 3145736 | tf_op jit(solution)/shard_map/ppermute | solution.py:530
  74.6 29.9 %all-to-all-start.2 = ((bf16[16,64,128]{2,1,0:T(8,128)(2,1)}), bf16[16,64,128]{2,1,0:T(8,128)(2,1)}, u32[]{:S(2)}, u32[]{:S(2)}) async-start(bf16[16,64,128]{2,1,0:T(8,128)(2,1)} %scan.1), calls=%async_computation.2 | async-start | bytes 524288 | tf_op jit(solution)/shard_map/all_to_all | solution.py:621
  80.2 30.1 %collective-permute-start.9 = (bf16[256,2048]{1,0:T(8,128)(2,1)S(1)}, bf16[256,2048]{1,0:T(8,128)(2,1)S(1)}, u32[]{:S(2)}, u32[]{:S(2)}) collective-permute-start(bf16[256,2048]{1,0:T(8,128)(2,1)S(1)} %join.1.refs_0_), channel_id=1, source_target_pairs={{0,1},{1,0},{2,3},{3,2},{4,5},{5,4},{6,7},{7,6},{8,9},{9,8},{10,11... | collective-permute-start | bytes 3145736 | tf_op jit(solution)/shard_map/ppermute | solution.py:531
  83.8 26.6 %collective-permute-start.12 = (bf16[256,2048]{1,0:T(8,128)(2,1)}, bf16[256,2048]{1,0:T(8,128)(2,1)S(1)}, u32[]{:S(2)}, u32[]{:S(2)}) collective-permute-start(bf16[256,2048]{1,0:T(8,128)(2,1)} %collective-permute-done.8.refs_3_), channel_id=1, source_target_pairs={{0,1},{1,0},{2,3},{3,2},{4,5},{5,4},{6,7},{7,6},{8,9},{9,8},{10,11... | collective-permute-start | bytes 3145736 | tf_op jit(solution)/shard_map/ppermute | solution.py:531
  85.7 24.6 %collective-permute-start.11 = (bf16[256,2048]{1,0:T(8,128)(2,1)}, bf16[256,2048]{1,0:T(8,128)(2,1)}, u32[]{:S(2)}, u32[]{:S(2)}) collective-permute-start(bf16[256,2048]{1,0:T(8,128)(2,1)} %collective-permute-done.7.refs_2_), channel_id=1, source_target_pairs={{0,1},{1,0},{2,3},{3,2},{4,5},{5,4},{6,7},{7,6},{8,9},{9,8},{10,11... | collective-permute-start | bytes 3145736 | tf_op jit(solution)/shard_map/ppermute | solution.py:531
  89.8 20.6 %collective-permute-start.10 = (bf16[256,2048]{1,0:T(8,128)(2,1)}, bf16[256,2048]{1,0:T(8,128)(2,1)}, u32[]{:S(2)}, u32[]{:S(2)}) collective-permute-start(bf16[256,2048]{1,0:T(8,128)(2,1)} %collective-permute-done.6.refs_1_), channel_id=1, source_target_pairs={{0,1},{1,0},{2,3},{3,2},{4,5},{5,4},{6,7},{7,6},{8,9},{9,8},{10,11... | collective-permute-start | bytes 3145736 | tf_op jit(solution)/shard_map/ppermute | solution.py:531
  91.7 8.2 %collective-permute-start.1 = (bf16[128,512]{1,0:T(8,128)(2,1)}, bf16[128,512]{1,0:T(8,128)(2,1)S(1)}, u32[]{:S(2)}, u32[]{:S(2)}) collective-permute-start(bf16[128,512]{1,0:T(8,128)(2,1)} %copy-done.3), channel_id=1, source_target_pairs={{0,32},{32,0},{64,96},{96,64},{128,160},{160,128},{192,224},{224,1... | collective-permute-start | bytes 393224 | tf_op jit(solution)/shard_map/ppermute | solution.py:518
  106.5 10.1 %copy-start.2 = (bf16[1,128,2048]{2,1,0:T(8,128)(2,1)S(1)}, bf16[1,128,2048]{2,1,0:T(8,128)(2,1)}, u32[]{:S(2)}) copy-start(bf16[1,128,2048]{2,1,0:T(8,128)(2,1)} %param.14) | copy-start | bytes 1572868
  106.5 10.1 %copy-start.6 = (f32[2048]{0:T(1024)S(1)}, f32[2048]{0:T(1024)}, u32[]{:S(2)}) copy-start(f32[2048]{0:T(1024)} %param.20) | copy-start | bytes 24580
  106.5 10.1 %collective-permute-start.2 = (bf16[128,1024]{1,0:T(8,128)(2,1)S(1)}, bf16[128,1024]{1,0:T(8,128)(2,1)S(1)}, u32[]{:S(2)}, u32[]{:S(2)}) collective-permute-start(bf16[128,1024]{1,0:T(8,128)(2,1)S(1)} %give.1), channel_id=1, source_target_pairs={{0,32},{32,0},{64,96},{96,64},{128,160},{160,128},{192,224},{224,1... | collective-permute-start | bytes 786440 | tf_op jit(solution)/shard_map/ppermute | solution.py:655
